TPU v7x, 512 devices: a whole 4x4x16 slice. The times are simulated.
512 devices in a mesh: fs: 16 (over y, x), tp: 32 (over z, core).
Axes of the slice: x: 4, y: 4, z: 16, core: 2. Of those that a mesh axis runs over, the one named last changes fastest.
Arguments:
- inputs: bfloat16 [6144, 2048], P('fs'), may hold values from -6 to 6
- pre_act: bfloat16 [6144, 8192], P('fs', 'tp'), may hold values from -6 to 6
- cotangent: bfloat16 [6144, 2048], P('fs'), may hold values from -6 to 6
- up_weight: bfloat16 [2048, 8192], P('fs', 'tp'), may hold values from -0.125 to 0.125
- down_weight: bfloat16 [8192, 2048], P('tp', 'fs'), may hold values from -0.0625 to 0.0625
Outputs:
- input_grad: bfloat16 [6144, 2048], P('fs')
- up_grad: float32 [2048, 8192], P('fs', 'tp')
- down_grad: float32 [8192, 2048], P('tp', 'fs')
- up_norms: float32 [2048], P('fs')
- down_norms: float32 [8192], P('tp')
All inputs are finite; a program needn't handle non-finite values.
Results may differ from a plain program's by a relative error of at most 0.0051.
Values may be sent and summed in bfloat16 or wider, within the bound.
No kernel may reach another device: no remote copies, remote signals or barrier semaphores. Data moves between devices by JAX's collectives and lax.ppermute only.
A program may use at most 64 MiB of HBM per device.

v0:
```python
import jax
import jax.numpy as jnp
from jax import lax
from jax.sharding import Mesh
from jax.sharding import PartitionSpec as P

FS = ("fs_0", "fs_1")


def laid_out(blocks, dim):
    dims = list(blocks.shape[1:])
    dims[dim] *= blocks.shape[0]
    return jnp.moveaxis(blocks, 0, dim).reshape(dims)


def from_everyone(array, axis):
    count = lax.axis_size(axis)
    return lax.all_to_all(
        jnp.broadcast_to(array[None], (count, *array.shape)), axis, 0, 0, tiled=True
    )


def gather_directly(array, axis, dim):
    return laid_out(from_everyone(array, axis), dim)


def in_blocks(array, dim, count):
    dims = array.shape
    blocks = array.reshape(*dims[:dim], count, dims[dim] // count, *dims[dim + 1 :])
    return jnp.moveaxis(blocks, dim, 0)


def sum_at_owner(array, axis, dim):
    count = lax.axis_size(axis)
    blocks = lax.all_to_all(in_blocks(array, dim, count), axis, 0, 0, tiled=True)
    return jnp.sum(blocks.astype(jnp.float32), axis=0)


def over_copies(array, axis):
    everything = from_everyone(array, axis)
    return jnp.sum(everything, axis=0)


def by_axis(array, axes):
    for axis in axes:
        array = lax.psum(array, axis)
    return array


def contract_last(left, right):
    return lax.dot_general(
        left, right, (((1,), (1,)), ((), ())), preferred_element_type=jnp.float32
    )


def contract_first(left, right):
    return lax.dot_general(
        left, right, (((0,), (0,)), ((), ())), preferred_element_type=jnp.float32
    )


def local(inputs, pre_act, cotangent, up_weight, down_weight):
    active = jnp.maximum(pre_act.astype(jnp.float32), 0.0)
    squared = (active * active).astype(jnp.bfloat16)
    columns = cotangent
    sq_grad = contract_last(columns, gather_directly(down_weight, FS, 1))
    pre_grad = (2.0 * active * sq_grad).astype(jnp.bfloat16)
    partial_value = contract_last(pre_grad, gather_directly(up_weight, FS, 0))
    input_grad = lax.psum(partial_value, "tp").astype(jnp.bfloat16)
    columns = inputs
    up_grad = sum_at_owner(contract_first(columns, pre_grad).astype(jnp.bfloat16), FS, 0)
    down_grad = sum_at_owner(contract_first(squared, cotangent).astype(jnp.bfloat16), FS, 1)
    up_norms = over_copies(jnp.sum(up_grad * up_grad, axis=1), "tp")
    down_norms = by_axis(jnp.sum(down_grad * down_grad, axis=1), FS)
    return (input_grad, up_grad, down_grad, up_norms, down_norms)


def solution(mesh):
    split = Mesh(mesh.devices.reshape(4, 4, mesh.shape["tp"]), ("fs_0", "fs_1", "tp"))
    return jax.shard_map(
        local,
        mesh=split,
        in_specs=(P(FS, None), P(FS, "tp"), P(FS, None), P(FS, "tp"), P("tp", FS)),
        out_specs=(P(FS, None), P(FS, "tp"), P("tp", FS), P(FS), P("tp")),
        check_vma=False,
    )
```

profile of v0, /device:TPU:1, one launch (start us, length us, event | category | flops | bytes accessed | tf_op | source)
XLA Modules:
  0.0 225.1 jit_solution(1907114211853007547)
XLA Ops:
  0.6 0.0 copy-start
  0.6 1.1 copy.21
  1.7 0.0 copy-start.6
  1.7 0.1 broadcast_in_dim.6
  1.8 22.2 %all_to_all.26 = bf16[16,256,128]{1,2,0:T(8,128)(2,1)} all-to-all(bf16[16,256,128]{1,2,0:T(8,128)(2,1)S(1)} %broadcast_in_dim.6), channel_id=1, replica_groups=mesh['fs_0'=4,'fs_1'=4,'tp'=32] {'fs_0','fs_1'}, dimensions={0} | all-to-all | bytes 2097152 | tf_op jit(solution)/shard_map/all_to_all | solution.py:18
  24.0 0.0 copy-done.6
  24.0 0.0 copy-start.5
  24.0 1.1 broadcast_in_dim.7
  25.1 3.7 %all-to-all-start.1 = ((bf16[16,128,256]{2,1,0:T(8,128)(2,1)}), bf16[16,128,256]{2,1,0:T(8,128)(2,1)S(1)}, u32[]{:S(2)}, u32[]{:S(2)}) async-start(bf16[16,128,256]{2,1,0:T(8,128)(2,1)} %broadcast_in_dim.7), calls=%async_computation.1 | async-start | bytes 2097152 | tf_op jit(solution)/shard_map/all_to_all | solution.py:18
  28.7 0.0 copy-done
  28.7 0.0 copy-done.5
  28.7 0.7 fusion.1
  29.5 1.2 copy.32
  30.7 11.8 %all-to-all-done.1 = bf16[16,128,256]{2,1,0:T(8,128)(2,1)S(1)} async-done(((bf16[16,128,256]{2,1,0:T(8,128)(2,1)}), bf16[16,128,256]{2,1,0:T(8,128)(2,1)S(1)}, u32[]{:S(2)}, u32[]{:S(2)}) %all-to-all-start.1) | async-done | bytes 1048608 | tf_op jit(solution)/shard_map/all_to_all | solution.py:18
  42.5 0.0 copy-start.1
  42.5 1.0 copy-done.1
  43.5 3.8 %all-to-all-start.3 = ((bf16[16,256,128]{2,1,0:T(8,128)(2,1)}), bf16[16,256,128]{2,1,0:T(8,128)(2,1)S(1)}, u32[]{:S(2)}, u32[]{:S(2)}) async-start(bf16[16,256,128]{2,1,0:T(8,128)(2,1)} %bitcast.26), calls=%async_computation.3 | async-start | bytes 2097152 | tf_op jit(solution)/shard_map/all_to_all | solution.py:35
  47.3 0.0 copy-start.3
  47.3 1.9 fusion.2
  49.2 0.0 copy-done.3
  49.3 0.7 fusion
  50.0 0.0 copy-start.2
  50.0 1.3 copy.33
  51.3 0.0 copy-done.2
  51.3 2.3 %fusion.5 = f32[384,2048]{1,0:T(8,128)} fusion(bf16[384,256]{1,0:T(8,128)(2,1)S(1)} %fusion.2, bf16[2048,256]{1,0:T(8,128)(2,1)S(1)} %bitcast.28), kind=kOutput, calls=%fused_computation.16 | convolution fusion | flops 402653184 | bytes 4390912 | tf_op jit(solution)/shard_map/dot_general | solution.py:51
  53.5 7.3 %all-to-all-done.3 = bf16[16,256,128]{2,1,0:T(8,128)(2,1)S(1)} async-done(((bf16[16,256,128]{2,1,0:T(8,128)(2,1)}), bf16[16,256,128]{2,1,0:T(8,128)(2,1)S(1)}, u32[]{:S(2)}, u32[]{:S(2)}) %all-to-all-start.3) | async-done | bytes 1048608 | tf_op jit(solution)/shard_map/all_to_all | solution.py:35
  60.9 4.4 %all-to-all-start.2 = ((bf16[16,128,256]{1,2,0:T(8,128)(2,1)}), bf16[16,128,256]{1,2,0:T(8,128)(2,1)}, u32[]{:S(2)}, u32[]{:S(2)}) async-start(bf16[16,128,256]{1,2,0:T(8,128)(2,1)} %bitcast.27), calls=%async_computation.2 | async-start | bytes 2097152 | tf_op jit(solution)/shard_map/all_to_all | solution.py:35
  65.2 126.2 %all-reduce.1 = bf16[384,2048]{1,0:T(8,128)(2,1)} all-reduce(f32[384,2048]{1,0:T(8,128)} %fusion.5), channel_id=1, replica_groups=mesh['fs_0'=4,'fs_1'=4,'tp'=32] {'tp'}, use_global_device_ids=true, to_apply=%region_0.0 | all-reduce | flops 786432 | bytes 4718592 | tf_op jit(solution)/shard_map/psum | solution.py:69
  191.4 0.1 convert_reduce_fusion
  191.5 0.0 copy-start.4
  191.6 0.0 all-to-all-done.2
  191.6 1.4 convert_reduce_fusion.1
  193.0 0.6 broadcast_in_dim.8
  193.6 12.2 %all-to-all-start.4 = ((f32[32,1,128]{2,1,0:T(1,128)}), f32[32,1,128]{2,1,0:T(1,128)S(1)}, u32[]{:S(2)}, u32[]{:S(2)}) async-start(f32[32,1,128]{2,1,0:T(1,128)} %broadcast_in_dim.8), calls=%async_computation.4 | async-start | bytes 32768 | tf_op jit(solution)/shard_map/all_to_all | solution.py:18
  205.8 0.1 multiply_reduce_fusion
  205.9 8.9 %psum.22 = f32[256]{0:T(256)S(1)} all-reduce(f32[256]{0:T(256)S(1)} %multiply_reduce_fusion), channel_id=1, replica_groups=mesh['fs_0'=4,'fs_1'=4,'tp'=32] {'fs_0'}, use_global_device_ids=true, to_apply=%region_6.0 | all-reduce | flops 256 | bytes 2048 | tf_op jit(solution)/shard_map/psum | solution.py:46
  214.8 8.9 %psum.23 = f32[256]{0:T(256)} all-reduce(f32[256]{0:T(256)S(1)} %psum.22), channel_id=1, replica_groups=mesh['fs_0'=4,'fs_1'=4,'tp'=32] {'fs_1'}, use_global_device_ids=true, to_apply=%region_7.0 | all-reduce | flops 256 | bytes 2048 | tf_op jit(solution)/shard_map/psum | solution.py:46
  223.8 0.8 copy.26
  224.5 0.0 all-to-all-done.4
  224.5 0.5 reduce_sum.48
  225.1 0.0 copy-done.4
  (1 shorter events, 0.0 us)
Async XLA Ops:
  0.6 28.1 %copy-start = (bf16[384,2048]{1,0:T(8,128)(2,1)S(1)}, bf16[384,2048]{1,0:T(8,128)(2,1)}, u32[]{:S(2)}) copy-start(bf16[384,2048]{1,0:T(8,128)(2,1)} %param.7) | copy-start | bytes 4718596
  1.7 22.3 %copy-start.6 = (bf16[128,256]{1,0:T(8,128)(2,1)S(1)}, bf16[128,256]{1,0:T(8,128)(2,1)}, u32[]{:S(2)}) copy-start(bf16[128,256]{1,0:T(8,128)(2,1)} %param.8) | copy-start | bytes 196612
  24.0 4.8 %copy-start.5 = (bf16[384,256]{1,0:T(8,128)(2,1)S(1)}, bf16[384,256]{1,0:T(8,128)(2,1)}, u32[]{:S(2)}) copy-start(bf16[384,256]{1,0:T(8,128)(2,1)} %param.6) | copy-start | bytes 589828
  25.1 17.5 %all-to-all-start.1 = ((bf16[16,128,256]{2,1,0:T(8,128)(2,1)}), bf16[16,128,256]{2,1,0:T(8,128)(2,1)S(1)}, u32[]{:S(2)}, u32[]{:S(2)}) async-start(bf16[16,128,256]{2,1,0:T(8,128)(2,1)} %broadcast_in_dim.7), calls=%async_computation.1 | async-start | bytes 2097152 | tf_op jit(solution)/shard_map/all_to_all | solution.py:18
  42.5 1.0 copy-start.1
  43.5 17.4 %all-to-all-start.3 = ((bf16[16,256,128]{2,1,0:T(8,128)(2,1)}), bf16[16,256,128]{2,1,0:T(8,128)(2,1)S(1)}, u32[]{:S(2)}, u32[]{:S(2)}) async-start(bf16[16,256,128]{2,1,0:T(8,128)(2,1)} %bitcast.26), calls=%async_computation.3 | async-start | bytes 2097152 | tf_op jit(solution)/shard_map/all_to_all | solution.py:35
  47.3 1.9 copy-start.3
  50.0 1.3 copy-start.2
  60.9 130.7 %all-to-all-start.2 = ((bf16[16,128,256]{1,2,0:T(8,128)(2,1)}), bf16[16,128,256]{1,2,0:T(8,128)(2,1)}, u32[]{:S(2)}, u32[]{:S(2)}) async-start(bf16[16,128,256]{1,2,0:T(8,128)(2,1)} %bitcast.27), calls=%async_computation.2 | async-start | bytes 2097152 | tf_op jit(solution)/shard_map/all_to_all | solution.py:35
  191.5 33.5 %copy-start.4 = (f32[256,128]{1,0:T(8,128)}, f32[256,128]{1,0:T(8,128)S(1)}, u32[]{:S(2)}) copy-start(f32[256,128]{1,0:T(8,128)S(1)} %convert_reduce_fusion) | copy-start | bytes 393220
  193.6 30.9 %all-to-all-start.4 = ((f32[32,1,128]{2,1,0:T(1,128)}), f32[32,1,128]{2,1,0:T(1,128)S(1)}, u32[]{:S(2)}, u32[]{:S(2)}) async-start(f32[32,1,128]{2,1,0:T(1,128)} %broadcast_in_dim.8), calls=%async_computation.4 | async-start | bytes 32768 | tf_op jit(solution)/shard_map/all_to_all | solution.py:18
where the time goes:
time: 228 us; the launch traced here: 225 us
  blocking collectives  166 us (73%)
  starting transfers between devices  24 us (11%)
  waiting for transfers between devices  19.1 us (8%)
  local copies, waits for them, and re-layouts  7.1 us (3%)
  matrix products  5.65 us (2%)
    psum x1, blocking collectives, local(): input_grad = lax.psum(partial_value, 'tp').astype(jnp.bfloat16)  126 us
    all_to_all x1, blocking collectives, from_everyone(): lax.all_to_all(jnp.broadcast_to(array[None], (count, *array.shape)), axis...  22.2 us
    psum x2, blocking collectives, by_axis(): array = lax.psum(array, axis)  17.9 us
    all_to_all x2, starting transfers between devices, from_everyone(): lax.all_to_all(jnp.broadcast_to(array[None], (count, *array.shape)), axis...  15.8 us
    all_to_all x2, waiting for transfers between devices, from_everyone(): lax.all_to_all(jnp.broadcast_to(array[None], (count, *array.shape)), axis...  11.8 us
    all_to_all x2, starting transfers between devices, sum_at_owner(): lax.all_to_all(in_blocks(array, dim, count), axis, 0, 0, tiled=True)  8.17 us
    all_to_all x2, waiting for transfers between devices, sum_at_owner(): lax.all_to_all(in_blocks(array, dim, count), axis, 0, 0, tiled=True)  7.32 us
  transfers between devices with their start and end apart: 4, of which 2 were waited for; matrix products, arithmetic and copies ran while one was open for 4% of the time, Pallas kernels for 0%

commit v1 on v0

v1 whole, which is shorter than its diff:
```python
import jax
import jax.numpy as jnp
from jax import lax
from jax.sharding import Mesh
from jax.sharding import PartitionSpec as P

FS = ("y", "xh", "xl")
TP = ("zh", "zl", "core")
BF = jnp.bfloat16
F32 = jnp.float32


def from_everyone(array, axes):
    count = lax.axis_size(axes)
    return lax.all_to_all(
        jnp.broadcast_to(array[None], (count, *array.shape)), axes, 0, 0, tiled=True
    )


def exchange(array, axes):
    return lax.all_to_all(array, axes, 0, 0, tiled=True)


def other_core(array):
    return lax.ppermute(array, "core", [(0, 1), (1, 0)])


def dot(left, right, over):
    return lax.dot_general(
        left, right, ((over[:1], over[1:]), ((), ())), preferred_element_type=F32
    )


def local(inputs, pre_act, cotangent, up_weight, down_weight):
    tokens, width = inputs.shape
    hidden = pre_act.shape[1]
    core = lax.axis_index("core")
    active = jnp.maximum(pre_act.astype(F32), 0.0)
    squared = (active * active).astype(BF)

    down_columns = from_everyone(down_weight.T, FS).reshape(width, hidden)
    rows = lax.ppermute(up_weight, ("xl", "core"), [(0, 0), (1, 2), (2, 3), (3, 1)])
    up_rows = from_everyone(rows, ("xl", "y", "xh")).reshape(2, width // 2, hidden)

    sq_grad = dot(cotangent, down_columns, (1, 0))
    pre_grad = (2.0 * active * sq_grad).astype(BF)
    theirs = other_core(pre_grad)
    half = (dot(pre_grad, up_rows[0], (1, 1)) + dot(theirs, up_rows[1], (1, 1))).astype(BF)

    for axis in ("zl", "zh"):
        count = lax.axis_size(axis)
        pieces = half.reshape(count, half.shape[0] // count, half.shape[1])
        half = jnp.sum(exchange(pieces, axis).astype(F32), axis=0).astype(BF)
    half = lax.all_gather(half, "zh", axis=0, tiled=True)
    half = lax.all_gather(half, "zl", axis=0, tiled=True)
    both = other_core(half)
    first = jnp.where(core == 0, half, both).reshape(tokens, width // 256, 1, 128)
    second = jnp.where(core == 0, both, half).reshape(tokens, width // 256, 1, 128)
    input_grad = jnp.concatenate([first, second], axis=2).reshape(tokens, width)

    count = lax.axis_size(FS)
    down_part = dot(cotangent, squared, (0, 0)).astype(BF).reshape(count, width // count, hidden)
    down_grad = jnp.sum(exchange(down_part, FS).astype(F32), axis=0)
    up_part = dot(inputs, pre_grad, (0, 0)).astype(BF).reshape(count, width // count, hidden)
    up_grad = jnp.sum(exchange(up_part, FS).astype(F32), axis=0)

    down_norms = jnp.sum(from_everyone(jnp.sum(down_grad * down_grad, axis=0), FS), axis=0)
    up_norms = jnp.sum(from_everyone(jnp.sum(up_grad * up_grad, axis=1), TP), axis=0)
    return input_grad, up_grad, down_grad.T, up_norms, down_norms


def solution(mesh):
    split = Mesh(mesh.devices.reshape(4, 2, 2, 4, 4, 2), (*FS, *TP))
    return jax.shard_map(
        local,
        mesh=split,
        in_specs=(P(FS, None), P(FS, TP), P(FS, None), P(FS, TP), P(TP, FS)),
        out_specs=(P(FS, None), P(FS, TP), P(TP, FS), P(FS), P(TP)),
        check_vma=False,
    )
```

time: 228 us -> 208 us (0.912)
  blocking collectives: 166 us -> 31.4 us
  starting transfers between devices: 24 us -> 84 us
  waiting for transfers between devices: 19.1 us -> 67.9 us
  local copies, waits for them, and re-layouts: 7.1 us -> 11 us
  other arithmetic: 2.25 us -> 5.13 us
    psum x3 -> x0, blocking collectives: 144 us -> none  [the longest x1 126 us: local(): input_grad = lax.psum(partial_value, 'tp').astype(jnp.bfloat16)]
    all_to_all x4 -> x8, waiting for transfers between devices: 19.1 us -> 61.8 us  [the longest x4 40.2 us: exchange(): return lax.all_to_all(array, axes, 0, 0, tiled=True)]
    all_to_all x4 -> x8, starting transfers between devices: 24 us -> 63.4 us  [the longest x4 34.5 us: exchange(): return lax.all_to_all(array, axes, 0, 0, tiled=True)]
    all_gather x0 -> x2, blocking collectives: none -> 31.4 us  [the longest x1 16.8 us: local(): half = lax.all_gather(half, 'zh', axis=0, tiled=True)]
    all_to_all x1 -> x0, blocking collectives: 22.2 us -> none  [from_everyone(): lax.all_to_all(jnp.broadcast_to(array[None], (count, *array.shape)), axis...]
    ppermute x0 -> x3, starting transfers between devices: none -> 20.6 us  [the longest x2 14.2 us: other_core(): return lax.ppermute(array, 'core', [(0, 1), (1, 0)])]
    ppermute x0 -> x3, waiting for transfers between devices: none -> 6.09 us  [the longest x1 6.08 us: local(): lax.ppermute(up_weight, ('xl', 'core'), [(0, 0), (1, 2), (2, 3), (3, 1)])]
    dot_general x4 -> x5, matrix products: 5.65 us -> 6.48 us  [dot(): lax.dot_general(left, right, ((over[:1], over[1:]), ((), ())), preferred_...]
  transfers between devices with their start and end apart: 4 -> 11, of which waited for: 2 -> 8; matrix products, arithmetic and copies ran while one was open for 4% -> 7% of each run, Pallas kernels for 0% -> 0%
where the time goes in v1:
time: 208 us; the launch traced here: 207 us
  starting transfers between devices  84 us (40%)
  waiting for transfers between devices  67.9 us (33%)
  blocking collectives  31.4 us (15%)
  local copies, waits for them, and re-layouts  11 us (5%)
  matrix products  6.48 us (3%)
  other arithmetic  5.13 us (2%)
    all_to_all x4, waiting for transfers between devices, exchange(): return lax.all_to_all(array, axes, 0, 0, tiled=True)  40.2 us
    all_to_all x4, starting transfers between devices, exchange(): return lax.all_to_all(array, axes, 0, 0, tiled=True)  34.5 us
    all_to_all x4, starting transfers between devices, from_everyone(): lax.all_to_all(jnp.broadcast_to(array[None], (count, *array.shape)), axes...  28.9 us
    all_to_all x4, waiting for transfers between devices, from_everyone(): lax.all_to_all(jnp.broadcast_to(array[None], (count, *array.shape)), axes...  21.7 us
    all_gather x1, blocking collectives, local(): half = lax.all_gather(half, 'zh', axis=0, tiled=True)  16.8 us
    all_gather x1, blocking collectives, local(): half = lax.all_gather(half, 'zl', axis=0, tiled=True)  14.6 us
    ppermute x2, starting transfers between devices, other_core(): return lax.ppermute(array, 'core', [(0, 1), (1, 0)])  14.2 us
    dot_general x5, matrix products, dot(): lax.dot_general(left, right, ((over[:1], over[1:]), ((), ())), preferred_...  6.48 us
  transfers between devices with their start and end apart: 11, of which 8 were waited for; matrix products, arithmetic and copies ran while one was open for 7% of the time, Pallas kernels for 0%

profile of v1, /device:TPU:1, one launch (start us, length us, event | category | flops | bytes accessed | tf_op | source)
XLA Modules:
  0.0 206.8 jit_solution(1023969479651005177)
XLA Ops:
  0.6 0.0 copy-start
  0.6 1.1 copy.35
  1.7 0.0 copy-start.7
  1.7 1.1 broadcast_in_dim.8
  2.8 7.6 %all-to-all-start = ((bf16[16,128,256]{2,1,0:T(8,128)(2,1)}), bf16[16,128,256]{2,1,0:T(8,128)(2,1)S(1)}, u32[]{:S(2)}, u32[]{:S(2)}) async-start(bf16[16,128,256]{2,1,0:T(8,128)(2,1)} %broadcast_in_dim.8), calls=%async_computation | async-start | bytes 2097152 | tf_op jit(solution)/shard_map/all_to_all | solution.py:15
  10.4 0.0 copy-done.7
  10.4 0.0 copy-start.5
  10.4 6.4 %collective-permute-start = (bf16[128,256]{1,0:T(8,128)(2,1)S(1)}, bf16[128,256]{1,0:T(8,128)(2,1)S(1)}, u32[]{:S(2)}, u32[]{:S(2)}) collective-permute-start(bf16[128,256]{1,0:T(8,128)(2,1)S(1)} %copy-done.7), channel_id=1, source_target_pairs={{0,0},{1,32},{32,33},{33,1},{2,2},{3,34},{34,35},{35,3},{4,4},{5,3... | collective-permute-start | bytes 196616 | tf_op jit(solution)/shard_map/ppermute | solution.py:42
  16.8 6.1 %collective-permute-done = bf16[128,256]{1,0:T(8,128)(2,1)S(1)} collective-permute-done((bf16[128,256]{1,0:T(8,128)(2,1)S(1)}, bf16[128,256]{1,0:T(8,128)(2,1)S(1)}, u32[]{:S(2)}, u32[]{:S(2)}) %collective-permute-start) | collective-permute-done | bytes 65568 | tf_op jit(solution)/shard_map/ppermute | solution.py:42
  22.9 2.0 all-to-all-done
  24.8 0.0 copy-start.2
  24.8 1.2 broadcast_in_dim.9
  26.0 0.1 copy-done.2
  26.1 4.1 %all-to-all-start.1 = ((bf16[16,128,256]{2,1,0:T(8,128)(2,1)}), bf16[16,128,256]{2,1,0:T(8,128)(2,1)S(1)}, u32[]{:S(2)}, u32[]{:S(2)}) async-start(bf16[16,128,256]{2,1,0:T(8,128)(2,1)} %broadcast_in_dim.9), calls=%async_computation.1 | async-start | bytes 2097152 | tf_op jit(solution)/shard_map/all_to_all | solution.py:15
  30.3 0.0 copy-done
  30.3 0.0 copy-done.5
  30.3 1.8 fusion.2
  32.1 0.0 copy-start.3
  32.1 6.1 %collective-permute-start.1 = (bf16[384,256]{1,0:T(8,128)(2,1)S(1)}, bf16[384,256]{1,0:T(8,128)(2,1)S(1)}, u32[]{:S(2)}, u32[]{:S(2)}) collective-permute-start(bf16[384,256]{1,0:T(8,128)(2,1)S(1)} %fusion.2), channel_id=1, source_target_pairs={{0,1},{1,0},{2,3},{3,2},{4,5},{5,4},{6,7},{7,6},{8,9},{9,8},{10,11... | collective-permute-start | bytes 589832 | tf_op jit(solution)/shard_map/ppermute | solution.py:25
  38.2 4.3 %all-to-all-done.1 = bf16[16,128,256]{2,1,0:T(8,128)(2,1)S(1)} async-done(((bf16[16,128,256]{2,1,0:T(8,128)(2,1)}), bf16[16,128,256]{2,1,0:T(8,128)(2,1)S(1)}, u32[]{:S(2)}, u32[]{:S(2)}) %all-to-all-start.1) | async-done | bytes 1048608 | tf_op jit(solution)/shard_map/all_to_all | solution.py:15
  42.5 0.1 fusion.5
  42.6 0.0 collective-permute-done.1
  42.6 0.4 fusion.6
  43.0 0.0 copy-done.3
  43.0 0.0 copy-start.6
  43.0 1.3 add_convert_fusion
  44.3 9.0 %all-to-all-start.2 = ((bf16[4,96,1024]{2,1,0:T(8,128)(2,1)}), bf16[4,96,1024]{2,1,0:T(8,128)(2,1)S(1)}, u32[]{:S(2)}, u32[]{:S(2)}) async-start(bf16[4,96,1024]{2,1,0:T(8,128)(2,1)} %bitcast.4), calls=%async_computation.2 | async-start | bytes 1572864 | tf_op jit(solution)/shard_map/all_to_all | solution.py:21
  53.4 0.0 copy-done.6
  53.4 0.7 fusion.1
  54.1 1.2 copy.53
  55.4 16.7 %all-to-all-done.2 = bf16[4,96,1024]{2,1,0:T(8,128)(2,1)S(1)} async-done(((bf16[4,96,1024]{2,1,0:T(8,128)(2,1)}), bf16[4,96,1024]{2,1,0:T(8,128)(2,1)S(1)}, u32[]{:S(2)}, u32[]{:S(2)}) %all-to-all-start.2) | async-done | bytes 786464 | tf_op jit(solution)/shard_map/all_to_all | solution.py:21
  72.1 6.9 %all-to-all-start.5 = ((bf16[16,128,256]{1,2,0:T(8,128)(2,1)}), bf16[16,128,256]{1,2,0:T(8,128)(2,1)S(1)}, u32[]{:S(2)}, u32[]{:S(2)}) async-start(bf16[16,128,256]{1,2,0:T(8,128)(2,1)} %bitcast.34), calls=%async_computation.5 | async-start | bytes 2097152 | tf_op jit(solution)/shard_map/all_to_all | solution.py:21
  79.0 0.8 reduce_sum.78
  79.8 14.5 %all-to-all-done.5 = bf16[16,128,256]{1,2,0:T(8,128)(2,1)S(1)} async-done(((bf16[16,128,256]{1,2,0:T(8,128)(2,1)}), bf16[16,128,256]{1,2,0:T(8,128)(2,1)S(1)}, u32[]{:S(2)}, u32[]{:S(2)}) %all-to-all-start.5) | async-done | bytes 1048608 | tf_op jit(solution)/shard_map/all_to_all | solution.py:21
  94.3 12.6 %all-to-all-start.3 = ((bf16[4,24,1024]{2,1,0:T(8,128)(2,1)}), bf16[4,24,1024]{2,1,0:T(8,128)(2,1)S(1)}, u32[]{:S(2)}, u32[]{:S(2)}) async-start(bf16[4,24,1024]{2,1,0:T(8,128)(2,1)} %bitcast.40), calls=%async_computation.3 | async-start | bytes 393216 | tf_op jit(solution)/shard_map/all_to_all | solution.py:21
  106.9 2.3 %fusion = bf16[32,16,8,128]{3,2,1,0:T(8,128)(2,1)S(1)} fusion(bf16[384,256]{1,0:T(8,128)(2,1)} %copy-done.3, bf16[384,2048]{1,0:T(8,128)(2,1)} %param.5), kind=kOutput, calls=%fused_computation.6 | convolution fusion | flops 403177472 | bytes 2818048 | tf_op jit(solution)/shard_map/dot_general | solution.py:29
  109.2 1.2 copy.54
  110.4 9.0 %all-to-all-done.3 = bf16[4,24,1024]{2,1,0:T(8,128)(2,1)S(1)} async-done(((bf16[4,24,1024]{2,1,0:T(8,128)(2,1)}), bf16[4,24,1024]{2,1,0:T(8,128)(2,1)S(1)}, u32[]{:S(2)}, u32[]{:S(2)}) %all-to-all-start.3) | async-done | bytes 196640 | tf_op jit(solution)/shard_map/all_to_all | solution.py:21
  119.4 5.9 %all-to-all-start.4 = ((bf16[16,128,256]{1,2,0:T(8,128)(2,1)}), bf16[16,128,256]{1,2,0:T(8,128)(2,1)}, u32[]{:S(2)}, u32[]{:S(2)}) async-start(bf16[16,128,256]{1,2,0:T(8,128)(2,1)} %bitcast.33), calls=%async_computation.4 | async-start | bytes 2097152 | tf_op jit(solution)/shard_map/all_to_all | solution.py:21
  125.4 16.8 %all_gather.6 = bf16[96,1024]{1,0:T(8,128)(2,1)S(1)} all-gather(bf16[24,1024]{1,0:T(8,128)(2,1)S(1)} %reduce_sum.79), channel_id=1, replica_groups=mesh['y'=4,'xh'=2,'xl'=2,'zh'=4,'zl'=4,'core'=2] {'zh'}, dimensions={0}, use_global_device_ids=true | all-gather | bytes 245760 | tf_op jit(solution)/shard_map/all_gather | solution.py:54
  142.2 14.6 %all_gather.7 = bf16[384,1024]{1,0:T(8,128)(2,1)S(1)} all-gather(bf16[96,1024]{1,0:T(8,128)(2,1)S(1)} %all_gather.6), channel_id=1, replica_groups=mesh['y'=4,'xh'=2,'xl'=2,'zh'=4,'zl'=4,'core'=2] {'zl'}, dimensions={0}, use_global_device_ids=true | all-gather | bytes 983040 | tf_op jit(solution)/shard_map/all_gather | solution.py:55
  156.8 1.2 copy.37
  158.0 8.1 %collective-permute-start.2 = (bf16[384,1024]{0,1:T(8,128)(2,1)}, bf16[384,1024]{0,1:T(8,128)(2,1)}, u32[]{:S(2)}, u32[]{:S(2)}) collective-permute-start(bf16[384,1024]{0,1:T(8,128)(2,1)} %copy.37), channel_id=1, source_target_pairs={{0,1},{1,0},{2,3},{3,2},{4,5},{5,4},{6,7},{7,6},{8,9},{9,8},{10,11... | collective-permute-start | bytes 2359304 | tf_op jit(solution)/shard_map/ppermute | solution.py:25
  166.1 0.1 convert_reduce_fusion
  166.3 0.0 copy-start.4
  166.3 0.1 multiply_reduce_fusion
  166.4 0.0 all-to-all-done.4
  166.4 0.6 broadcast_in_dim.11
  167.0 8.9 %all-to-all-start.7 = ((f32[16,1,256]{2,1,0:T(1,128)}), f32[16,1,256]{2,1,0:T(1,128)S(1)}, u32[]{:S(2)}, u32[]{:S(2)}) async-start(f32[16,1,256]{2,1,0:T(1,128)} %broadcast_in_dim.11), calls=%async_computation.7 | async-start | bytes 32768 | tf_op jit(solution)/shard_map/all_to_all | solution.py:15
  175.9 1.4 convert_reduce_fusion.1
  177.4 5.0 %all-to-all-done.7 = f32[16,1,256]{2,1,0:T(1,128)S(1)} async-done(((f32[16,1,256]{2,1,0:T(1,128)}), f32[16,1,256]{2,1,0:T(1,128)S(1)}, u32[]{:S(2)}, u32[]{:S(2)}) %all-to-all-start.7) | async-done | bytes 16416 | tf_op jit(solution)/shard_map/all_to_all | solution.py:15
  182.4 0.6 broadcast_in_dim.10
  183.0 8.2 %all-to-all-start.6 = ((f32[32,1,128]{2,1,0:T(1,128)}), f32[32,1,128]{2,1,0:T(1,128)S(1)}, u32[]{:S(2)}, u32[]{:S(2)}) async-start(f32[32,1,128]{2,1,0:T(1,128)} %broadcast_in_dim.10), calls=%async_computation.6 | async-start | bytes 32768 | tf_op jit(solution)/shard_map/all_to_all | solution.py:15
  191.2 0.6 reduce_sum.85
  191.8 0.8 copy.46
  192.6 10.4 %all-to-all-done.6 = f32[32,1,128]{2,1,0:T(1,128)S(1)} async-done(((f32[32,1,128]{2,1,0:T(1,128)}), f32[32,1,128]{2,1,0:T(1,128)S(1)}, u32[]{:S(2)}, u32[]{:S(2)}) %all-to-all-start.6) | async-done | bytes 16416 | tf_op jit(solution)/shard_map/all_to_all | solution.py:15
  203.0 0.5 reduce_sum.83
  203.5 0.0 collective-permute-done.2
  203.5 0.0 copy-done.1
  203.5 1.3 broadcast_select_fusion.1
  204.8 0.0 copy-done.4
  204.8 0.2 pad_maximum_fusion
  205.0 0.2 copy.39
  205.2 1.6 copy.45
  (3 shorter events, 0.1 us)
Async XLA Ops:
  0.6 29.7 %copy-start = (bf16[384,2048]{1,0:T(8,128)(2,1)S(1)}, bf16[384,2048]{1,0:T(8,128)(2,1)}, u32[]{:S(2)}) copy-start(bf16[384,2048]{1,0:T(8,128)(2,1)} %param.7) | copy-start | bytes 4718596
  1.7 8.7 %copy-start.7 = (bf16[128,256]{1,0:T(8,128)(2,1)S(1)}, bf16[128,256]{1,0:T(8,128)(2,1)}, u32[]{:S(2)}) copy-start(bf16[128,256]{1,0:T(8,128)(2,1)} %param.8) | copy-start | bytes 196612
  2.8 22.0 %all-to-all-start = ((bf16[16,128,256]{2,1,0:T(8,128)(2,1)}), bf16[16,128,256]{2,1,0:T(8,128)(2,1)S(1)}, u32[]{:S(2)}, u32[]{:S(2)}) async-start(bf16[16,128,256]{2,1,0:T(8,128)(2,1)} %broadcast_in_dim.8), calls=%async_computation | async-start | bytes 2097152 | tf_op jit(solution)/shard_map/all_to_all | solution.py:15
  10.4 19.9 %copy-start.5 = (bf16[384,256]{1,0:T(8,128)(2,1)S(1)}, bf16[384,256]{1,0:T(8,128)(2,1)}, u32[]{:S(2)}) copy-start(bf16[384,256]{1,0:T(8,128)(2,1)} %param.6) | copy-start | bytes 589828
  10.4 12.5 %collective-permute-start = (bf16[128,256]{1,0:T(8,128)(2,1)S(1)}, bf16[128,256]{1,0:T(8,128)(2,1)S(1)}, u32[]{:S(2)}, u32[]{:S(2)}) collective-permute-start(bf16[128,256]{1,0:T(8,128)(2,1)S(1)} %copy-done.7), channel_id=1, source_target_pairs={{0,0},{1,32},{32,33},{33,1},{2,2},{3,34},{34,35},{35,3},{4,4},{5,3... | collective-permute-start | bytes 196616 | tf_op jit(solution)/shard_map/ppermute | solution.py:42
  24.8 1.3 copy-start.2
  26.1 16.4 %all-to-all-start.1 = ((bf16[16,128,256]{2,1,0:T(8,128)(2,1)}), bf16[16,128,256]{2,1,0:T(8,128)(2,1)S(1)}, u32[]{:S(2)}, u32[]{:S(2)}) async-start(bf16[16,128,256]{2,1,0:T(8,128)(2,1)} %broadcast_in_dim.9), calls=%async_computation.1 | async-start | bytes 2097152 | tf_op jit(solution)/shard_map/all_to_all | solution.py:15
  32.1 10.9 %copy-start.3 = (bf16[384,256]{1,0:T(8,128)(2,1)}, bf16[384,256]{1,0:T(8,128)(2,1)S(1)}, u32[]{:S(2)}) copy-start(bf16[384,256]{1,0:T(8,128)(2,1)S(1)} %fusion.2) | copy-start | bytes 589828
  32.1 10.5 %collective-permute-start.1 = (bf16[384,256]{1,0:T(8,128)(2,1)S(1)}, bf16[384,256]{1,0:T(8,128)(2,1)S(1)}, u32[]{:S(2)}, u32[]{:S(2)}) collective-permute-start(bf16[384,256]{1,0:T(8,128)(2,1)S(1)} %fusion.2), channel_id=1, source_target_pairs={{0,1},{1,0},{2,3},{3,2},{4,5},{5,4},{6,7},{7,6},{8,9},{9,8},{10,11... | collective-permute-start | bytes 589832 | tf_op jit(solution)/shard_map/ppermute | solution.py:25
  43.0 10.4 %copy-start.6 = (bf16[384,256]{1,0:T(8,128)(2,1)S(1)}, bf16[384,256]{1,0:T(8,128)(2,1)}, u32[]{:S(2)}) copy-start(bf16[384,256]{1,0:T(8,128)(2,1)} %param.6) | copy-start | bytes 589828
  44.3 27.7 %all-to-all-start.2 = ((bf16[4,96,1024]{2,1,0:T(8,128)(2,1)}), bf16[4,96,1024]{2,1,0:T(8,128)(2,1)S(1)}, u32[]{:S(2)}, u32[]{:S(2)}) async-start(bf16[4,96,1024]{2,1,0:T(8,128)(2,1)} %bitcast.4), calls=%async_computation.2 | async-start | bytes 1572864 | tf_op jit(solution)/shard_map/all_to_all | solution.py:21
  72.1 22.2 %all-to-all-start.5 = ((bf16[16,128,256]{1,2,0:T(8,128)(2,1)}), bf16[16,128,256]{1,2,0:T(8,128)(2,1)S(1)}, u32[]{:S(2)}, u32[]{:S(2)}) async-start(bf16[16,128,256]{1,2,0:T(8,128)(2,1)} %bitcast.34), calls=%async_computation.5 | async-start | bytes 2097152 | tf_op jit(solution)/shard_map/all_to_all | solution.py:21
  94.3 25.1 %all-to-all-start.3 = ((bf16[4,24,1024]{2,1,0:T(8,128)(2,1)}), bf16[4,24,1024]{2,1,0:T(8,128)(2,1)S(1)}, u32[]{:S(2)}, u32[]{:S(2)}) async-start(bf16[4,24,1024]{2,1,0:T(8,128)(2,1)} %bitcast.40), calls=%async_computation.3 | async-start | bytes 393216 | tf_op jit(solution)/shard_map/all_to_all | solution.py:21
  119.4 47.0 %all-to-all-start.4 = ((bf16[16,128,256]{1,2,0:T(8,128)(2,1)}), bf16[16,128,256]{1,2,0:T(8,128)(2,1)}, u32[]{:S(2)}, u32[]{:S(2)}) async-start(bf16[16,128,256]{1,2,0:T(8,128)(2,1)} %bitcast.33), calls=%async_computation.4 | async-start | bytes 2097152 | tf_op jit(solution)/shard_map/all_to_all | solution.py:21
  158.0 45.5 %copy-start.1 = (bf16[384,1024]{0,1:T(8,128)(2,1)S(1)}, bf16[384,1024]{0,1:T(8,128)(2,1)}, u32[]{:S(2)}) copy-start(bf16[384,1024]{0,1:T(8,128)(2,1)} %copy.37) | copy-start | bytes 2359300
  158.0 45.5 %collective-permute-start.2 = (bf16[384,1024]{0,1:T(8,128)(2,1)}, bf16[384,1024]{0,1:T(8,128)(2,1)}, u32[]{:S(2)}, u32[]{:S(2)}) collective-permute-start(bf16[384,1024]{0,1:T(8,128)(2,1)} %copy.37), channel_id=1, source_target_pairs={{0,1},{1,0},{2,3},{3,2},{4,5},{5,4},{6,7},{7,6},{8,9},{9,8},{10,11... | collective-permute-start | bytes 2359304 | tf_op jit(solution)/shard_map/ppermute | solution.py:25
  166.3 38.5 %copy-start.4 = (f32[128,256]{0,1:T(8,128)}, f32[128,256]{0,1:T(8,128)S(1)}, u32[]{:S(2)}) copy-start(f32[128,256]{0,1:T(8,128)S(1)} %convert_reduce_fusion) | copy-start | bytes 393220
  167.0 15.4 %all-to-all-start.7 = ((f32[16,1,256]{2,1,0:T(1,128)}), f32[16,1,256]{2,1,0:T(1,128)S(1)}, u32[]{:S(2)}, u32[]{:S(2)}) async-start(f32[16,1,256]{2,1,0:T(1,128)} %broadcast_in_dim.11), calls=%async_computation.7 | async-start | bytes 32768 | tf_op jit(solution)/shard_map/all_to_all | solution.py:15
  183.0 20.0 %all-to-all-start.6 = ((f32[32,1,128]{2,1,0:T(1,128)}), f32[32,1,128]{2,1,0:T(1,128)S(1)}, u32[]{:S(2)}, u32[]{:S(2)}) async-start(f32[32,1,128]{2,1,0:T(1,128)} %broadcast_in_dim.10), calls=%async_computation.6 | async-start | bytes 32768 | tf_op jit(solution)/shard_map/all_to_all | solution.py:15

commit v2 on v1

v2 whole, which is shorter than its diff:
```python
import jax
import jax.numpy as jnp
from jax import lax
from jax.sharding import Mesh
from jax.sharding import PartitionSpec as P


FS = ("y", "x")
TP = ("zh", "zl", "core")
BF = jnp.bfloat16
F32 = jnp.float32


def exchange(array, axes):
    return lax.all_to_all(array, axes, 0, 0, tiled=True)


def from_everyone(array, axes):
    count = lax.axis_size(axes)
    return exchange(jnp.broadcast_to(array[None], (count, *array.shape)), axes)


def other_core(array):
    return lax.ppermute(array, "core", [(0, 1), (1, 0)])


def dot(left, right, over):
    return lax.dot_general(
        left, right, ((over[:1], over[1:]), ((), ())), preferred_element_type=F32
    )


def local(inputs, pre_act, cotangent, up_weight, down_weight):
    tokens, width = inputs.shape
    hidden = pre_act.shape[1]
    many = lax.axis_size(FS)
    part = width // many
    core = lax.axis_index("core")
    active = jnp.maximum(pre_act.astype(F32), 0.0)
    squared = (active * active).astype(BF)

    mine = jnp.concatenate([down_weight.T, up_weight], axis=0)
    weights = from_everyone(mine, FS)
    down_columns = weights[:, :part].reshape(width, hidden)
    halves = weights[:, part:].reshape(2, width // 2, hidden)
    own_rows = lax.dynamic_index_in_dim(halves, core, 0, False)
    their_rows = other_core(lax.dynamic_index_in_dim(halves, 1 - core, 0, False))
    sq_grad = dot(cotangent, down_columns, (1, 0))
    pre_grad = (2.0 * active * sq_grad).astype(BF)
    theirs = other_core(pre_grad)
    half = (dot(pre_grad, own_rows, (1, 1)) + dot(theirs, their_rows, (1, 1))).astype(BF)

    near = lax.axis_size("zl")
    pieces = exchange(half.reshape(near, tokens // near, width // 2), "zl")
    quarter = jnp.sum(pieces.astype(F32), axis=0).astype(BF)

    down_part = dot(squared, cotangent, (0, 0)).astype(BF)
    up_part = dot(pre_grad, inputs, (0, 0)).astype(BF)
    parts = jnp.concatenate([down_part, up_part], axis=0)
    parts = jnp.moveaxis(parts.reshape(2 * hidden, many, part), 1, 0)
    parts, quarter = lax.optimization_barrier((parts, quarter))
    grads = exchange(parts, FS)
    grads = jnp.sum(grads.astype(F32), axis=0)
    down_grad, up_grad = grads[:hidden], grads[hidden:]

    groups = lax.all_gather(quarter, "zh", axis=0, tiled=False)
    quarter = jnp.sum(groups.astype(F32), axis=0).astype(BF)
    up_squares = jnp.sum(up_grad * up_grad, axis=0)
    up_squares, quarter = lax.optimization_barrier((up_squares, quarter))
    up_norms = from_everyone(up_squares, TP)
    up_norms = jnp.sum(up_norms, axis=0)
    half = lax.all_gather(quarter, "zl", axis=0, tiled=True)

    down_squares = jnp.sum(down_grad * down_grad, axis=1)
    down_squares, half = lax.optimization_barrier((down_squares, half))
    down_norms = from_everyone(down_squares, FS)
    down_norms = jnp.sum(down_norms, axis=0)
    both = other_core(half)
    input_grad = jnp.concatenate(
        [jnp.where(core == 0, half, both), jnp.where(core == 0, both, half)], axis=1
    )
    return input_grad, up_grad.T, down_grad, up_norms, down_norms


def solution(mesh):
    split = Mesh(mesh.devices.reshape(4, 4, 4, 4, 2), (*FS, *TP))
    return jax.shard_map(
        local,
        mesh=split,
        in_specs=(P(FS, None), P(FS, TP), P(FS, None), P(FS, TP), P(TP, FS)),
        out_specs=(P(FS, None), P(FS, TP), P(TP, FS), P(FS), P(TP)),
        check_vma=False,
    )
```

time: 208 us -> 182 us (0.88)
  starting transfers between devices: 84 us -> 43.6 us
  blocking collectives: 31.4 us -> 66.8 us
  waiting for transfers between devices: 67.9 us -> 51.9 us
  local copies, waits for them, and re-layouts: 11 us -> 6.63 us
  other arithmetic: 5.13 us -> 8.03 us
  matrix products: 6.48 us -> 3.92 us
    all_to_all x4 -> x0, starting transfers between devices: 28.9 us -> none  [from_everyone(): lax.all_to_all(jnp.broadcast_to(array[None], (count, *array.shape)), axes...]
    all_gather x2, blocking collectives: 31.4 us -> 54.6 us  [the longest x1 38.7 us: local(): groups = lax.all_gather(quarter, 'zh', axis=0, tiled=False)]
    all_to_all x4 -> x0, waiting for transfers between devices: 21.7 us -> none  [from_everyone(): lax.all_to_all(jnp.broadcast_to(array[None], (count, *array.shape)), axes...]
    all_to_all x0 -> x1, blocking collectives: none -> 12.3 us  [exchange(): return lax.all_to_all(array, axes, 0, 0, tiled=True)]
    all_to_all x4, waiting for transfers between devices: 40.2 us -> 50.9 us  [exchange(): return lax.all_to_all(array, axes, 0, 0, tiled=True)]
    all_to_all x4, starting transfers between devices: 34.5 us -> 27.9 us  [exchange(): return lax.all_to_all(array, axes, 0, 0, tiled=True)]
    ppermute x1 -> x0, starting transfers between devices: 6.37 us -> none  [local(): lax.ppermute(up_weight, ('xl', 'core'), [(0, 0), (1, 2), (2, 3), (3, 1)])]
    ppermute x1 -> x0, waiting for transfers between devices: 6.08 us -> none  [local(): lax.ppermute(up_weight, ('xl', 'core'), [(0, 0), (1, 2), (2, 3), (3, 1)])]
  transfers between devices with their start and end apart: 11 -> 7, of which waited for: 8 -> 4; matrix products, arithmetic and copies ran while one was open for 7% -> 4% of each run, Pallas kernels for 0% -> 0%
where the time goes in v2:
time: 182 us
  blocking collectives  66.8 us (37%)
  waiting for transfers between devices  51.9 us (29%)
  starting transfers between devices  43.6 us (24%)
  other arithmetic  8.03 us (4%)
  local copies, waits for them, and re-layouts  6.63 us (4%)
  matrix products  3.92 us (2%)
    all_to_all x4, waiting for transfers between devices, exchange(): return lax.all_to_all(array, axes, 0, 0, tiled=True)  50.9 us
    all_gather x1, blocking collectives, local(): groups = lax.all_gather(quarter, 'zh', axis=0, tiled=False)  38.7 us
    all_to_all x4, starting transfers between devices, exchange(): return lax.all_to_all(array, axes, 0, 0, tiled=True)  27.9 us
    all_gather x1, blocking collectives, local(): half = lax.all_gather(quarter, 'zl', axis=0, tiled=True)  15.9 us
    ppermute x3, starting transfers between devices, other_core(): return lax.ppermute(array, 'core', [(0, 1), (1, 0)])  15.7 us
    all_to_all x1, blocking collectives, exchange(): return lax.all_to_all(array, axes, 0, 0, tiled=True)  12.3 us
    dot_general x5, matrix products, dot(): lax.dot_general(left, right, ((over[:1], over[1:]), ((), ())), preferred_...  3.92 us
  transfers between devices with their start and end apart: 7, of which 4 were waited for; matrix products, arithmetic and copies ran while one was open for 4% of the time, Pallas kernels for 0%

profile of v2, /device:TPU:1, one launch (start us, length us, event | category | flops | bytes accessed | tf_op | source)
XLA Modules:
  0.0 181.8 jit_solution(13428883112434322644)
XLA Ops:
  0.6 0.0 copy-start
  0.6 1.1 copy.25
  1.7 0.9 pad_maximum_fusion.1
  2.6 0.1 copy.26
  2.7 1.5 broadcast_in_dim.6
  4.2 0.0 copy-start.2
  4.2 7.8 %all-to-all-start = ((bf16[16,256,256]{2,1,0:T(8,128)(2,1)}), bf16[16,256,256]{2,1,0:T(8,128)(2,1)}, u32[]{:S(2)}, u32[]{:S(2)}) async-start(bf16[16,256,256]{2,1,0:T(8,128)(2,1)} %broadcast_in_dim.6), calls=%async_computation | async-start | bytes 4194304 | tf_op jit(solution)/shard_map/all_to_all | solution.py:15
  12.0 0.0 copy-done.2
  12.0 0.2 copy.24
  12.1 24.7 %all-to-all-done = bf16[16,256,256]{2,1,0:T(8,128)(2,1)} async-done(((bf16[16,256,256]{2,1,0:T(8,128)(2,1)}), bf16[16,256,256]{2,1,0:T(8,128)(2,1)}, u32[]{:S(2)}, u32[]{:S(2)}) %all-to-all-start) | async-done | bytes 2097184 | tf_op jit(solution)/shard_map/all_to_all | solution.py:15
  36.8 1.7 fusion.8
  38.5 8.1 %collective-permute-start.1 = (bf16[1024,256]{1,0:T(8,128)(2,1)S(1)}, bf16[1024,256]{1,0:T(8,128)(2,1)S(1)}, u32[]{:S(2)}, u32[]{:S(2)}) collective-permute-start(bf16[1024,256]{1,0:T(8,128)(2,1)S(1)} %dynamic-slice_bitcast_fusion), channel_id=1, source_target_pairs={{0,1},{1,0},{2,3},{3,2},{4,5},{5,4},{6,7},{7,6},{8,9},{9,8},{10,11... | collective-permute-start | bytes 1572872 | tf_op jit(solution)/shard_map/ppermute | solution.py:24
  46.6 0.0 copy-done
  46.6 0.8 fusion.1
  47.4 1.9 %collective-permute-start = (bf16[384,256]{0,1:T(8,128)(2,1)S(1)}, bf16[384,256]{0,1:T(8,128)(2,1)S(1)}, u32[]{:S(2)}, u32[]{:S(2)}) collective-permute-start(bf16[384,256]{0,1:T(8,128)(2,1)S(1)} %fusion.1), channel_id=1, source_target_pairs={{0,1},{1,0},{2,3},{3,2},{4,5},{5,4},{6,7},{7,6},{8,9},{9,8},{10,11... | collective-permute-start | bytes 589832 | tf_op jit(solution)/shard_map/ppermute | solution.py:24
  49.3 0.4 fusion.2
  49.8 1.0 collective-permute-done
  50.7 0.0 collective-permute-done.1
  50.7 1.3 add_convert_fusion
  52.0 7.4 %all-to-all-start.1 = ((bf16[4,96,1024]{2,1,0:T(8,128)(2,1)}), bf16[4,96,1024]{2,1,0:T(8,128)(2,1)S(1)}, u32[]{:S(2)}, u32[]{:S(2)}) async-start(bf16[4,96,1024]{2,1,0:T(8,128)(2,1)} %bitcast.7), calls=%async_computation.1 | async-start | bytes 1572864 | tf_op jit(solution)/shard_map/all_to_all | solution.py:15
  59.4 0.0 copy-start.1
  59.4 0.7 convolution_convert_fusion.1
  60.2 0.7 copy-done.1
  60.9 0.7 convolution_convert_fusion
  61.6 1.8 %bitcast_bitcast_fusion = bf16[16,512,128]{2,1,0:T(8,128)(2,1)} fusion(bf16[256,2048]{1,0:T(8,128)(2,1)S(1)} %convolution_convert_fusion, bf16[256,2048]{1,0:T(8,128)(2,1)S(1)} %convolution_convert_fusion.1), kind=kLoop, calls=%fused_computation.3 | loop fusion | flops 4194304 | bytes 4194304 | tf_op jit(solution)/shard_map/transpose | solution.py:60
  63.4 15.8 %all-to-all-done.1 = bf16[4,96,1024]{2,1,0:T(8,128)(2,1)S(1)} async-done(((bf16[4,96,1024]{2,1,0:T(8,128)(2,1)}), bf16[4,96,1024]{2,1,0:T(8,128)(2,1)S(1)}, u32[]{:S(2)}, u32[]{:S(2)}) %all-to-all-start.1) | async-done | bytes 786464 | tf_op jit(solution)/shard_map/all_to_all | solution.py:15
  79.2 0.1 reduce_sum.69
  79.4 4.4 %all-to-all-start.2 = ((bf16[16,512,128]{2,1,0:T(8,128)(2,1)}), bf16[16,512,128]{2,1,0:T(8,128)(2,1)}, u32[]{:S(2)}, u32[]{:S(2)}) async-start(bf16[16,512,128]{2,1,0:T(8,128)(2,1)} %bitcast_bitcast_fusion), calls=%async_computation.2 | async-start | bytes 4194304 | tf_op jit(solution)/shard_map/all_to_all | solution.py:15
  83.8 38.7 %all-gather = bf16[384,1024]{1,0:T(8,128)(2,1)S(1)} all-gather(bf16[96,1024]{1,0:T(8,128)(2,1)S(1)} %reduce_sum.69), channel_id=2, replica_groups=mesh['y'=4,'x'=4,'zh'=4,'zl'=4,'core'=2] {'zh'}, dimensions={0}, use_global_device_ids=true | all-gather | bytes 983040 | tf_op jit(solution)/shard_map/all_gather | solution.py:66
  122.5 0.1 reduce_sum.73
  122.6 0.0 all-to-all-done.2
  122.6 1.9 %convert_reduce_fusion = f32[512,128]{1,0:T(8,128)S(1)} fusion(bf16[16,512,128]{2,1,0:T(8,128)(2,1)} %all-to-all-done.2), kind=kLoop, calls=%fused_computation | loop fusion | flops 2031616 | bytes 2359296 | tf_op jit(solution)/shard_map/reduce_sum | solution.py:63
  124.6 0.7 slice_bitcast_fusion
  125.2 15.9 %all_gather.11 = bf16[384,1024]{1,0:T(8,128)(2,1)S(1)} all-gather(bf16[96,1024]{1,0:T(8,128)(2,1)S(1)} %reduce_sum.73), channel_id=1, replica_groups=mesh['y'=4,'x'=4,'zh'=4,'zl'=4,'core'=2] {'zl'}, dimensions={0}, use_global_device_ids=true | all-gather | bytes 983040 | tf_op jit(solution)/shard_map/all_gather | solution.py:72
  141.1 5.7 %collective-permute-start.2 = (bf16[384,1024]{1,0:T(8,128)(2,1)S(1)}, bf16[384,1024]{1,0:T(8,128)(2,1)S(1)}, u32[]{:S(2)}, u32[]{:S(2)}) collective-permute-start(bf16[384,1024]{1,0:T(8,128)(2,1)S(1)} %all_gather.11), channel_id=1, source_target_pairs={{0,1},{1,0},{2,3},{3,2},{4,5},{5,4},{6,7},{7,6},{8,9},{9,8},{10,11... | collective-permute-start | bytes 2359304 | tf_op jit(solution)/shard_map/ppermute | solution.py:24
  146.9 12.3 %all_to_all.27 = f32[16,1,256]{2,1,0:T(1,128)S(1)} all-to-all(f32[16,1,256]{2,1,0:T(1,128)S(1)} %broadcast_in_dim.8), channel_id=1, replica_groups=mesh['y'=4,'x'=4,'zh'=4,'zl'=4,'core'=2] {'y','x'}, dimensions={0} | all-to-all | bytes 32768 | tf_op jit(solution)/shard_map/all_to_all | solution.py:15
  159.2 0.6 broadcast_in_dim.7
  159.8 8.3 %all-to-all-start.3 = ((f32[32,1,128]{2,1,0:T(1,128)}), f32[32,1,128]{2,1,0:T(1,128)S(1)}, u32[]{:S(2)}, u32[]{:S(2)}) async-start(f32[32,1,128]{2,1,0:T(1,128)} %broadcast_in_dim.7), calls=%async_computation.3 | async-start | bytes 32768 | tf_op jit(solution)/shard_map/all_to_all | solution.py:15
  168.1 0.8 copy.30
  168.9 0.6 reduce_sum.75
  169.5 10.4 %all-to-all-done.3 = f32[32,1,128]{2,1,0:T(1,128)S(1)} async-done(((f32[32,1,128]{2,1,0:T(1,128)}), f32[32,1,128]{2,1,0:T(1,128)S(1)}, u32[]{:S(2)}, u32[]{:S(2)}) %all-to-all-start.3) | async-done | bytes 16416 | tf_op jit(solution)/shard_map/all_to_all | solution.py:15
  179.9 0.5 reduce_sum.74
  180.4 0.0 collective-permute-done.2
  180.4 0.1 broadcast_select_fusion.1
  180.5 1.2 pad_maximum_fusion
  (2 shorter events, 0.1 us)
Async XLA Ops:
  0.6 46.0 %copy-start = (bf16[384,2048]{1,0:T(8,128)(2,1)S(1)}, bf16[384,2048]{1,0:T(8,128)(2,1)}, u32[]{:S(2)}) copy-start(bf16[384,2048]{1,0:T(8,128)(2,1)} %param.7) | copy-start | bytes 4718596
  4.2 7.8 %copy-start.2 = (bf16[384,256]{1,0:T(8,128)(2,1)S(1)}, bf16[384,256]{1,0:T(8,128)(2,1)}, u32[]{:S(2)}) copy-start(bf16[384,256]{1,0:T(8,128)(2,1)} %param.6) | copy-start | bytes 589828
  4.2 32.6 %all-to-all-start = ((bf16[16,256,256]{2,1,0:T(8,128)(2,1)}), bf16[16,256,256]{2,1,0:T(8,128)(2,1)}, u32[]{:S(2)}, u32[]{:S(2)}) async-start(bf16[16,256,256]{2,1,0:T(8,128)(2,1)} %broadcast_in_dim.6), calls=%async_computation | async-start | bytes 4194304 | tf_op jit(solution)/shard_map/all_to_all | solution.py:15
  38.5 12.2 %collective-permute-start.1 = (bf16[1024,256]{1,0:T(8,128)(2,1)S(1)}, bf16[1024,256]{1,0:T(8,128)(2,1)S(1)}, u32[]{:S(2)}, u32[]{:S(2)}) collective-permute-start(bf16[1024,256]{1,0:T(8,128)(2,1)S(1)} %dynamic-slice_bitcast_fusion), channel_id=1, source_target_pairs={{0,1},{1,0},{2,3},{3,2},{4,5},{5,4},{6,7},{7,6},{8,9},{9,8},{10,11... | collective-permute-start | bytes 1572872 | tf_op jit(solution)/shard_map/ppermute | solution.py:24
  47.4 3.3 %collective-permute-start = (bf16[384,256]{0,1:T(8,128)(2,1)S(1)}, bf16[384,256]{0,1:T(8,128)(2,1)S(1)}, u32[]{:S(2)}, u32[]{:S(2)}) collective-permute-start(bf16[384,256]{0,1:T(8,128)(2,1)S(1)} %fusion.1), channel_id=1, source_target_pairs={{0,1},{1,0},{2,3},{3,2},{4,5},{5,4},{6,7},{7,6},{8,9},{9,8},{10,11... | collective-permute-start | bytes 589832 | tf_op jit(solution)/shard_map/ppermute | solution.py:24
  52.0 27.2 %all-to-all-start.1 = ((bf16[4,96,1024]{2,1,0:T(8,128)(2,1)}), bf16[4,96,1024]{2,1,0:T(8,128)(2,1)S(1)}, u32[]{:S(2)}, u32[]{:S(2)}) async-start(bf16[4,96,1024]{2,1,0:T(8,128)(2,1)} %bitcast.7), calls=%async_computation.1 | async-start | bytes 1572864 | tf_op jit(solution)/shard_map/all_to_all | solution.py:15
  59.4 1.4 copy-start.1
  79.4 43.3 %all-to-all-start.2 = ((bf16[16,512,128]{2,1,0:T(8,128)(2,1)}), bf16[16,512,128]{2,1,0:T(8,128)(2,1)}, u32[]{:S(2)}, u32[]{:S(2)}) async-start(bf16[16,512,128]{2,1,0:T(8,128)(2,1)} %bitcast_bitcast_fusion), calls=%async_computation.2 | async-start | bytes 4194304 | tf_op jit(solution)/shard_map/all_to_all | solution.py:15
  141.1 39.3 %collective-permute-start.2 = (bf16[384,1024]{1,0:T(8,128)(2,1)S(1)}, bf16[384,1024]{1,0:T(8,128)(2,1)S(1)}, u32[]{:S(2)}, u32[]{:S(2)}) collective-permute-start(bf16[384,1024]{1,0:T(8,128)(2,1)S(1)} %all_gather.11), channel_id=1, source_target_pairs={{0,1},{1,0},{2,3},{3,2},{4,5},{5,4},{6,7},{7,6},{8,9},{9,8},{10,11... | collective-permute-start | bytes 2359304 | tf_op jit(solution)/shard_map/ppermute | solution.py:24
  159.8 20.1 %all-to-all-start.3 = ((f32[32,1,128]{2,1,0:T(1,128)}), f32[32,1,128]{2,1,0:T(1,128)S(1)}, u32[]{:S(2)}, u32[]{:S(2)}) async-start(f32[32,1,128]{2,1,0:T(1,128)} %broadcast_in_dim.7), calls=%async_computation.3 | async-start | bytes 32768 | tf_op jit(solution)/shard_map/all_to_all | solution.py:15

commit v3 on v2

v3 whole, which is shorter than its diff:
```python
import jax
import jax.numpy as jnp
from jax import lax
from jax.sharding import Mesh
from jax.sharding import PartitionSpec as P


FS = ("yh", "yl", "x")
TP = ("zh", "zl", "core")
BF = jnp.bfloat16
F32 = jnp.float32


def exchange(array, axes):
    return lax.all_to_all(array, axes, 0, 0, tiled=True)


def from_everyone(array, axes):
    count = lax.axis_size(axes)
    return exchange(jnp.broadcast_to(array[None], (count, *array.shape)), axes)


def other_core(array):
    return lax.ppermute(array, "core", [(0, 1), (1, 0)])


def dot(left, right, over):
    return lax.dot_general(
        left, right, ((over[:1], over[1:]), ((), ())), preferred_element_type=F32
    )


def sum_near(half, axis):
    count = lax.axis_size(axis)
    here = lax.axis_index(axis)
    pieces = half.reshape(count, half.shape[0] // count, half.shape[1])
    total = lax.dynamic_index_in_dim(pieces, here, 0, False).astype(F32)
    for step in (1, 3, 2):
        there = lax.rem(here + step, count)
        piece = lax.dynamic_index_in_dim(pieces, there, 0, False)
        ring = [(i, (i + step) % count) for i in range(count)]
        total += lax.ppermute(piece, axis, ring).astype(F32)
    return total.astype(BF)


def local(inputs, pre_act, cotangent, up_weight, down_weight):
    tokens, width = inputs.shape
    hidden = pre_act.shape[1]
    many = lax.axis_size(FS)
    core = lax.axis_index("core")
    active = jnp.maximum(pre_act.astype(F32), 0.0)
    squared = (active * active).astype(BF)

    down_columns = from_everyone(down_weight.T, FS).reshape(width, hidden)
    rows = lax.ppermute(up_weight, ("yh", "core"), [(0, 0), (1, 2), (2, 3), (3, 1)])
    up_rows = from_everyone(rows, FS).reshape(2, width // 2, hidden)

    sq_grad = dot(cotangent, down_columns, (1, 0))
    pre_grad = (2.0 * active * sq_grad).astype(BF)
    theirs = other_core(pre_grad)
    half = (dot(pre_grad, up_rows[0], (1, 1)) + dot(theirs, up_rows[1], (1, 1))).astype(BF)

    down_part = dot(squared, cotangent, (0, 0)).astype(BF)
    up_part = dot(pre_grad, inputs, (0, 0)).astype(BF)
    parts = jnp.concatenate([down_part, up_part], axis=0)
    parts = jnp.moveaxis(parts.reshape(2 * hidden, many, width // many), 1, 0)
    grads = exchange(parts, FS)
    grads = jnp.sum(grads.astype(F32), axis=0)
    down_grad, up_grad = grads[:hidden], grads[hidden:]

    half = sum_near(half, "zl")
    pieces = exchange(half.reshape(4, tokens // 16, width // 2), "zh")
    half = jnp.sum(pieces.astype(F32), axis=0).astype(BF)

    up_norms = from_everyone(jnp.sum(up_grad * up_grad, axis=0), TP)
    half = lax.all_gather(half, "zh", axis=0, tiled=True)
    down_norms = from_everyone(jnp.sum(down_grad * down_grad, axis=1), FS)
    half = lax.all_gather(half, "zl", axis=0, tiled=True)
    both = other_core(half)
    input_grad = jnp.concatenate(
        [jnp.where(core == 0, half, both), jnp.where(core == 0, both, half)], axis=1
    )
    up_norms, down_norms = jnp.sum(up_norms, axis=0), jnp.sum(down_norms, axis=0)
    return input_grad, up_grad.T, down_grad, up_norms, down_norms


def solution(mesh):
    split = Mesh(mesh.devices.reshape(2, 2, 4, 4, 4, 2), (*FS, *TP))
    return jax.shard_map(
        local,
        mesh=split,
        in_specs=(P(FS, None), P(FS, TP), P(FS, None), P(FS, TP), P(TP, FS)),
        out_specs=(P(FS, None), P(FS, TP), P(TP, FS), P(FS), P(TP)),
        check_vma=False,
    )
```

time: 182 us -> 185 us (1.016)
  starting transfers between devices: 43.6 us -> 82.4 us
  blocking collectives: 66.8 us -> 35.6 us
  waiting for transfers between devices: 51.9 us -> 42.6 us
  other arithmetic: 8.03 us -> 11.9 us
    all_to_all x4 -> x6, waiting for transfers between devices: 50.9 us -> 29.6 us  [exchange(): return lax.all_to_all(array, axes, 0, 0, tiled=True)]
    ppermute x0 -> x4, starting transfers between devices: none -> 21.1 us  [the longest x3 13.1 us: sum_near(): total += lax.ppermute(piece, axis, ring).astype(F32)]
    all_to_all x4 -> x6, starting transfers between devices: 27.9 us -> 47.4 us  [exchange(): return lax.all_to_all(array, axes, 0, 0, tiled=True)]
    all_gather x2, blocking collectives: 54.6 us -> 35.6 us  [the longest x1 19.7 us: local(): half = lax.all_gather(half, 'zl', axis=0, tiled=True)]
    ppermute x0 -> x4, waiting for transfers between devices: none -> 13 us  [the longest x3 8.31 us: sum_near(): total += lax.ppermute(piece, axis, ring).astype(F32)]
    all_to_all x1 -> x0, blocking collectives: 12.3 us -> none  [exchange(): return lax.all_to_all(array, axes, 0, 0, tiled=True)]
    select_n x1, other arithmetic: 0.11 us -> 2.13 us  [local(): jnp.where(core == 0, half, both)]
    ppermute x3 -> x2, starting transfers between devices: 15.7 us -> 14 us  [other_core(): return lax.ppermute(array, 'core', [(0, 1), (1, 0)])]
  transfers between devices with their start and end apart: 7 -> 12, of which waited for: 4 -> 7; matrix products, arithmetic and copies ran while one was open for 4% -> 8% of each run, Pallas kernels for 0% -> 0%
where the time goes in v3:
time: 185 us; the launch traced here: 184 us
  starting transfers between devices  82.4 us (45%)
  waiting for transfers between devices  42.6 us (23%)
  blocking collectives  35.6 us (19%)
  other arithmetic  11.9 us (6%)
  local copies, waits for them, and re-layouts  5.58 us (3%)
  matrix products  4.98 us (3%)
    all_to_all x6, starting transfers between devices, exchange(): return lax.all_to_all(array, axes, 0, 0, tiled=True)  47.4 us
    all_to_all x6, waiting for transfers between devices, exchange(): return lax.all_to_all(array, axes, 0, 0, tiled=True)  29.6 us
    all_gather x1, blocking collectives, local(): half = lax.all_gather(half, 'zl', axis=0, tiled=True)  19.7 us
    all_gather x1, blocking collectives, local(): half = lax.all_gather(half, 'zh', axis=0, tiled=True)  15.9 us
    ppermute x2, starting transfers between devices, other_core(): return lax.ppermute(array, 'core', [(0, 1), (1, 0)])  14 us
    ppermute x3, starting transfers between devices, sum_near(): total += lax.ppermute(piece, axis, ring).astype(F32)  13.1 us
    ppermute x3, waiting for transfers between devices, sum_near(): total += lax.ppermute(piece, axis, ring).astype(F32)  8.31 us
    ppermute x1, starting transfers between devices, local(): lax.ppermute(up_weight, ('yh', 'core'), [(0, 0), (1, 2), (2, 3), (3, 1)])  7.92 us
  transfers between devices with their start and end apart: 12, of which 7 were waited for; matrix products, arithmetic and copies ran while one was open for 8% of the time, Pallas kernels for 0%

profile of v3, /device:TPU:1, one launch (start us, length us, event | category | flops | bytes accessed | tf_op | source)
XLA Modules:
  0.0 184.0 jit_solution(7870780589260334892)
XLA Ops:
  0.6 0.0 copy-start
  0.6 1.1 copy.18
  1.7 0.0 copy-start.4
  1.7 1.1 broadcast_in_dim.8
  2.8 7.6 %all-to-all-start = ((bf16[16,128,256]{2,1,0:T(8,128)(2,1)}), bf16[16,128,256]{2,1,0:T(8,128)(2,1)S(1)}, u32[]{:S(2)}, u32[]{:S(2)}) async-start(bf16[16,128,256]{2,1,0:T(8,128)(2,1)} %broadcast_in_dim.8), calls=%async_computation | async-start | bytes 2097152 | tf_op jit(solution)/shard_map/all_to_all | solution.py:15
  10.4 0.0 copy-done.4
  10.4 0.0 copy-start.3
  10.4 7.9 %collective-permute-start = (bf16[128,256]{1,0:T(8,128)(2,1)S(1)}, bf16[128,256]{1,0:T(8,128)(2,1)S(1)}, u32[]{:S(2)}, u32[]{:S(2)}) collective-permute-start(bf16[128,256]{1,0:T(8,128)(2,1)S(1)} %copy-done.4), channel_id=1, source_target_pairs={{0,0},{1,256},{256,257},{257,1},{2,2},{3,258},{258,259},{259,3},{4... | collective-permute-start | bytes 196616 | tf_op jit(solution)/shard_map/ppermute | solution.py:55
  18.3 4.6 %collective-permute-done = bf16[128,256]{1,0:T(8,128)(2,1)S(1)} collective-permute-done((bf16[128,256]{1,0:T(8,128)(2,1)S(1)}, bf16[128,256]{1,0:T(8,128)(2,1)S(1)}, u32[]{:S(2)}, u32[]{:S(2)}) %collective-permute-start) | collective-permute-done | bytes 65568 | tf_op jit(solution)/shard_map/ppermute | solution.py:55
  23.0 1.9 %all-to-all-done = bf16[16,128,256]{2,1,0:T(8,128)(2,1)S(1)} async-done(((bf16[16,128,256]{2,1,0:T(8,128)(2,1)}), bf16[16,128,256]{2,1,0:T(8,128)(2,1)S(1)}, u32[]{:S(2)}, u32[]{:S(2)}) %all-to-all-start) | async-done | bytes 1048608 | tf_op jit(solution)/shard_map/all_to_all | solution.py:15
  24.9 0.0 copy-start.2
  24.9 1.1 broadcast_in_dim.9
  26.0 0.2 copy-done.2
  26.2 4.7 %all-to-all-start.1 = ((bf16[16,128,256]{2,1,0:T(8,128)(2,1)}), bf16[16,128,256]{2,1,0:T(8,128)(2,1)S(1)}, u32[]{:S(2)}, u32[]{:S(2)}) async-start(bf16[16,128,256]{2,1,0:T(8,128)(2,1)} %broadcast_in_dim.9), calls=%async_computation.1 | async-start | bytes 2097152 | tf_op jit(solution)/shard_map/all_to_all | solution.py:15
  31.0 0.0 copy-done
  31.0 0.0 copy-done.3
  31.0 1.8 fusion
  32.8 5.2 %collective-permute-start.1 = (bf16[384,256]{1,0:T(8,128)(2,1)S(1)}, bf16[384,256]{1,0:T(8,128)(2,1)S(1)}, u32[]{:S(2)}, u32[]{:S(2)}) collective-permute-start(bf16[384,256]{1,0:T(8,128)(2,1)S(1)} %fusion), channel_id=1, source_target_pairs={{0,1},{1,0},{2,3},{3,2},{4,5},{5,4},{6,7},{7,6},{8,9},{9,8},{10,11... | collective-permute-start | bytes 589832 | tf_op jit(solution)/shard_map/ppermute | solution.py:24
  38.0 7.0 %all-to-all-done.1 = bf16[16,128,256]{2,1,0:T(8,128)(2,1)S(1)} async-done(((bf16[16,128,256]{2,1,0:T(8,128)(2,1)}), bf16[16,128,256]{2,1,0:T(8,128)(2,1)S(1)}, u32[]{:S(2)}, u32[]{:S(2)}) %all-to-all-start.1) | async-done | bytes 1048608 | tf_op jit(solution)/shard_map/all_to_all | solution.py:15
  45.0 0.1 fusion.6
  45.1 0.0 collective-permute-done.1
  45.2 0.4 fusion.7
  45.6 0.4 add_convert_fusion
  46.0 0.1 dynamic-slice_bitcast_fusion.2
  46.0 5.6 %collective-permute-start.2 = (bf16[96,1024]{1,0:T(8,128)(2,1)S(1)}, bf16[96,1024]{1,0:T(8,128)(2,1)S(1)}, u32[]{:S(2)}, u32[]{:S(2)}) collective-permute-start(bf16[96,1024]{1,0:T(8,128)(2,1)S(1)} %get-tuple-element.31), channel_id=1, source_target_pairs={{0,2},{2,4},{4,6},{6,0},{1,3},{3,5},{5,7},{7,1},{8,10},{10,12},{12... | collective-permute-start | bytes 589832 | tf_op jit(solution)/shard_map/ppermute | solution.py:42
  51.6 4.9 %collective-permute-start.4 = (bf16[96,1024]{1,0:T(8,128)(2,1)S(1)}, bf16[96,1024]{1,0:T(8,128)(2,1)S(1)}, u32[]{:S(2)}, u32[]{:S(2)}) collective-permute-start(bf16[96,1024]{1,0:T(8,128)(2,1)S(1)} %get-tuple-element.32), channel_id=1, source_target_pairs={{0,4},{2,6},{4,0},{6,2},{1,5},{3,7},{5,1},{7,3},{8,12},{10,14},{12... | collective-permute-start | bytes 589832 | tf_op jit(solution)/shard_map/ppermute | solution.py:42
  56.5 2.6 %collective-permute-start.3 = (bf16[96,1024]{1,0:T(8,128)(2,1)S(1)}, bf16[96,1024]{1,0:T(8,128)(2,1)}, u32[]{:S(2)}, u32[]{:S(2)}) collective-permute-start(bf16[96,1024]{1,0:T(8,128)(2,1)S(1)} %get-tuple-element.33), channel_id=1, source_target_pairs={{0,6},{2,0},{4,2},{6,4},{1,7},{3,1},{5,3},{7,5},{8,14},{10,8},{12,... | collective-permute-start | bytes 589832 | tf_op jit(solution)/shard_map/ppermute | solution.py:42
  59.2 0.0 collective-permute-done.2
  59.2 8.3 %collective-permute-done.4 = bf16[96,1024]{1,0:T(8,128)(2,1)S(1)} collective-permute-done((bf16[96,1024]{1,0:T(8,128)(2,1)S(1)}, bf16[96,1024]{1,0:T(8,128)(2,1)S(1)}, u32[]{:S(2)}, u32[]{:S(2)}) %collective-permute-start.4) | collective-permute-done | bytes 196640 | tf_op jit(solution)/shard_map/ppermute | solution.py:42
  67.5 0.0 collective-permute-done.3
  67.5 1.7 fusion.3
  69.2 0.0 copy-start.1
  69.2 15.7 %all-to-all-start.2 = ((bf16[4,24,1024]{2,1,0:T(8,128)(2,1)}), bf16[4,24,1024]{2,1,0:T(8,128)(2,1)S(1)}, u32[]{:S(2)}, u32[]{:S(2)}) async-start(bf16[4,24,1024]{2,1,0:T(8,128)(2,1)} %bitcast.9), calls=%async_computation.2 | async-start | bytes 393216 | tf_op jit(solution)/shard_map/all_to_all | solution.py:15
  84.9 1.7 convolution_convert_fusion.1
  86.6 0.0 copy-done.1
  86.6 0.7 convolution_convert_fusion
  87.3 1.9 %bitcast_bitcast_fusion = bf16[16,512,128]{2,1,0:T(8,128)(2,1)} fusion(bf16[256,2048]{1,0:T(8,128)(2,1)S(1)} %convolution_convert_fusion, bf16[256,2048]{1,0:T(8,128)(2,1)S(1)} %convolution_convert_fusion.1), kind=kLoop, calls=%fused_computation.3 | loop fusion | flops 4194304 | bytes 4194304 | tf_op jit(solution)/shard_map/transpose | solution.py:66
  89.2 8.3 %all-to-all-done.2 = bf16[4,24,1024]{2,1,0:T(8,128)(2,1)S(1)} async-done(((bf16[4,24,1024]{2,1,0:T(8,128)(2,1)}), bf16[4,24,1024]{2,1,0:T(8,128)(2,1)S(1)}, u32[]{:S(2)}, u32[]{:S(2)}) %all-to-all-start.2) | async-done | bytes 196640 | tf_op jit(solution)/shard_map/all_to_all | solution.py:15
  97.6 4.4 %all-to-all-start.3 = ((bf16[16,512,128]{2,1,0:T(8,128)(2,1)}), bf16[16,512,128]{2,1,0:T(8,128)(2,1)}, u32[]{:S(2)}, u32[]{:S(2)}) async-start(bf16[16,512,128]{2,1,0:T(8,128)(2,1)} %bitcast_bitcast_fusion), calls=%async_computation.3 | async-start | bytes 4194304 | tf_op jit(solution)/shard_map/all_to_all | solution.py:15
  102.0 15.9 %all_gather.6 = bf16[96,1024]{1,0:T(8,128)(2,1)S(1)} all-gather(bf16[24,1024]{1,0:T(8,128)(2,1)S(1)} %reduce_sum.57), channel_id=1, replica_groups=mesh['yh'=2,'yl'=2,'x'=4,'zh'=4,'zl'=4,'core'=2] {'zh'}, dimensions={0}, use_global_device_ids=true | all-gather | bytes 245760 | tf_op jit(solution)/shard_map/all_gather | solution.py:76
  118.0 19.7 %all_gather.7 = bf16[384,1024]{1,0:T(8,128)(2,1)S(1)} all-gather(bf16[96,1024]{1,0:T(8,128)(2,1)S(1)} %all_gather.6), channel_id=1, replica_groups=mesh['yh'=2,'yl'=2,'x'=4,'zh'=4,'zl'=4,'core'=2] {'zl'}, dimensions={0}, use_global_device_ids=true | all-gather | bytes 983040 | tf_op jit(solution)/shard_map/all_gather | solution.py:78
  137.6 8.8 %collective-permute-start.5 = (bf16[384,1024]{1,0:T(8,128)(2,1)S(1)}, bf16[384,1024]{1,0:T(8,128)(2,1)}, u32[]{:S(2)}, u32[]{:S(2)}) collective-permute-start(bf16[384,1024]{1,0:T(8,128)(2,1)S(1)} %all_gather.7), channel_id=1, source_target_pairs={{0,1},{1,0},{2,3},{3,2},{4,5},{5,4},{6,7},{7,6},{8,9},{9,8},{10,11... | collective-permute-start | bytes 2359304 | tf_op jit(solution)/shard_map/ppermute | solution.py:24
  146.4 0.0 all-to-all-done.3
  146.4 1.9 %convert_reduce_fusion = f32[512,128]{1,0:T(8,128)S(1)} fusion(bf16[16,512,128]{2,1,0:T(8,128)(2,1)} %all-to-all-done.3), kind=kLoop, calls=%fused_computation | loop fusion | flops 2031616 | bytes 2359296 | tf_op jit(solution)/shard_map/reduce_sum | solution.py:68
  148.3 0.7 multiply_reduce_fusion
  149.0 0.6 broadcast_in_dim.11
  149.6 6.7 %all-to-all-start.5 = ((f32[16,1,256]{2,1,0:T(1,128)}), f32[16,1,256]{2,1,0:T(1,128)S(1)}, u32[]{:S(2)}, u32[]{:S(2)}) async-start(f32[16,1,256]{2,1,0:T(1,128)} %broadcast_in_dim.11), calls=%async_computation.5 | async-start | bytes 32768 | tf_op jit(solution)/shard_map/all_to_all | solution.py:15
  156.3 0.0 collective-permute-done.5
  156.3 2.1 %broadcast_select_fusion.1 = (bf16[384,1024]{1,0:T(8,128)(2,1)S(1)}, bf16[384,1024]{1,0:T(8,128)(2,1)}) fusion(bf16[384,1024]{1,0:T(8,128)(2,1)S(1)} %all_gather.7, bf16[384,1024]{1,0:T(8,128)(2,1)} %collective-permute-done.5, pred[]{:T(512)S(6)} %eq.4), kind=kLoop, calls=%fused_computation.10 | loop fusion | flops 786432 | bytes 3145729 | tf_op jit(solution)/shard_map/jit(_where)/select_n | solution.py:81
  158.4 4.3 %all-to-all-done.5 = f32[16,1,256]{2,1,0:T(1,128)S(1)} async-done(((f32[16,1,256]{2,1,0:T(1,128)}), f32[16,1,256]{2,1,0:T(1,128)S(1)}, u32[]{:S(2)}, u32[]{:S(2)}) %all-to-all-start.5) | async-done | bytes 16416 | tf_op jit(solution)/shard_map/all_to_all | solution.py:15
  162.7 0.6 broadcast_in_dim.10
  163.3 8.3 %all-to-all-start.4 = ((f32[32,1,128]{2,1,0:T(1,128)}), f32[32,1,128]{2,1,0:T(1,128)S(1)}, u32[]{:S(2)}, u32[]{:S(2)}) async-start(f32[32,1,128]{2,1,0:T(1,128)} %broadcast_in_dim.10), calls=%async_computation.4 | async-start | bytes 32768 | tf_op jit(solution)/shard_map/all_to_all | solution.py:15
  171.7 2.4 %pad_maximum_fusion = bf16[384,2048]{1,0:T(8,128)(2,1)} fusion(bf16[384,1024]{1,0:T(8,128)(2,1)} %get-tuple-element.28, bf16[384,1024]{1,0:T(8,128)(2,1)S(1)} %get-tuple-element.27), kind=kLoop, calls=%fused_computation.5 | loop fusion | flops 3145728 | bytes 3145728 | tf_op jit(solution)/shard_map/concatenate | solution.py:80
  174.1 0.8 copy.22
  174.8 0.6 reduce_sum.62
  175.4 8.0 %all-to-all-done.4 = f32[32,1,128]{2,1,0:T(1,128)S(1)} async-done(((f32[32,1,128]{2,1,0:T(1,128)}), f32[32,1,128]{2,1,0:T(1,128)S(1)}, u32[]{:S(2)}, u32[]{:S(2)}) %all-to-all-start.4) | async-done | bytes 16416 | tf_op jit(solution)/shard_map/all_to_all | solution.py:15
  183.4 0.5 reduce_sum.60
  (1 shorter events, 0.0 us)
Async XLA Ops:
  0.6 30.4 %copy-start = (bf16[384,2048]{1,0:T(8,128)(2,1)S(1)}, bf16[384,2048]{1,0:T(8,128)(2,1)}, u32[]{:S(2)}) copy-start(bf16[384,2048]{1,0:T(8,128)(2,1)} %param.7) | copy-start | bytes 4718596
  1.7 8.7 %copy-start.4 = (bf16[128,256]{1,0:T(8,128)(2,1)S(1)}, bf16[128,256]{1,0:T(8,128)(2,1)}, u32[]{:S(2)}) copy-start(bf16[128,256]{1,0:T(8,128)(2,1)} %param.8) | copy-start | bytes 196612
  2.8 22.1 %all-to-all-start = ((bf16[16,128,256]{2,1,0:T(8,128)(2,1)}), bf16[16,128,256]{2,1,0:T(8,128)(2,1)S(1)}, u32[]{:S(2)}, u32[]{:S(2)}) async-start(bf16[16,128,256]{2,1,0:T(8,128)(2,1)} %broadcast_in_dim.8), calls=%async_computation | async-start | bytes 2097152 | tf_op jit(solution)/shard_map/all_to_all | solution.py:15
  10.4 20.6 %copy-start.3 = (bf16[384,256]{1,0:T(8,128)(2,1)S(1)}, bf16[384,256]{1,0:T(8,128)(2,1)}, u32[]{:S(2)}) copy-start(bf16[384,256]{1,0:T(8,128)(2,1)} %param.6) | copy-start | bytes 589828
  10.4 12.6 %collective-permute-start = (bf16[128,256]{1,0:T(8,128)(2,1)S(1)}, bf16[128,256]{1,0:T(8,128)(2,1)S(1)}, u32[]{:S(2)}, u32[]{:S(2)}) collective-permute-start(bf16[128,256]{1,0:T(8,128)(2,1)S(1)} %copy-done.4), channel_id=1, source_target_pairs={{0,0},{1,256},{256,257},{257,1},{2,2},{3,258},{258,259},{259,3},{4... | collective-permute-start | bytes 196616 | tf_op jit(solution)/shard_map/ppermute | solution.py:55
  24.9 1.3 copy-start.2
  26.2 18.8 %all-to-all-start.1 = ((bf16[16,128,256]{2,1,0:T(8,128)(2,1)}), bf16[16,128,256]{2,1,0:T(8,128)(2,1)S(1)}, u32[]{:S(2)}, u32[]{:S(2)}) async-start(bf16[16,128,256]{2,1,0:T(8,128)(2,1)} %broadcast_in_dim.9), calls=%async_computation.1 | async-start | bytes 2097152 | tf_op jit(solution)/shard_map/all_to_all | solution.py:15
  32.8 12.3 %collective-permute-start.1 = (bf16[384,256]{1,0:T(8,128)(2,1)S(1)}, bf16[384,256]{1,0:T(8,128)(2,1)S(1)}, u32[]{:S(2)}, u32[]{:S(2)}) collective-permute-start(bf16[384,256]{1,0:T(8,128)(2,1)S(1)} %fusion), channel_id=1, source_target_pairs={{0,1},{1,0},{2,3},{3,2},{4,5},{5,4},{6,7},{7,6},{8,9},{9,8},{10,11... | collective-permute-start | bytes 589832 | tf_op jit(solution)/shard_map/ppermute | solution.py:24
  46.0 13.2 %collective-permute-start.2 = (bf16[96,1024]{1,0:T(8,128)(2,1)S(1)}, bf16[96,1024]{1,0:T(8,128)(2,1)S(1)}, u32[]{:S(2)}, u32[]{:S(2)}) collective-permute-start(bf16[96,1024]{1,0:T(8,128)(2,1)S(1)} %get-tuple-element.31), channel_id=1, source_target_pairs={{0,2},{2,4},{4,6},{6,0},{1,3},{3,5},{5,7},{7,1},{8,10},{10,12},{12... | collective-permute-start | bytes 589832 | tf_op jit(solution)/shard_map/ppermute | solution.py:42
  51.6 15.9 %collective-permute-start.4 = (bf16[96,1024]{1,0:T(8,128)(2,1)S(1)}, bf16[96,1024]{1,0:T(8,128)(2,1)S(1)}, u32[]{:S(2)}, u32[]{:S(2)}) collective-permute-start(bf16[96,1024]{1,0:T(8,128)(2,1)S(1)} %get-tuple-element.32), channel_id=1, source_target_pairs={{0,4},{2,6},{4,0},{6,2},{1,5},{3,7},{5,1},{7,3},{8,12},{10,14},{12... | collective-permute-start | bytes 589832 | tf_op jit(solution)/shard_map/ppermute | solution.py:42
  56.5 11.0 %collective-permute-start.3 = (bf16[96,1024]{1,0:T(8,128)(2,1)S(1)}, bf16[96,1024]{1,0:T(8,128)(2,1)}, u32[]{:S(2)}, u32[]{:S(2)}) collective-permute-start(bf16[96,1024]{1,0:T(8,128)(2,1)S(1)} %get-tuple-element.33), channel_id=1, source_target_pairs={{0,6},{2,0},{4,2},{6,4},{1,7},{3,1},{5,3},{7,5},{8,14},{10,8},{12,... | collective-permute-start | bytes 589832 | tf_op jit(solution)/shard_map/ppermute | solution.py:42
  69.2 17.4 %copy-start.1 = (bf16[384,2048]{1,0:T(8,128)(2,1)S(1)}, bf16[384,2048]{1,0:T(8,128)(2,1)}, u32[]{:S(2)}) copy-start(bf16[384,2048]{1,0:T(8,128)(2,1)} %param.5) | copy-start | bytes 4718596
  69.2 28.3 %all-to-all-start.2 = ((bf16[4,24,1024]{2,1,0:T(8,128)(2,1)}), bf16[4,24,1024]{2,1,0:T(8,128)(2,1)S(1)}, u32[]{:S(2)}, u32[]{:S(2)}) async-start(bf16[4,24,1024]{2,1,0:T(8,128)(2,1)} %bitcast.9), calls=%async_computation.2 | async-start | bytes 393216 | tf_op jit(solution)/shard_map/all_to_all | solution.py:15
  97.6 48.9 %all-to-all-start.3 = ((bf16[16,512,128]{2,1,0:T(8,128)(2,1)}), bf16[16,512,128]{2,1,0:T(8,128)(2,1)}, u32[]{:S(2)}, u32[]{:S(2)}) async-start(bf16[16,512,128]{2,1,0:T(8,128)(2,1)} %bitcast_bitcast_fusion), calls=%async_computation.3 | async-start | bytes 4194304 | tf_op jit(solution)/shard_map/all_to_all | solution.py:15
  137.6 18.7 %collective-permute-start.5 = (bf16[384,1024]{1,0:T(8,128)(2,1)S(1)}, bf16[384,1024]{1,0:T(8,128)(2,1)}, u32[]{:S(2)}, u32[]{:S(2)}) collective-permute-start(bf16[384,1024]{1,0:T(8,128)(2,1)S(1)} %all_gather.7), channel_id=1, source_target_pairs={{0,1},{1,0},{2,3},{3,2},{4,5},{5,4},{6,7},{7,6},{8,9},{9,8},{10,11... | collective-permute-start | bytes 2359304 | tf_op jit(solution)/shard_map/ppermute | solution.py:24
  149.6 13.1 %all-to-all-start.5 = ((f32[16,1,256]{2,1,0:T(1,128)}), f32[16,1,256]{2,1,0:T(1,128)S(1)}, u32[]{:S(2)}, u32[]{:S(2)}) async-start(f32[16,1,256]{2,1,0:T(1,128)} %broadcast_in_dim.11), calls=%async_computation.5 | async-start | bytes 32768 | tf_op jit(solution)/shard_map/all_to_all | solution.py:15
  163.3 20.1 %all-to-all-start.4 = ((f32[32,1,128]{2,1,0:T(1,128)}), f32[32,1,128]{2,1,0:T(1,128)S(1)}, u32[]{:S(2)}, u32[]{:S(2)}) async-start(f32[32,1,128]{2,1,0:T(1,128)} %broadcast_in_dim.10), calls=%async_computation.4 | async-start | bytes 32768 | tf_op jit(solution)/shard_map/all_to_all | solution.py:15

commit v4 on v3

--- a/solution.py
+++ b/solution.py
@@ -30,21 +30,8 @@
     )
 
 
-def sum_near(half, axis):
-    count = lax.axis_size(axis)
-    here = lax.axis_index(axis)
-    pieces = half.reshape(count, half.shape[0] // count, half.shape[1])
-    total = lax.dynamic_index_in_dim(pieces, here, 0, False).astype(F32)
-    for step in (1, 3, 2):
-        there = lax.rem(here + step, count)
-        piece = lax.dynamic_index_in_dim(pieces, there, 0, False)
-        ring = [(i, (i + step) % count) for i in range(count)]
-        total += lax.ppermute(piece, axis, ring).astype(F32)
-    return total.astype(BF)
-
-
 def local(inputs, pre_act, cotangent, up_weight, down_weight):
-    tokens, width = inputs.shape
+    _, width = inputs.shape
     hidden = pre_act.shape[1]
     many = lax.axis_size(FS)
     core = lax.axis_index("core")
@@ -58,7 +45,7 @@
     sq_grad = dot(cotangent, down_columns, (1, 0))
     pre_grad = (2.0 * active * sq_grad).astype(BF)
     theirs = other_core(pre_grad)
-    half = (dot(pre_grad, up_rows[0], (1, 1)) + dot(theirs, up_rows[1], (1, 1))).astype(BF)
+    half = dot(pre_grad, up_rows[0], (1, 1)) + dot(theirs, up_rows[1], (1, 1))
 
     down_part = dot(squared, cotangent, (0, 0)).astype(BF)
     up_part = dot(pre_grad, inputs, (0, 0)).astype(BF)
@@ -68,14 +55,9 @@
     grads = jnp.sum(grads.astype(F32), axis=0)
     down_grad, up_grad = grads[:hidden], grads[hidden:]
 
-    half = sum_near(half, "zl")
-    pieces = exchange(half.reshape(4, tokens // 16, width // 2), "zh")
-    half = jnp.sum(pieces.astype(F32), axis=0).astype(BF)
-
+    half = lax.psum(half, ("zh", "zl")).astype(BF)
     up_norms = from_everyone(jnp.sum(up_grad * up_grad, axis=0), TP)
-    half = lax.all_gather(half, "zh", axis=0, tiled=True)
     down_norms = from_everyone(jnp.sum(down_grad * down_grad, axis=1), FS)
-    half = lax.all_gather(half, "zl", axis=0, tiled=True)
     both = other_core(half)
     input_grad = jnp.concatenate(
         [jnp.where(core == 0, half, both), jnp.where(core == 0, both, half)], axis=1

time: 185 us -> 175 us (0.946)
  blocking collectives: 35.6 us -> 70.5 us
  starting transfers between devices: 82.4 us -> 60.6 us
  waiting for transfers between devices: 42.6 us -> 23.2 us
  matrix products: 4.98 us -> 2.83 us
    psum x0 -> x1, blocking collectives: none -> 70.5 us  [local(): half = lax.psum(half, ('zh', 'zl')).astype(BF)]
    all_gather x2 -> x0, blocking collectives: 35.6 us -> none  [the longest x1 19.7 us: local(): half = lax.all_gather(half, 'zl', axis=0, tiled=True)]
    all_to_all x6 -> x5, starting transfers between devices: 47.4 us -> 33.2 us  [exchange(): return lax.all_to_all(array, axes, 0, 0, tiled=True)]
    ppermute x3 -> x0, starting transfers between devices: 13.1 us -> none  [sum_near(): total += lax.ppermute(piece, axis, ring).astype(F32)]
    all_to_all x6 -> x5, waiting for transfers between devices: 29.6 us -> 18.6 us  [exchange(): return lax.all_to_all(array, axes, 0, 0, tiled=True)]
    ppermute x3 -> x0, waiting for transfers between devices: 8.31 us -> none  [sum_near(): total += lax.ppermute(piece, axis, ring).astype(F32)]
    ppermute x2, starting transfers between devices: 14 us -> 19.4 us  [other_core(): return lax.ppermute(array, 'core', [(0, 1), (1, 0)])]
    dot_general x5, matrix products: 4.98 us -> 2.83 us  [dot(): lax.dot_general(left, right, ((over[:1], over[1:]), ((), ())), preferred_...]
  transfers between devices with their start and end apart: 12 -> 8, of which waited for: 7 -> 5; matrix products, arithmetic and copies ran while one was open for 8% -> 8% of each run, Pallas kernels for 0% -> 0%
where the time goes in v4:
time: 175 us; the launch traced here: 174 us
  blocking collectives  70.5 us (40%)
  starting transfers between devices  60.6 us (35%)
  waiting for transfers between devices  23.2 us (13%)
  other arithmetic  10.2 us (6%)
  local copies, waits for them, and re-layouts  6.02 us (3%)
  matrix products  2.83 us (2%)
    psum x1, blocking collectives, local(): half = lax.psum(half, ('zh', 'zl')).astype(BF)  70.5 us
    all_to_all x5, starting transfers between devices, exchange(): return lax.all_to_all(array, axes, 0, 0, tiled=True)  33.2 us
    ppermute x2, starting transfers between devices, other_core(): return lax.ppermute(array, 'core', [(0, 1), (1, 0)])  19.4 us
    all_to_all x5, waiting for transfers between devices, exchange(): return lax.all_to_all(array, axes, 0, 0, tiled=True)  18.6 us
    ppermute x1, starting transfers between devices, local(): lax.ppermute(up_weight, ('yh', 'core'), [(0, 0), (1, 2), (2, 3), (3, 1)])  7.92 us
    ppermute x1, waiting for transfers between devices, local(): lax.ppermute(up_weight, ('yh', 'core'), [(0, 0), (1, 2), (2, 3), (3, 1)])  4.65 us
  transfers between devices with their start and end apart: 8, of which 5 were waited for; matrix products, arithmetic and copies ran while one was open for 8% of the time, Pallas kernels for 0%

profile of v4, /device:TPU:1, one launch (start us, length us, event | category | flops | bytes accessed | tf_op | source)
XLA Modules:
  0.0 174.2 jit_solution(229934856447896750)
XLA Ops:
  0.6 0.0 copy-start
  0.6 1.1 copy.18
  1.7 0.0 copy-start.6
  1.7 1.1 broadcast_in_dim.8
  2.8 7.6 %all-to-all-start = ((bf16[16,128,256]{2,1,0:T(8,128)(2,1)}), bf16[16,128,256]{2,1,0:T(8,128)(2,1)S(1)}, u32[]{:S(2)}, u32[]{:S(2)}) async-start(bf16[16,128,256]{2,1,0:T(8,128)(2,1)} %broadcast_in_dim.8), calls=%async_computation | async-start | bytes 2097152 | tf_op jit(solution)/shard_map/all_to_all | solution.py:15
  10.4 0.0 copy-done.6
  10.4 0.0 copy-start.5
  10.4 7.9 %collective-permute-start = (bf16[128,256]{1,0:T(8,128)(2,1)S(1)}, bf16[128,256]{1,0:T(8,128)(2,1)S(1)}, u32[]{:S(2)}, u32[]{:S(2)}) collective-permute-start(bf16[128,256]{1,0:T(8,128)(2,1)S(1)} %copy-done.6), channel_id=1, source_target_pairs={{0,0},{1,256},{256,257},{257,1},{2,2},{3,258},{258,259},{259,3},{4... | collective-permute-start | bytes 196616 | tf_op jit(solution)/shard_map/ppermute | solution.py:42
  18.3 4.6 %collective-permute-done = bf16[128,256]{1,0:T(8,128)(2,1)S(1)} collective-permute-done((bf16[128,256]{1,0:T(8,128)(2,1)S(1)}, bf16[128,256]{1,0:T(8,128)(2,1)S(1)}, u32[]{:S(2)}, u32[]{:S(2)}) %collective-permute-start) | collective-permute-done | bytes 65568 | tf_op jit(solution)/shard_map/ppermute | solution.py:42
  23.0 1.9 %all-to-all-done = bf16[16,128,256]{2,1,0:T(8,128)(2,1)S(1)} async-done(((bf16[16,128,256]{2,1,0:T(8,128)(2,1)}), bf16[16,128,256]{2,1,0:T(8,128)(2,1)S(1)}, u32[]{:S(2)}, u32[]{:S(2)}) %all-to-all-start) | async-done | bytes 1048608 | tf_op jit(solution)/shard_map/all_to_all | solution.py:15
  24.9 0.0 copy-start.3
  24.9 1.2 broadcast_in_dim.9
  26.1 0.1 copy-done.3
  26.2 4.7 %all-to-all-start.1 = ((bf16[16,128,256]{2,1,0:T(8,128)(2,1)}), bf16[16,128,256]{2,1,0:T(8,128)(2,1)S(1)}, u32[]{:S(2)}, u32[]{:S(2)}) async-start(bf16[16,128,256]{2,1,0:T(8,128)(2,1)} %broadcast_in_dim.9), calls=%async_computation.1 | async-start | bytes 2097152 | tf_op jit(solution)/shard_map/all_to_all | solution.py:15
  31.0 0.0 copy-done
  31.0 0.0 copy-done.5
  31.0 0.0 copy-start.4
  31.0 0.7 convolution_convert_fusion.1
  31.8 0.5 copy-done.4
  32.2 0.0 copy-start.2
  32.2 0.6 fusion
  32.8 5.2 %collective-permute-start.1 = (bf16[384,256]{1,0:T(8,128)(2,1)S(1)}, bf16[384,256]{1,0:T(8,128)(2,1)S(1)}, u32[]{:S(2)}, u32[]{:S(2)}) collective-permute-start(bf16[384,256]{1,0:T(8,128)(2,1)S(1)} %fusion), channel_id=1, source_target_pairs={{0,1},{1,0},{2,3},{3,2},{4,5},{5,4},{6,7},{7,6},{8,9},{9,8},{10,11... | collective-permute-start | bytes 589832 | tf_op jit(solution)/shard_map/ppermute | solution.py:24
  38.0 0.0 copy-done.2
  38.0 0.7 convolution_convert_fusion
  38.7 1.9 %bitcast_bitcast_fusion = bf16[16,512,128]{2,1,0:T(8,128)(2,1)} fusion(bf16[256,2048]{1,0:T(8,128)(2,1)S(1)} %convolution_convert_fusion, bf16[256,2048]{1,0:T(8,128)(2,1)S(1)} %convolution_convert_fusion.1), kind=kLoop, calls=%fused_computation.3 | loop fusion | flops 4194304 | bytes 4194304 | tf_op jit(solution)/shard_map/transpose | solution.py:53
  40.6 4.4 %all-to-all-done.1 = bf16[16,128,256]{2,1,0:T(8,128)(2,1)S(1)} async-done(((bf16[16,128,256]{2,1,0:T(8,128)(2,1)}), bf16[16,128,256]{2,1,0:T(8,128)(2,1)S(1)}, u32[]{:S(2)}, u32[]{:S(2)}) %all-to-all-start.1) | async-done | bytes 1048608 | tf_op jit(solution)/shard_map/all_to_all | solution.py:15
  45.0 4.4 %all-to-all-start.2 = ((bf16[16,512,128]{2,1,0:T(8,128)(2,1)}), bf16[16,512,128]{2,1,0:T(8,128)(2,1)}, u32[]{:S(2)}, u32[]{:S(2)}) async-start(bf16[16,512,128]{2,1,0:T(8,128)(2,1)} %bitcast_bitcast_fusion), calls=%async_computation.2 | async-start | bytes 4194304 | tf_op jit(solution)/shard_map/all_to_all | solution.py:15
  49.5 0.1 fusion.3
  49.6 0.0 collective-permute-done.1
  49.6 0.4 fusion.4
  50.0 0.4 convolution_add_fusion
  50.4 70.5 %all-reduce.1 = bf16[384,1024]{1,0:T(8,128)(2,1)} all-reduce(f32[384,1024]{1,0:T(8,128)S(1)} %convolution_add_fusion), channel_id=1, replica_groups=mesh['yh'=2,'yl'=2,'x'=4,'zh'=4,'zl'=4,'core'=2] {'zh','zl'}, use_global_device_ids=true, to_apply=%region_0.0 | all-reduce | flops 393216 | bytes 2359296 | tf_op jit(solution)/shard_map/psum | solution.py:58
  120.9 0.0 copy-start.1
  120.9 14.3 %collective-permute-start.2 = (bf16[384,1024]{1,0:T(8,128)(2,1)}, bf16[384,1024]{1,0:T(8,128)(2,1)}, u32[]{:S(2)}, u32[]{:S(2)}) collective-permute-start(bf16[384,1024]{1,0:T(8,128)(2,1)} %all-reduce.1), channel_id=1, source_target_pairs={{0,1},{1,0},{2,3},{3,2},{4,5},{5,4},{6,7},{7,6},{8,9},{9,8},{10,11... | collective-permute-start | bytes 2359304 | tf_op jit(solution)/shard_map/ppermute | solution.py:24
  135.2 0.0 all-to-all-done.2
  135.2 1.9 %convert_reduce_fusion = f32[512,128]{1,0:T(8,128)S(1)} fusion(bf16[16,512,128]{2,1,0:T(8,128)(2,1)} %all-to-all-done.2), kind=kLoop, calls=%fused_computation | loop fusion | flops 2031616 | bytes 2359296 | tf_op jit(solution)/shard_map/reduce_sum | solution.py:55
  137.1 0.7 multiply_reduce_fusion
  137.8 0.6 broadcast_in_dim.11
  138.4 6.2 %all-to-all-start.4 = ((f32[16,1,256]{2,1,0:T(1,128)}), f32[16,1,256]{2,1,0:T(1,128)S(1)}, u32[]{:S(2)}, u32[]{:S(2)}) async-start(f32[16,1,256]{2,1,0:T(1,128)} %broadcast_in_dim.11), calls=%async_computation.4 | async-start | bytes 32768 | tf_op jit(solution)/shard_map/all_to_all | solution.py:15
  144.6 0.0 collective-permute-done.2
  144.6 0.0 copy-done.1
  144.6 2.1 %broadcast_select_fusion.1 = (bf16[384,1024]{1,0:T(8,128)(2,1)S(1)}, bf16[384,1024]{1,0:T(8,128)(2,1)}) fusion(bf16[384,1024]{1,0:T(8,128)(2,1)S(1)} %copy-done.1, bf16[384,1024]{1,0:T(8,128)(2,1)} %collective-permute-done.2, pred[]{:T(512)S(6)} %eq.4), kind=kLoop, calls=%fused_computation.10 | loop fusion | flops 786432 | bytes 3145729 | tf_op jit(solution)/shard_map/jit(_where)/select_n | solution.py:63
  146.7 4.3 %all-to-all-done.4 = f32[16,1,256]{2,1,0:T(1,128)S(1)} async-done(((f32[16,1,256]{2,1,0:T(1,128)}), f32[16,1,256]{2,1,0:T(1,128)S(1)}, u32[]{:S(2)}, u32[]{:S(2)}) %all-to-all-start.4) | async-done | bytes 16416 | tf_op jit(solution)/shard_map/all_to_all | solution.py:15
  151.0 0.6 broadcast_in_dim.10
  151.6 10.3 %all-to-all-start.3 = ((f32[32,1,128]{2,1,0:T(1,128)}), f32[32,1,128]{2,1,0:T(1,128)S(1)}, u32[]{:S(2)}, u32[]{:S(2)}) async-start(f32[32,1,128]{2,1,0:T(1,128)} %broadcast_in_dim.10), calls=%async_computation.3 | async-start | bytes 32768 | tf_op jit(solution)/shard_map/all_to_all | solution.py:15
  161.9 2.4 %pad_maximum_fusion = bf16[384,2048]{1,0:T(8,128)(2,1)} fusion(bf16[384,1024]{1,0:T(8,128)(2,1)} %get-tuple-element.28, bf16[384,1024]{1,0:T(8,128)(2,1)S(1)} %get-tuple-element.27), kind=kLoop, calls=%fused_computation.5 | loop fusion | flops 3145728 | bytes 3145728 | tf_op jit(solution)/shard_map/concatenate | solution.py:62
  164.3 0.8 copy.22
  165.1 0.6 reduce_sum.49
  165.7 7.9 %all-to-all-done.3 = f32[32,1,128]{2,1,0:T(1,128)S(1)} async-done(((f32[32,1,128]{2,1,0:T(1,128)}), f32[32,1,128]{2,1,0:T(1,128)S(1)}, u32[]{:S(2)}, u32[]{:S(2)}) %all-to-all-start.3) | async-done | bytes 16416 | tf_op jit(solution)/shard_map/all_to_all | solution.py:15
  173.6 0.5 reduce_sum.47
Async XLA Ops:
  0.6 30.4 %copy-start = (bf16[384,2048]{1,0:T(8,128)(2,1)S(1)}, bf16[384,2048]{1,0:T(8,128)(2,1)}, u32[]{:S(2)}) copy-start(bf16[384,2048]{1,0:T(8,128)(2,1)} %param.7) | copy-start | bytes 4718596
  1.7 8.7 %copy-start.6 = (bf16[128,256]{1,0:T(8,128)(2,1)S(1)}, bf16[128,256]{1,0:T(8,128)(2,1)}, u32[]{:S(2)}) copy-start(bf16[128,256]{1,0:T(8,128)(2,1)} %param.8) | copy-start | bytes 196612
  2.8 22.1 %all-to-all-start = ((bf16[16,128,256]{2,1,0:T(8,128)(2,1)}), bf16[16,128,256]{2,1,0:T(8,128)(2,1)S(1)}, u32[]{:S(2)}, u32[]{:S(2)}) async-start(bf16[16,128,256]{2,1,0:T(8,128)(2,1)} %broadcast_in_dim.8), calls=%async_computation | async-start | bytes 2097152 | tf_op jit(solution)/shard_map/all_to_all | solution.py:15
  10.4 20.6 %copy-start.5 = (bf16[384,256]{1,0:T(8,128)(2,1)S(1)}, bf16[384,256]{1,0:T(8,128)(2,1)}, u32[]{:S(2)}) copy-start(bf16[384,256]{1,0:T(8,128)(2,1)} %param.6) | copy-start | bytes 589828
  10.4 12.6 %collective-permute-start = (bf16[128,256]{1,0:T(8,128)(2,1)S(1)}, bf16[128,256]{1,0:T(8,128)(2,1)S(1)}, u32[]{:S(2)}, u32[]{:S(2)}) collective-permute-start(bf16[128,256]{1,0:T(8,128)(2,1)S(1)} %copy-done.6), channel_id=1, source_target_pairs={{0,0},{1,256},{256,257},{257,1},{2,2},{3,258},{258,259},{259,3},{4... | collective-permute-start | bytes 196616 | tf_op jit(solution)/shard_map/ppermute | solution.py:42
  24.9 1.3 copy-start.3
  26.2 18.8 %all-to-all-start.1 = ((bf16[16,128,256]{2,1,0:T(8,128)(2,1)}), bf16[16,128,256]{2,1,0:T(8,128)(2,1)S(1)}, u32[]{:S(2)}, u32[]{:S(2)}) async-start(bf16[16,128,256]{2,1,0:T(8,128)(2,1)} %broadcast_in_dim.9), calls=%async_computation.1 | async-start | bytes 2097152 | tf_op jit(solution)/shard_map/all_to_all | solution.py:15
  31.0 1.2 copy-start.4
  32.2 5.8 %copy-start.2 = (bf16[384,2048]{1,0:T(8,128)(2,1)S(1)}, bf16[384,2048]{1,0:T(8,128)(2,1)}, u32[]{:S(2)}) copy-start(bf16[384,2048]{1,0:T(8,128)(2,1)} %param.5) | copy-start | bytes 4718596
  32.8 16.8 %collective-permute-start.1 = (bf16[384,256]{1,0:T(8,128)(2,1)S(1)}, bf16[384,256]{1,0:T(8,128)(2,1)S(1)}, u32[]{:S(2)}, u32[]{:S(2)}) collective-permute-start(bf16[384,256]{1,0:T(8,128)(2,1)S(1)} %fusion), channel_id=1, source_target_pairs={{0,1},{1,0},{2,3},{3,2},{4,5},{5,4},{6,7},{7,6},{8,9},{9,8},{10,11... | collective-permute-start | bytes 589832 | tf_op jit(solution)/shard_map/ppermute | solution.py:24
  45.0 90.1 %all-to-all-start.2 = ((bf16[16,512,128]{2,1,0:T(8,128)(2,1)}), bf16[16,512,128]{2,1,0:T(8,128)(2,1)}, u32[]{:S(2)}, u32[]{:S(2)}) async-start(bf16[16,512,128]{2,1,0:T(8,128)(2,1)} %bitcast_bitcast_fusion), calls=%async_computation.2 | async-start | bytes 4194304 | tf_op jit(solution)/shard_map/all_to_all | solution.py:15
  120.9 23.7 %copy-start.1 = (bf16[384,1024]{1,0:T(8,128)(2,1)S(1)}, bf16[384,1024]{1,0:T(8,128)(2,1)}, u32[]{:S(2)}) copy-start(bf16[384,1024]{1,0:T(8,128)(2,1)} %all-reduce.1) | copy-start | bytes 2359300
  120.9 23.6 %collective-permute-start.2 = (bf16[384,1024]{1,0:T(8,128)(2,1)}, bf16[384,1024]{1,0:T(8,128)(2,1)}, u32[]{:S(2)}, u32[]{:S(2)}) collective-permute-start(bf16[384,1024]{1,0:T(8,128)(2,1)} %all-reduce.1), channel_id=1, source_target_pairs={{0,1},{1,0},{2,3},{3,2},{4,5},{5,4},{6,7},{7,6},{8,9},{9,8},{10,11... | collective-permute-start | bytes 2359304 | tf_op jit(solution)/shard_map/ppermute | solution.py:24
  138.4 12.6 %all-to-all-start.4 = ((f32[16,1,256]{2,1,0:T(1,128)}), f32[16,1,256]{2,1,0:T(1,128)S(1)}, u32[]{:S(2)}, u32[]{:S(2)}) async-start(f32[16,1,256]{2,1,0:T(1,128)} %broadcast_in_dim.11), calls=%async_computation.4 | async-start | bytes 32768 | tf_op jit(solution)/shard_map/all_to_all | solution.py:15
  151.6 22.0 %all-to-all-start.3 = ((f32[32,1,128]{2,1,0:T(1,128)}), f32[32,1,128]{2,1,0:T(1,128)S(1)}, u32[]{:S(2)}, u32[]{:S(2)}) async-start(f32[32,1,128]{2,1,0:T(1,128)} %broadcast_in_dim.10), calls=%async_computation.3 | async-start | bytes 32768 | tf_op jit(solution)/shard_map/all_to_all | solution.py:15

commit v5 on v4

--- a/solution.py
+++ b/solution.py
@@ -30,40 +30,55 @@
     )
 
 
+def gather_ring(block, axes):
+    count = lax.axis_size(axes)
+    here = lax.axis_index(axes)
+    blocks = jnp.zeros((count, *block.shape), block.dtype)
+    blocks = lax.dynamic_update_index_in_dim(blocks, block, here, 0)
+    for step in (1, 3, 2):
+        ring = [(i, (i + step) % count) for i in range(count)]
+        got = lax.ppermute(block, axes, ring)
+        there = lax.rem(here + count - step, count)
+        blocks = lax.dynamic_update_index_in_dim(blocks, got, there, 0)
+    return blocks
+
+
+def sum_at_owner(part):
+    rows, width = part.shape
+    many = lax.axis_size(FS)
+    blocks = jnp.moveaxis(part.reshape(rows, many, width // many), 1, 0)
+    return jnp.sum(exchange(blocks, FS).astype(F32), axis=0)
+
+
 def local(inputs, pre_act, cotangent, up_weight, down_weight):
     _, width = inputs.shape
     hidden = pre_act.shape[1]
-    many = lax.axis_size(FS)
     core = lax.axis_index("core")
     active = jnp.maximum(pre_act.astype(F32), 0.0)
     squared = (active * active).astype(BF)
 
     down_columns = from_everyone(down_weight.T, FS).reshape(width, hidden)
     rows = lax.ppermute(up_weight, ("yh", "core"), [(0, 0), (1, 2), (2, 3), (3, 1)])
-    up_rows = from_everyone(rows, FS).reshape(2, width // 2, hidden)
+    rows = lax.all_gather(rows, "x", axis=0, tiled=True)
+    up_rows = gather_ring(rows, ("yh", "yl")).reshape(2, width // 2, hidden)
 
     sq_grad = dot(cotangent, down_columns, (1, 0))
     pre_grad = (2.0 * active * sq_grad).astype(BF)
     theirs = other_core(pre_grad)
     half = dot(pre_grad, up_rows[0], (1, 1)) + dot(theirs, up_rows[1], (1, 1))
 
-    down_part = dot(squared, cotangent, (0, 0)).astype(BF)
-    up_part = dot(pre_grad, inputs, (0, 0)).astype(BF)
-    parts = jnp.concatenate([down_part, up_part], axis=0)
-    parts = jnp.moveaxis(parts.reshape(2 * hidden, many, width // many), 1, 0)
-    grads = exchange(parts, FS)
-    grads = jnp.sum(grads.astype(F32), axis=0)
-    down_grad, up_grad = grads[:hidden], grads[hidden:]
+    up_grad = sum_at_owner(dot(pre_grad, inputs, (0, 0)).astype(BF))
+    down_grad = sum_at_owner(dot(squared, cotangent, (0, 0)).astype(BF))
 
-    half = lax.psum(half, ("zh", "zl")).astype(BF)
-    up_norms = from_everyone(jnp.sum(up_grad * up_grad, axis=0), TP)
+    half, up_norms = lax.psum((half, jnp.sum(up_grad * up_grad, axis=0)), ("zh", "zl"))
+    half = half.astype(BF)
+    up_norms += other_core(up_norms)
     down_norms = from_everyone(jnp.sum(down_grad * down_grad, axis=1), FS)
     both = other_core(half)
     input_grad = jnp.concatenate(
         [jnp.where(core == 0, half, both), jnp.where(core == 0, both, half)], axis=1
     )
-    up_norms, down_norms = jnp.sum(up_norms, axis=0), jnp.sum(down_norms, axis=0)
-    return input_grad, up_grad.T, down_grad, up_norms, down_norms
+    return input_grad, up_grad.T, down_grad, up_norms, jnp.sum(down_norms, axis=0)
 
 
 def solution(mesh):

time: 175 us -> 185 us (1.057)
  blocking collectives: 70.5 us -> 88.9 us
  waiting for transfers between devices: 23.2 us -> 5.69 us
  starting transfers between devices: 60.6 us -> 71.9 us
  other arithmetic: 10.2 us -> 5.38 us
    all_gather x0 -> x1, blocking collectives: none -> 19.6 us  [local(): rows = lax.all_gather(rows, 'x', axis=0, tiled=True)]
    all_to_all x5 -> x4, waiting for transfers between devices: 18.6 us -> 4.23 us  [exchange(): return lax.all_to_all(array, axes, 0, 0, tiled=True)]
    ppermute x2 -> x3, starting transfers between devices: 19.4 us -> 32.8 us  [other_core(): return lax.ppermute(array, 'core', [(0, 1), (1, 0)])]
    all_to_all x5 -> x4, starting transfers between devices: 33.2 us -> 23 us  [exchange(): return lax.all_to_all(array, axes, 0, 0, tiled=True)]
    ppermute x0 -> x3, starting transfers between devices: none -> 9.81 us  [gather_ring(): got = lax.ppermute(block, axes, ring)]
    ppermute x1, waiting for transfers between devices: 4.65 us -> 0.01 us  [local(): lax.ppermute(up_weight, ('yh', 'core'), [(0, 0), (1, 2), (2, 3), (3, 1)])]
    reshape x0 -> x2, local copies, waits for them, and re-layouts: none -> 2.49 us  [sum_at_owner(): blocks = jnp.moveaxis(part.reshape(rows, many, width // many), 1, 0)]
    select_n x1, other arithmetic: 2.14 us -> 0.11 us  [local(): jnp.where(core == 0, half, both)]
  transfers between devices with their start and end apart: 8 -> 11, of which waited for: 5 -> 3; matrix products, arithmetic and copies ran while one was open for 8% -> 8% of each run, Pallas kernels for 0% -> 0%
where the time goes in v5:
time: 185 us; the launch traced here: 184 us
  blocking collectives  88.9 us (48%)
  starting transfers between devices  71.9 us (39%)
  local copies, waits for them, and re-layouts  7.09 us (4%)
  waiting for transfers between devices  5.69 us (3%)
  other arithmetic  5.38 us (3%)
  matrix products  4.19 us (2%)
    psum x1, blocking collectives, local(): lax.psum((half, jnp.sum(up_grad * up_grad, axis=0)), ('zh', 'zl'))  69.3 us
    ppermute x3, starting transfers between devices, other_core(): return lax.ppermute(array, 'core', [(0, 1), (1, 0)])  32.8 us
    all_to_all x4, starting transfers between devices, exchange(): return lax.all_to_all(array, axes, 0, 0, tiled=True)  23 us
    all_gather x1, blocking collectives, local(): rows = lax.all_gather(rows, 'x', axis=0, tiled=True)  19.6 us
    ppermute x3, starting transfers between devices, gather_ring(): got = lax.ppermute(block, axes, ring)  9.81 us
    ppermute x1, starting transfers between devices, local(): lax.ppermute(up_weight, ('yh', 'core'), [(0, 0), (1, 2), (2, 3), (3, 1)])  6.33 us
    all_to_all x4, waiting for transfers between devices, exchange(): return lax.all_to_all(array, axes, 0, 0, tiled=True)  4.23 us
    dot_general x5, matrix products, dot(): lax.dot_general(left, right, ((over[:1], over[1:]), ((), ())), preferred_...  4.19 us
  transfers between devices with their start and end apart: 11, of which 3 were waited for; matrix products, arithmetic and copies ran while one was open for 8% of the time, Pallas kernels for 0%

profile of v5, /device:TPU:1, one launch (start us, length us, event | category | flops | bytes accessed | tf_op | source)
XLA Modules:
  0.0 184.1 jit_solution(17560600010842546769)
XLA Ops:
  0.6 0.0 copy-start
  0.6 6.3 %collective-permute-start = (bf16[128,256]{1,0:T(8,128)(2,1)}, bf16[128,256]{1,0:T(8,128)(2,1)S(1)}, u32[]{:S(2)}, u32[]{:S(2)}) collective-permute-start(bf16[128,256]{1,0:T(8,128)(2,1)} %param.8), channel_id=1, source_target_pairs={{0,0},{1,256},{256,257},{257,1},{2,2},{3,258},{258,259},{259,3},{4... | collective-permute-start | bytes 196616 | tf_op jit(solution)/shard_map/ppermute | solution.py:61
  7.0 0.9 copy.21
  7.9 0.0 copy-start.4
  7.9 1.1 broadcast_in_dim.28
  9.0 4.3 %all-to-all-start = ((bf16[16,128,256]{2,1,0:T(8,128)(2,1)}), bf16[16,128,256]{2,1,0:T(8,128)(2,1)}, u32[]{:S(2)}, u32[]{:S(2)}) async-start(bf16[16,128,256]{2,1,0:T(8,128)(2,1)} %broadcast_in_dim.28), calls=%async_computation | async-start | bytes 2097152 | tf_op jit(solution)/shard_map/all_to_all | solution.py:15
  13.4 0.0 collective-permute-done
  13.4 19.6 %all_gather.3 = bf16[512,256]{1,0:T(8,128)(2,1)S(1)} all-gather(bf16[128,256]{1,0:T(8,128)(2,1)S(1)} %collective-permute-done), channel_id=1, replica_groups=mesh['yh'=2,'yl'=2,'x'=4,'zh'=4,'zl'=4,'core'=2] {'x'}, dimensions={0}, use_global_device_ids=true | all-gather | bytes 327680 | tf_op jit(solution)/shard_map/all_gather | solution.py:62
  33.0 3.1 %collective-permute-start.1 = (bf16[512,256]{1,0:T(8,128)(2,1)S(1)}, bf16[512,256]{1,0:T(8,128)(2,1)S(1)}, u32[]{:S(2)}, u32[]{:S(2)}) collective-permute-start(bf16[512,256]{1,0:T(8,128)(2,1)S(1)} %all_gather.3), channel_id=1, source_target_pairs={{0,128},{128,256},{256,384},{384,0},{1,129},{129,257},{257,385},{3... | collective-permute-start | bytes 786440 | tf_op jit(solution)/shard_map/ppermute | solution.py:40
  36.0 0.0 copy-done
  36.0 0.0 copy-done.4
  36.0 0.7 fusion.1
  36.8 1.2 copy.33
  38.1 3.4 %collective-permute-start.2 = (bf16[512,256]{1,0:T(8,128)(2,1)S(1)}, bf16[512,256]{1,0:T(8,128)(2,1)S(1)}, u32[]{:S(2)}, u32[]{:S(2)}) collective-permute-start(bf16[512,256]{1,0:T(8,128)(2,1)S(1)} %all_gather.3), channel_id=1, source_target_pairs={{0,384},{128,0},{256,128},{384,256},{1,385},{129,1},{257,129},{385... | collective-permute-start | bytes 786440 | tf_op jit(solution)/shard_map/ppermute | solution.py:40
  41.5 3.3 %collective-permute-start.3 = (bf16[512,256]{1,0:T(8,128)(2,1)S(1)}, bf16[512,256]{1,0:T(8,128)(2,1)}, u32[]{:S(2)}, u32[]{:S(2)}) collective-permute-start(bf16[512,256]{1,0:T(8,128)(2,1)S(1)} %all_gather.3), channel_id=1, source_target_pairs={{0,256},{128,384},{256,0},{384,128},{1,257},{129,385},{257,1},{385... | collective-permute-start | bytes 786440 | tf_op jit(solution)/shard_map/ppermute | solution.py:40
  44.8 0.1 broadcast_in_dim.29
  44.9 0.0 collective-permute-done.1
  45.0 0.5 collective-permute-done.2
  45.5 0.0 all-to-all-done
  45.5 0.0 copy-start.1
  45.5 1.9 %fusion.2 = bf16[384,256]{1,0:T(8,128)(2,1)S(1)} fusion(bf16[384,2048]{1,0:T(8,128)(2,1)S(1)} %copy-done, bf16[2048,256]{1,0:T(8,128)(2,1)} %bitcast.1, bf16[384,256]{1,0:T(8,128)(2,1)} %param.6), kind=kOutput, calls=%fused_computation.9 | convolution fusion | flops 403144704 | bytes 3014656 | tf_op jit(solution)/shard_map/dot_general | solution.py:28
  47.4 0.0 copy-done.1
  47.4 0.7 fusion
  48.2 1.2 copy.34
  49.4 4.8 %all-to-all-start.1 = ((bf16[16,256,128]{2,1,0:T(8,128)(2,1)}), bf16[16,256,128]{2,1,0:T(8,128)(2,1)}, u32[]{:S(2)}, u32[]{:S(2)}) async-start(bf16[16,256,128]{2,1,0:T(8,128)(2,1)} %bitcast.37), calls=%async_computation.1 | async-start | bytes 2097152 | tf_op jit(solution)/shard_map/all_to_all | solution.py:15
  54.2 0.0 collective-permute-done.3
  54.2 1.0 bitcast_dynamic-update-slice_fusion
  55.2 12.2 %collective-permute-start.4 = (bf16[384,256]{1,0:T(8,128)(2,1)S(1)}, bf16[384,256]{1,0:T(8,128)(2,1)S(1)}, u32[]{:S(2)}, u32[]{:S(2)}) collective-permute-start(bf16[384,256]{1,0:T(8,128)(2,1)S(1)} %fusion.2), channel_id=1, source_target_pairs={{0,1},{1,0},{2,3},{3,2},{4,5},{5,4},{6,7},{7,6},{8,9},{9,8},{10,11... | collective-permute-start | bytes 589832 | tf_op jit(solution)/shard_map/ppermute | solution.py:24
  67.4 0.1 fusion.5
  67.5 1.0 collective-permute-done.4
  68.5 0.4 fusion.6
  68.9 0.4 convolution_add_fusion
  69.3 0.0 all-to-all-done.1
  69.3 6.9 %all-to-all-start.2 = ((bf16[16,256,128]{2,1,0:T(8,128)(2,1)}), bf16[16,256,128]{2,1,0:T(8,128)(2,1)}, u32[]{:S(2)}, u32[]{:S(2)}) async-start(bf16[16,256,128]{2,1,0:T(8,128)(2,1)} %bitcast.38), calls=%async_computation.2 | async-start | bytes 2097152 | tf_op jit(solution)/shard_map/all_to_all | solution.py:15
  76.3 1.4 convert_reduce_fusion.1
  77.7 69.3 %all-reduce.2 = (bf16[384,1024]{1,0:T(8,128)(2,1)}, f32[128]{0:T(128)S(1)}) all-reduce(f32[384,1024]{1,0:T(8,128)S(1)} %convolution_add_fusion, f32[128]{0:T(128)S(1)} %multiply_reduce_fusion.1), channel_id=1, replica_groups=mesh['yh'=2,'yl'=2,'x'=4,'zh'=4,'zl'=4,'core'=2] {'zh','zl'}, use_global_device_ids=true, to_apply=%region_0.1 | all-reduce | flops 393344 | bytes 2360320 | tf_op jit(solution)/shard_map/psum | solution.py:73
  147.0 0.0 copy-start.2
  147.0 18.3 %collective-permute-start.5 = (bf16[384,1024]{1,0:T(8,128)(2,1)}, bf16[384,1024]{1,0:T(8,128)(2,1)S(1)}, u32[]{:S(2)}, u32[]{:S(2)}) collective-permute-start(bf16[384,1024]{1,0:T(8,128)(2,1)} %get-tuple-element.20), channel_id=1, source_target_pairs={{0,1},{1,0},{2,3},{3,2},{4,5},{5,4},{6,7},{7,6},{8,9},{9,8},{10,11... | collective-permute-start | bytes 2359304 | tf_op jit(solution)/shard_map/ppermute | solution.py:24
  165.3 0.0 all-to-all-done.2
  165.3 1.4 convert_reduce_fusion
  166.7 0.0 copy-start.3
  166.7 0.1 multiply_reduce_fusion
  166.8 0.6 broadcast_in_dim.34
  167.5 6.9 %all-to-all-start.3 = ((f32[16,1,256]{2,1,0:T(1,128)}), f32[16,1,256]{2,1,0:T(1,128)S(1)}, u32[]{:S(2)}, u32[]{:S(2)}) async-start(f32[16,1,256]{2,1,0:T(1,128)} %broadcast_in_dim.34), calls=%async_computation.3 | async-start | bytes 32768 | tf_op jit(solution)/shard_map/all_to_all | solution.py:15
  174.4 2.2 %collective-permute-start.6 = (f32[128]{0:T(128)S(1)}, f32[128]{0:T(128)S(1)}, u32[]{:S(2)}, u32[]{:S(2)}) collective-permute-start(f32[128]{0:T(128)S(1)} %get-tuple-element.21), channel_id=1, source_target_pairs={{0,1},{1,0},{2,3},{3,2},{4,5},{5,4},{6,7},{7,6},{8,9},{9,8},{10,11... | collective-permute-start | bytes 1544 | tf_op jit(solution)/shard_map/ppermute | solution.py:24
  176.6 4.2 %all-to-all-done.3 = f32[16,1,256]{2,1,0:T(1,128)S(1)} async-done(((f32[16,1,256]{2,1,0:T(1,128)}), f32[16,1,256]{2,1,0:T(1,128)S(1)}, u32[]{:S(2)}, u32[]{:S(2)}) %all-to-all-start.3) | async-done | bytes 16416 | tf_op jit(solution)/shard_map/all_to_all | solution.py:15
  180.8 0.6 reduce_sum.49
  181.4 0.8 copy.26
  182.2 0.0 collective-permute-done.6
  182.2 0.5 add.44
  182.7 0.0 collective-permute-done.5
  182.7 0.0 copy-done.2
  182.7 0.1 broadcast_select_fusion.1
  182.8 0.0 copy-done.3
  182.8 1.2 pad_maximum_fusion
  (4 shorter events, 0.1 us)
Async XLA Ops:
  0.6 35.4 %copy-start = (bf16[384,2048]{1,0:T(8,128)(2,1)S(1)}, bf16[384,2048]{1,0:T(8,128)(2,1)}, u32[]{:S(2)}) copy-start(bf16[384,2048]{1,0:T(8,128)(2,1)} %param.7) | copy-start | bytes 4718596
  0.6 12.7 %collective-permute-start = (bf16[128,256]{1,0:T(8,128)(2,1)}, bf16[128,256]{1,0:T(8,128)(2,1)S(1)}, u32[]{:S(2)}, u32[]{:S(2)}) collective-permute-start(bf16[128,256]{1,0:T(8,128)(2,1)} %param.8), channel_id=1, source_target_pairs={{0,0},{1,256},{256,257},{257,1},{2,2},{3,258},{258,259},{259,3},{4... | collective-permute-start | bytes 196616 | tf_op jit(solution)/shard_map/ppermute | solution.py:61
  7.9 28.1 %copy-start.4 = (bf16[384,256]{1,0:T(8,128)(2,1)S(1)}, bf16[384,256]{1,0:T(8,128)(2,1)}, u32[]{:S(2)}) copy-start(bf16[384,256]{1,0:T(8,128)(2,1)} %param.6) | copy-start | bytes 589828
  9.0 36.5 %all-to-all-start = ((bf16[16,128,256]{2,1,0:T(8,128)(2,1)}), bf16[16,128,256]{2,1,0:T(8,128)(2,1)}, u32[]{:S(2)}, u32[]{:S(2)}) async-start(bf16[16,128,256]{2,1,0:T(8,128)(2,1)} %broadcast_in_dim.28), calls=%async_computation | async-start | bytes 2097152 | tf_op jit(solution)/shard_map/all_to_all | solution.py:15
  33.0 12.0 %collective-permute-start.1 = (bf16[512,256]{1,0:T(8,128)(2,1)S(1)}, bf16[512,256]{1,0:T(8,128)(2,1)S(1)}, u32[]{:S(2)}, u32[]{:S(2)}) collective-permute-start(bf16[512,256]{1,0:T(8,128)(2,1)S(1)} %all_gather.3), channel_id=1, source_target_pairs={{0,128},{128,256},{256,384},{384,0},{1,129},{129,257},{257,385},{3... | collective-permute-start | bytes 786440 | tf_op jit(solution)/shard_map/ppermute | solution.py:40
  38.1 7.4 %collective-permute-start.2 = (bf16[512,256]{1,0:T(8,128)(2,1)S(1)}, bf16[512,256]{1,0:T(8,128)(2,1)S(1)}, u32[]{:S(2)}, u32[]{:S(2)}) collective-permute-start(bf16[512,256]{1,0:T(8,128)(2,1)S(1)} %all_gather.3), channel_id=1, source_target_pairs={{0,384},{128,0},{256,128},{384,256},{1,385},{129,1},{257,129},{385... | collective-permute-start | bytes 786440 | tf_op jit(solution)/shard_map/ppermute | solution.py:40
  41.5 12.7 %collective-permute-start.3 = (bf16[512,256]{1,0:T(8,128)(2,1)S(1)}, bf16[512,256]{1,0:T(8,128)(2,1)}, u32[]{:S(2)}, u32[]{:S(2)}) collective-permute-start(bf16[512,256]{1,0:T(8,128)(2,1)S(1)} %all_gather.3), channel_id=1, source_target_pairs={{0,256},{128,384},{256,0},{384,128},{1,257},{129,385},{257,1},{385... | collective-permute-start | bytes 786440 | tf_op jit(solution)/shard_map/ppermute | solution.py:40
  45.5 2.0 %copy-start.1 = (bf16[384,2048]{1,0:T(8,128)(2,1)S(1)}, bf16[384,2048]{1,0:T(8,128)(2,1)}, u32[]{:S(2)}) copy-start(bf16[384,2048]{1,0:T(8,128)(2,1)} %param.5) | copy-start | bytes 4718596
  49.4 19.9 %all-to-all-start.1 = ((bf16[16,256,128]{2,1,0:T(8,128)(2,1)}), bf16[16,256,128]{2,1,0:T(8,128)(2,1)}, u32[]{:S(2)}, u32[]{:S(2)}) async-start(bf16[16,256,128]{2,1,0:T(8,128)(2,1)} %bitcast.37), calls=%async_computation.1 | async-start | bytes 2097152 | tf_op jit(solution)/shard_map/all_to_all | solution.py:15
  55.2 13.3 %collective-permute-start.4 = (bf16[384,256]{1,0:T(8,128)(2,1)S(1)}, bf16[384,256]{1,0:T(8,128)(2,1)S(1)}, u32[]{:S(2)}, u32[]{:S(2)}) collective-permute-start(bf16[384,256]{1,0:T(8,128)(2,1)S(1)} %fusion.2), channel_id=1, source_target_pairs={{0,1},{1,0},{2,3},{3,2},{4,5},{5,4},{6,7},{7,6},{8,9},{9,8},{10,11... | collective-permute-start | bytes 589832 | tf_op jit(solution)/shard_map/ppermute | solution.py:24
  69.3 96.0 %all-to-all-start.2 = ((bf16[16,256,128]{2,1,0:T(8,128)(2,1)}), bf16[16,256,128]{2,1,0:T(8,128)(2,1)}, u32[]{:S(2)}, u32[]{:S(2)}) async-start(bf16[16,256,128]{2,1,0:T(8,128)(2,1)} %bitcast.38), calls=%async_computation.2 | async-start | bytes 2097152 | tf_op jit(solution)/shard_map/all_to_all | solution.py:15
  147.0 35.7 %copy-start.2 = (bf16[384,1024]{1,0:T(8,128)(2,1)S(1)}, bf16[384,1024]{1,0:T(8,128)(2,1)}, u32[]{:S(2)}) copy-start(bf16[384,1024]{1,0:T(8,128)(2,1)} %get-tuple-element.20) | copy-start | bytes 2359300
  147.0 35.7 %collective-permute-start.5 = (bf16[384,1024]{1,0:T(8,128)(2,1)}, bf16[384,1024]{1,0:T(8,128)(2,1)S(1)}, u32[]{:S(2)}, u32[]{:S(2)}) collective-permute-start(bf16[384,1024]{1,0:T(8,128)(2,1)} %get-tuple-element.20), channel_id=1, source_target_pairs={{0,1},{1,0},{2,3},{3,2},{4,5},{5,4},{6,7},{7,6},{8,9},{9,8},{10,11... | collective-permute-start | bytes 2359304 | tf_op jit(solution)/shard_map/ppermute | solution.py:24
  166.7 16.1 %copy-start.3 = (f32[256,128]{1,0:T(8,128)}, f32[256,128]{1,0:T(8,128)S(1)}, u32[]{:S(2)}) copy-start(f32[256,128]{1,0:T(8,128)S(1)} %convert_reduce_fusion) | copy-start | bytes 393220
  167.5 13.4 %all-to-all-start.3 = ((f32[16,1,256]{2,1,0:T(1,128)}), f32[16,1,256]{2,1,0:T(1,128)S(1)}, u32[]{:S(2)}, u32[]{:S(2)}) async-start(f32[16,1,256]{2,1,0:T(1,128)} %broadcast_in_dim.34), calls=%async_computation.3 | async-start | bytes 32768 | tf_op jit(solution)/shard_map/all_to_all | solution.py:15
  174.4 7.8 %collective-permute-start.6 = (f32[128]{0:T(128)S(1)}, f32[128]{0:T(128)S(1)}, u32[]{:S(2)}, u32[]{:S(2)}) collective-permute-start(f32[128]{0:T(128)S(1)} %get-tuple-element.21), channel_id=1, source_target_pairs={{0,1},{1,0},{2,3},{3,2},{4,5},{5,4},{6,7},{7,6},{8,9},{9,8},{10,11... | collective-permute-start | bytes 1544 | tf_op jit(solution)/shard_map/ppermute | solution.py:24

commit v6 on v4

--- a/solution.py
+++ b/solution.py
@@ -57,12 +57,13 @@
 
     half = lax.psum(half, ("zh", "zl")).astype(BF)
     up_norms = from_everyone(jnp.sum(up_grad * up_grad, axis=0), TP)
-    down_norms = from_everyone(jnp.sum(down_grad * down_grad, axis=1), FS)
+    down_norms = lax.psum(jnp.sum(down_grad * down_grad, axis=1), ("yh", "yl"))
+    down_norms = lax.psum(down_norms, "x")
     both = other_core(half)
     input_grad = jnp.concatenate(
         [jnp.where(core == 0, half, both), jnp.where(core == 0, both, half)], axis=1
     )
-    up_norms, down_norms = jnp.sum(up_norms, axis=0), jnp.sum(down_norms, axis=0)
+    up_norms = jnp.sum(up_norms, axis=0)
     return input_grad, up_grad.T, down_grad, up_norms, down_norms
 
 

time: 175 us -> 175 us (level); the launches traced: 174 us -> 172 us
  blocking collectives: 70.5 us -> 90.5 us
  waiting for transfers between devices: 23.2 us -> 13.2 us
  starting transfers between devices: 60.6 us -> 51.3 us
  other arithmetic: 10.2 us -> 7.76 us
    psum x0 -> x2, blocking collectives: none -> 20 us  [the longest x1 10.5 us: local(): down_norms = lax.psum(jnp.sum(down_grad * down_grad, axis=1), ('yh', 'yl'))]
    all_to_all x5 -> x4, waiting for transfers between devices: 18.6 us -> 6.35 us  [exchange(): return lax.all_to_all(array, axes, 0, 0, tiled=True)]
    all_to_all x5 -> x4, starting transfers between devices: 33.2 us -> 24.1 us  [exchange(): return lax.all_to_all(array, axes, 0, 0, tiled=True)]
    ppermute x2, waiting for transfers between devices: 0.01 us -> 2.23 us  [other_core(): return lax.ppermute(array, 'core', [(0, 1), (1, 0)])]
  transfers between devices with their start and end apart: 8 -> 7, of which waited for: 5 -> 4; matrix products, arithmetic and copies ran while one was open for 8% -> 5% of each run, Pallas kernels for 0% -> 0%
where the time goes in v6:
time: 175 us; the launch traced here: 172 us
  blocking collectives  90.5 us (52%)
  starting transfers between devices  51.3 us (29%)
  waiting for transfers between devices  13.2 us (8%)
  other arithmetic  7.76 us (4%)
  local copies, waits for them, and re-layouts  5.4 us (3%)
  matrix products  2.83 us (2%)
    psum x1, blocking collectives, local(): half = lax.psum(half, ('zh', 'zl')).astype(BF)  70.5 us
    all_to_all x4, starting transfers between devices, exchange(): return lax.all_to_all(array, axes, 0, 0, tiled=True)  24.1 us
    ppermute x2, starting transfers between devices, other_core(): return lax.ppermute(array, 'core', [(0, 1), (1, 0)])  19.3 us
    psum x1, blocking collectives, local(): down_norms = lax.psum(jnp.sum(down_grad * down_grad, axis=1), ('yh', 'yl'))  10.5 us
    psum x1, blocking collectives, local(): down_norms = lax.psum(down_norms, 'x')  9.51 us
    ppermute x1, starting transfers between devices, local(): lax.ppermute(up_weight, ('yh', 'core'), [(0, 0), (1, 2), (2, 3), (3, 1)])  7.92 us
    all_to_all x4, waiting for transfers between devices, exchange(): return lax.all_to_all(array, axes, 0, 0, tiled=True)  6.35 us
    ppermute x1, waiting for transfers between devices, local(): lax.ppermute(up_weight, ('yh', 'core'), [(0, 0), (1, 2), (2, 3), (3, 1)])  4.65 us
  transfers between devices with their start and end apart: 7, of which 4 were waited for; matrix products, arithmetic and copies ran while one was open for 5% of the time, Pallas kernels for 0%

profile of v6, /device:TPU:1, one launch (start us, length us, event | category | flops | bytes accessed | tf_op | source)
XLA Modules:
  0.0 171.9 jit_solution(14783247208691357248)
XLA Ops:
  0.6 0.0 copy-start
  0.6 1.1 copy.18
  1.7 0.0 copy-start.5
  1.7 1.1 broadcast_in_dim.6
  2.8 7.6 %all-to-all-start = ((bf16[16,128,256]{2,1,0:T(8,128)(2,1)}), bf16[16,128,256]{2,1,0:T(8,128)(2,1)S(1)}, u32[]{:S(2)}, u32[]{:S(2)}) async-start(bf16[16,128,256]{2,1,0:T(8,128)(2,1)} %broadcast_in_dim.6), calls=%async_computation | async-start | bytes 2097152 | tf_op jit(solution)/shard_map/all_to_all | solution.py:15
  10.4 0.0 copy-done.5
  10.4 0.0 copy-start.4
  10.4 7.9 %collective-permute-start = (bf16[128,256]{1,0:T(8,128)(2,1)S(1)}, bf16[128,256]{1,0:T(8,128)(2,1)S(1)}, u32[]{:S(2)}, u32[]{:S(2)}) collective-permute-start(bf16[128,256]{1,0:T(8,128)(2,1)S(1)} %copy-done.5), channel_id=1, source_target_pairs={{0,0},{1,256},{256,257},{257,1},{2,2},{3,258},{258,259},{259,3},{4... | collective-permute-start | bytes 196616 | tf_op jit(solution)/shard_map/ppermute | solution.py:42
  18.3 4.6 %collective-permute-done = bf16[128,256]{1,0:T(8,128)(2,1)S(1)} collective-permute-done((bf16[128,256]{1,0:T(8,128)(2,1)S(1)}, bf16[128,256]{1,0:T(8,128)(2,1)S(1)}, u32[]{:S(2)}, u32[]{:S(2)}) %collective-permute-start) | collective-permute-done | bytes 65568 | tf_op jit(solution)/shard_map/ppermute | solution.py:42
  23.0 1.9 %all-to-all-done = bf16[16,128,256]{2,1,0:T(8,128)(2,1)S(1)} async-done(((bf16[16,128,256]{2,1,0:T(8,128)(2,1)}), bf16[16,128,256]{2,1,0:T(8,128)(2,1)S(1)}, u32[]{:S(2)}, u32[]{:S(2)}) %all-to-all-start) | async-done | bytes 1048608 | tf_op jit(solution)/shard_map/all_to_all | solution.py:15
  24.9 0.0 copy-start.2
  24.9 1.2 broadcast_in_dim.7
  26.1 0.2 copy-done.2
  26.2 4.7 %all-to-all-start.1 = ((bf16[16,128,256]{2,1,0:T(8,128)(2,1)}), bf16[16,128,256]{2,1,0:T(8,128)(2,1)S(1)}, u32[]{:S(2)}, u32[]{:S(2)}) async-start(bf16[16,128,256]{2,1,0:T(8,128)(2,1)} %broadcast_in_dim.7), calls=%async_computation.1 | async-start | bytes 2097152 | tf_op jit(solution)/shard_map/all_to_all | solution.py:15
  31.0 0.0 copy-done
  31.0 0.0 copy-done.4
  31.0 0.0 copy-start.3
  31.0 0.7 convolution_convert_fusion.1
  31.8 0.5 copy-done.3
  32.2 0.0 copy-start.1
  32.2 0.6 fusion
  32.8 5.2 %collective-permute-start.1 = (bf16[384,256]{1,0:T(8,128)(2,1)S(1)}, bf16[384,256]{1,0:T(8,128)(2,1)S(1)}, u32[]{:S(2)}, u32[]{:S(2)}) collective-permute-start(bf16[384,256]{1,0:T(8,128)(2,1)S(1)} %fusion), channel_id=1, source_target_pairs={{0,1},{1,0},{2,3},{3,2},{4,5},{5,4},{6,7},{7,6},{8,9},{9,8},{10,11... | collective-permute-start | bytes 589832 | tf_op jit(solution)/shard_map/ppermute | solution.py:24
  38.0 0.0 copy-done.1
  38.0 0.7 convolution_convert_fusion
  38.7 1.9 %bitcast_bitcast_fusion = bf16[16,512,128]{2,1,0:T(8,128)(2,1)} fusion(bf16[256,2048]{1,0:T(8,128)(2,1)S(1)} %convolution_convert_fusion, bf16[256,2048]{1,0:T(8,128)(2,1)S(1)} %convolution_convert_fusion.1), kind=kLoop, calls=%fused_computation.3 | loop fusion | flops 4194304 | bytes 4194304 | tf_op jit(solution)/shard_map/transpose | solution.py:53
  40.6 4.4 %all-to-all-done.1 = bf16[16,128,256]{2,1,0:T(8,128)(2,1)S(1)} async-done(((bf16[16,128,256]{2,1,0:T(8,128)(2,1)}), bf16[16,128,256]{2,1,0:T(8,128)(2,1)S(1)}, u32[]{:S(2)}, u32[]{:S(2)}) %all-to-all-start.1) | async-done | bytes 1048608 | tf_op jit(solution)/shard_map/all_to_all | solution.py:15
  45.0 4.4 %all-to-all-start.2 = ((bf16[16,512,128]{2,1,0:T(8,128)(2,1)}), bf16[16,512,128]{2,1,0:T(8,128)(2,1)}, u32[]{:S(2)}, u32[]{:S(2)}) async-start(bf16[16,512,128]{2,1,0:T(8,128)(2,1)} %bitcast_bitcast_fusion), calls=%async_computation.2 | async-start | bytes 4194304 | tf_op jit(solution)/shard_map/all_to_all | solution.py:15
  49.5 0.1 fusion.3
  49.6 0.0 collective-permute-done.1
  49.6 0.4 fusion.4
  50.0 0.4 convolution_add_fusion
  50.4 70.5 %all-reduce.1 = bf16[384,1024]{1,0:T(8,128)(2,1)} all-reduce(f32[384,1024]{1,0:T(8,128)S(1)} %convolution_add_fusion), channel_id=1, replica_groups=mesh['yh'=2,'yl'=2,'x'=4,'zh'=4,'zl'=4,'core'=2] {'zh','zl'}, use_global_device_ids=true, to_apply=%region_0.0 | all-reduce | flops 393216 | bytes 2359296 | tf_op jit(solution)/shard_map/psum | solution.py:58
  120.9 14.1 %collective-permute-start.2 = (bf16[384,1024]{1,0:T(8,128)(2,1)}, bf16[384,1024]{1,0:T(8,128)(2,1)}, u32[]{:S(2)}, u32[]{:S(2)}) collective-permute-start(bf16[384,1024]{1,0:T(8,128)(2,1)} %all-reduce.1), channel_id=1, source_target_pairs={{0,1},{1,0},{2,3},{3,2},{4,5},{5,4},{6,7},{7,6},{8,9},{9,8},{10,11... | collective-permute-start | bytes 2359304 | tf_op jit(solution)/shard_map/ppermute | solution.py:24
  135.1 2.2 %collective-permute-done.2 = bf16[384,1024]{1,0:T(8,128)(2,1)} collective-permute-done((bf16[384,1024]{1,0:T(8,128)(2,1)}, bf16[384,1024]{1,0:T(8,128)(2,1)}, u32[]{:S(2)}, u32[]{:S(2)}) %collective-permute-start.2) | collective-permute-done | bytes 786464 | tf_op jit(solution)/shard_map/ppermute | solution.py:24
  137.3 1.5 broadcast_select_fusion.1
  138.8 0.0 all-to-all-done.2
  138.8 1.9 %convert_reduce_fusion = f32[512,128]{1,0:T(8,128)S(1)} fusion(bf16[16,512,128]{2,1,0:T(8,128)(2,1)} %all-to-all-done.2), kind=kLoop, calls=%fused_computation | loop fusion | flops 2031616 | bytes 2359296 | tf_op jit(solution)/shard_map/reduce_sum | solution.py:55
  140.7 0.7 multiply_reduce_fusion
  141.4 0.6 broadcast_in_dim.8
  142.0 7.4 %all-to-all-start.3 = ((f32[32,1,128]{2,1,0:T(1,128)}), f32[32,1,128]{2,1,0:T(1,128)S(1)}, u32[]{:S(2)}, u32[]{:S(2)}) async-start(f32[32,1,128]{2,1,0:T(1,128)} %broadcast_in_dim.8), calls=%async_computation.3 | async-start | bytes 32768 | tf_op jit(solution)/shard_map/all_to_all | solution.py:15
  149.3 1.3 pad_maximum_fusion
  150.6 0.8 copy.21
  151.4 10.5 %psum.22 = f32[256]{0:T(256)S(1)} all-reduce(f32[256]{0:T(256)S(1)} %get-tuple-element.25), channel_id=1, replica_groups=mesh['yh'=2,'yl'=2,'x'=4,'zh'=4,'zl'=4,'core'=2] {'yh','yl'}, use_global_device_ids=true, to_apply=%region_5.0 | all-reduce | flops 256 | bytes 2048 | tf_op jit(solution)/shard_map/psum | solution.py:60
  161.8 9.5 %psum.23 = f32[256]{0:T(256)} all-reduce(f32[256]{0:T(256)S(1)} %psum.22), channel_id=1, replica_groups=mesh['yh'=2,'yl'=2,'x'=4,'zh'=4,'zl'=4,'core'=2] {'x'}, use_global_device_ids=true, to_apply=%region_6.7 | all-reduce | flops 256 | bytes 2048 | tf_op jit(solution)/shard_map/psum | solution.py:61
  171.3 0.0 all-to-all-done.3
  171.3 0.5 reduce_sum.38
Async XLA Ops:
  0.6 30.4 %copy-start = (bf16[384,2048]{1,0:T(8,128)(2,1)S(1)}, bf16[384,2048]{1,0:T(8,128)(2,1)}, u32[]{:S(2)}) copy-start(bf16[384,2048]{1,0:T(8,128)(2,1)} %param.7) | copy-start | bytes 4718596
  1.7 8.7 %copy-start.5 = (bf16[128,256]{1,0:T(8,128)(2,1)S(1)}, bf16[128,256]{1,0:T(8,128)(2,1)}, u32[]{:S(2)}) copy-start(bf16[128,256]{1,0:T(8,128)(2,1)} %param.8) | copy-start | bytes 196612
  2.8 22.1 %all-to-all-start = ((bf16[16,128,256]{2,1,0:T(8,128)(2,1)}), bf16[16,128,256]{2,1,0:T(8,128)(2,1)S(1)}, u32[]{:S(2)}, u32[]{:S(2)}) async-start(bf16[16,128,256]{2,1,0:T(8,128)(2,1)} %broadcast_in_dim.6), calls=%async_computation | async-start | bytes 2097152 | tf_op jit(solution)/shard_map/all_to_all | solution.py:15
  10.4 20.6 %copy-start.4 = (bf16[384,256]{1,0:T(8,128)(2,1)S(1)}, bf16[384,256]{1,0:T(8,128)(2,1)}, u32[]{:S(2)}) copy-start(bf16[384,256]{1,0:T(8,128)(2,1)} %param.6) | copy-start | bytes 589828
  10.4 12.6 %collective-permute-start = (bf16[128,256]{1,0:T(8,128)(2,1)S(1)}, bf16[128,256]{1,0:T(8,128)(2,1)S(1)}, u32[]{:S(2)}, u32[]{:S(2)}) collective-permute-start(bf16[128,256]{1,0:T(8,128)(2,1)S(1)} %copy-done.5), channel_id=1, source_target_pairs={{0,0},{1,256},{256,257},{257,1},{2,2},{3,258},{258,259},{259,3},{4... | collective-permute-start | bytes 196616 | tf_op jit(solution)/shard_map/ppermute | solution.py:42
  24.9 1.3 copy-start.2
  26.2 18.8 %all-to-all-start.1 = ((bf16[16,128,256]{2,1,0:T(8,128)(2,1)}), bf16[16,128,256]{2,1,0:T(8,128)(2,1)S(1)}, u32[]{:S(2)}, u32[]{:S(2)}) async-start(bf16[16,128,256]{2,1,0:T(8,128)(2,1)} %broadcast_in_dim.7), calls=%async_computation.1 | async-start | bytes 2097152 | tf_op jit(solution)/shard_map/all_to_all | solution.py:15
  31.0 1.2 copy-start.3
  32.2 5.8 %copy-start.1 = (bf16[384,2048]{1,0:T(8,128)(2,1)S(1)}, bf16[384,2048]{1,0:T(8,128)(2,1)}, u32[]{:S(2)}) copy-start(bf16[384,2048]{1,0:T(8,128)(2,1)} %param.5) | copy-start | bytes 4718596
  32.8 16.8 %collective-permute-start.1 = (bf16[384,256]{1,0:T(8,128)(2,1)S(1)}, bf16[384,256]{1,0:T(8,128)(2,1)S(1)}, u32[]{:S(2)}, u32[]{:S(2)}) collective-permute-start(bf16[384,256]{1,0:T(8,128)(2,1)S(1)} %fusion), channel_id=1, source_target_pairs={{0,1},{1,0},{2,3},{3,2},{4,5},{5,4},{6,7},{7,6},{8,9},{9,8},{10,11... | collective-permute-start | bytes 589832 | tf_op jit(solution)/shard_map/ppermute | solution.py:24
  45.0 93.7 %all-to-all-start.2 = ((bf16[16,512,128]{2,1,0:T(8,128)(2,1)}), bf16[16,512,128]{2,1,0:T(8,128)(2,1)}, u32[]{:S(2)}, u32[]{:S(2)}) async-start(bf16[16,512,128]{2,1,0:T(8,128)(2,1)} %bitcast_bitcast_fusion), calls=%async_computation.2 | async-start | bytes 4194304 | tf_op jit(solution)/shard_map/all_to_all | solution.py:15
  120.9 16.4 %collective-permute-start.2 = (bf16[384,1024]{1,0:T(8,128)(2,1)}, bf16[384,1024]{1,0:T(8,128)(2,1)}, u32[]{:S(2)}, u32[]{:S(2)}) collective-permute-start(bf16[384,1024]{1,0:T(8,128)(2,1)} %all-reduce.1), channel_id=1, source_target_pairs={{0,1},{1,0},{2,3},{3,2},{4,5},{5,4},{6,7},{7,6},{8,9},{9,8},{10,11... | collective-permute-start | bytes 2359304 | tf_op jit(solution)/shard_map/ppermute | solution.py:24
  142.0 29.4 %all-to-all-start.3 = ((f32[32,1,128]{2,1,0:T(1,128)}), f32[32,1,128]{2,1,0:T(1,128)S(1)}, u32[]{:S(2)}, u32[]{:S(2)}) async-start(f32[32,1,128]{2,1,0:T(1,128)} %broadcast_in_dim.8), calls=%async_computation.3 | async-start | bytes 32768 | tf_op jit(solution)/shard_map/all_to_all | solution.py:15

commit v7 on v4

v7 whole, which is shorter than its diff:
```python
import jax
import jax.numpy as jnp
from jax import lax
from jax.sharding import Mesh
from jax.sharding import PartitionSpec as P


FS = ("yh", "yl", "x")
TP = ("zh", "zl", "core")
BF = jnp.bfloat16
F32 = jnp.float32


def exchange(array, axes):
    return lax.all_to_all(array, axes, 0, 0, tiled=True)


def from_everyone(array, axes):
    count = lax.axis_size(axes)
    return exchange(jnp.broadcast_to(array[None], (count, *array.shape)), axes)


def other_core(array):
    return lax.ppermute(array, "core", [(0, 1), (1, 0)])


def dot(left, right, over):
    return lax.dot_general(
        left, right, ((over[:1], over[1:]), ((), ())), preferred_element_type=F32
    )


def both_ways(block, part):
    many = lax.axis_size(FS)
    rows, columns = block.shape
    parts = jnp.moveaxis(part.reshape(rows, many, columns), 1, 0)
    blocks = jnp.broadcast_to(block[None], parts.shape)
    got = exchange(jnp.concatenate([blocks, parts], axis=1), FS)
    return got[:, :rows], jnp.sum(got[:, rows:].astype(F32), axis=0)


def local(inputs, pre_act, cotangent, up_weight, down_weight):
    _, width = inputs.shape
    hidden = pre_act.shape[1]
    many = lax.axis_size(FS)
    core = lax.axis_index("core")
    active = jnp.maximum(pre_act.astype(F32), 0.0)
    squared = (active * active).astype(BF)

    down_part = dot(squared, cotangent, (0, 0)).astype(BF)
    down_columns, down_grad = both_ways(down_weight, down_part)
    down_columns = jnp.moveaxis(down_columns, 0, 1).reshape(hidden, width)
    sq_grad = dot(cotangent, down_columns, (1, 1))
    pre_grad = (2.0 * active * sq_grad).astype(BF)

    rows = lax.ppermute(up_weight.T, ("yh", "core"), [(0, 0), (1, 2), (2, 3), (3, 1)])
    up_part = dot(pre_grad, inputs, (0, 0)).astype(BF)
    up_rows, up_grad = both_ways(rows, up_part)
    theirs = other_core(pre_grad)
    up_rows = up_rows.reshape(2, many // 2, hidden, width // many)
    up_rows = jnp.moveaxis(up_rows, 1, 2).reshape(2, hidden, width // 2)
    half = dot(pre_grad, up_rows[0], (1, 0)) + dot(theirs, up_rows[1], (1, 0))

    down_norms = from_everyone(jnp.sum(down_grad * down_grad, axis=1), FS)
    down_norms = jnp.sum(down_norms, axis=0)
    half, up_norms = lax.psum((half, jnp.sum(up_grad * up_grad, axis=0)), ("zh", "zl"))
    half = half.astype(BF)
    up_norms += other_core(up_norms)
    both = other_core(half)
    input_grad = jnp.concatenate(
        [jnp.where(core == 0, half, both), jnp.where(core == 0, both, half)], axis=1
    )
    return input_grad, up_grad.T, down_grad, up_norms, down_norms


def solution(mesh):
    split = Mesh(mesh.devices.reshape(2, 2, 4, 4, 4, 2), (*FS, *TP))
    return jax.shard_map(
        local,
        mesh=split,
        in_specs=(P(FS, None), P(FS, TP), P(FS, None), P(FS, TP), P(TP, FS)),
        out_specs=(P(FS, None), P(FS, TP), P(TP, FS), P(FS), P(TP)),
        check_vma=False,
    )
```

time: 175 us -> 190 us (1.086)
  waiting for transfers between devices: 23.2 us -> 40.6 us
  starting transfers between devices: 60.6 us -> 52.1 us
  local copies, waits for them, and re-layouts: 6.02 us -> 10.4 us
  blocking collectives: 70.5 us -> 72.4 us
    all_to_all x5 -> x3, starting transfers between devices: 33.2 us -> 19.5 us  [exchange(): return lax.all_to_all(array, axes, 0, 0, tiled=True)]
    ppermute x1, waiting for transfers between devices: 4.65 us -> 15.1 us  [local(): lax.ppermute(up_weight.T, ('yh', 'core'), [(0, 0), (1, 2), (2, 3), (3, 1)])]
    all_to_all x5 -> x3, waiting for transfers between devices: 18.6 us -> 25.5 us  [exchange(): return lax.all_to_all(array, axes, 0, 0, tiled=True)]
    slice x1 -> x4, local copies, waits for them, and re-layouts: 0.09 us -> 5.16 us  [the longest x3 5.07 us: both_ways(): return (got[:, :rows], jnp.sum(got[:, rows:].astype(F32), axis=0))]
    ppermute x2 -> x3, starting transfers between devices: 19.4 us -> 24.1 us  [other_core(): return lax.ppermute(array, 'core', [(0, 1), (1, 0)])]
    concatenate x0 -> x2, other arithmetic: none -> 2.95 us  [both_ways(): got = exchange(jnp.concatenate([blocks, parts], axis=1), FS)]
    broadcast_in_dim x4 -> x1, local copies, waits for them, and re-layouts: 3.46 us -> 0.62 us  [from_everyone(): return exchange(jnp.broadcast_to(array[None], (count, *array.shape)), axes)]
    unnamed x15, local copies, waits for them, and re-layouts: 1.41 us -> 3.59 us
  transfers between devices with their start and end apart: 8 -> 7, of which waited for: 5 -> 4; matrix products, arithmetic and copies ran while one was open for 8% -> 5% of each run, Pallas kernels for 0% -> 0%
where the time goes in v7:
time: 190 us; the launch traced here: 189 us
  blocking collectives  72.4 us (38%)
  starting transfers between devices  52.1 us (27%)
  waiting for transfers between devices  40.6 us (21%)
  local copies, waits for them, and re-layouts  10.4 us (5%)
  other arithmetic  8.34 us (4%)
  matrix products  4.37 us (2%)
    psum x1, blocking collectives, local(): lax.psum((half, jnp.sum(up_grad * up_grad, axis=0)), ('zh', 'zl'))  72.4 us
    all_to_all x3, waiting for transfers between devices, exchange(): return lax.all_to_all(array, axes, 0, 0, tiled=True)  25.5 us
    ppermute x3, starting transfers between devices, other_core(): return lax.ppermute(array, 'core', [(0, 1), (1, 0)])  24.1 us
    all_to_all x3, starting transfers between devices, exchange(): return lax.all_to_all(array, axes, 0, 0, tiled=True)  19.5 us
    ppermute x1, waiting for transfers between devices, local(): lax.ppermute(up_weight.T, ('yh', 'core'), [(0, 0), (1, 2), (2, 3), (3, 1)])  15.1 us
    ppermute x1, starting transfers between devices, local(): lax.ppermute(up_weight.T, ('yh', 'core'), [(0, 0), (1, 2), (2, 3), (3, 1)])  8.44 us
    slice x3, local copies, waits for them, and re-layouts, both_ways(): return (got[:, :rows], jnp.sum(got[:, rows:].astype(F32), axis=0))  5.07 us
    dot_general x5, matrix products, dot(): lax.dot_general(left, right, ((over[:1], over[1:]), ((), ())), preferred_...  4.37 us
  transfers between devices with their start and end apart: 7, of which 4 were waited for; matrix products, arithmetic and copies ran while one was open for 5% of the time, Pallas kernels for 0%

profile of v7, /device:TPU:1, one launch (start us, length us, event | category | flops | bytes accessed | tf_op | source)
XLA Modules:
  0.0 189.0 jit_solution(7544436052553210312)
XLA Ops:
  0.6 0.0 copy-start
  0.6 1.2 copy.34
  1.9 0.3 copy-done
  2.1 0.0 copy-start.4
  2.1 0.7 fusion
  2.9 0.3 copy.51
  3.1 0.0 copy-done.4
  3.1 0.2 broadcast_in_dim.6
  3.4 1.5 pad_maximum_fusion
  4.8 0.0 copy-start.5
  4.8 7.8 %all-to-all-start = ((bf16[16,512,128]{2,1,0:T(8,128)(2,1)}), bf16[16,512,128]{2,1,0:T(8,128)(2,1)}, u32[]{:S(2)}, u32[]{:S(2)}) async-start(bf16[16,512,128]{2,1,0:T(8,128)(2,1)} %pad_maximum_fusion), calls=%async_computation | async-start | bytes 4194304 | tf_op jit(solution)/shard_map/all_to_all | solution.py:15
  12.6 0.0 copy-done.5
  12.6 8.4 %collective-permute-start = (bf16[256,128]{0,1:T(8,128)(2,1)S(1)}, bf16[256,128]{0,1:T(8,128)(2,1)S(1)}, u32[]{:S(2)}, u32[]{:S(2)}) collective-permute-start(bf16[256,128]{0,1:T(8,128)(2,1)S(1)} %bitcast.48), channel_id=1, source_target_pairs={{0,0},{1,256},{256,257},{257,1},{2,2},{3,258},{258,259},{259,3},{4... | collective-permute-start | bytes 196616 | tf_op jit(solution)/shard_map/ppermute | solution.py:56
  21.0 15.1 %collective-permute-done = bf16[256,128]{0,1:T(8,128)(2,1)S(1)} collective-permute-done((bf16[256,128]{0,1:T(8,128)(2,1)S(1)}, bf16[256,128]{0,1:T(8,128)(2,1)S(1)}, u32[]{:S(2)}, u32[]{:S(2)}) %collective-permute-start) | collective-permute-done | bytes 65568 | tf_op jit(solution)/shard_map/ppermute | solution.py:56
  36.1 0.1 copy.37
  36.2 1.1 all-to-all-done
  37.4 1.3 slice.26
  38.7 1.3 copy.45
  40.0 0.0 copy-start.1
  40.0 2.1 %fusion.3 = bf16[384,256]{0,1:T(8,128)(2,1)S(1)} fusion(bf16[256,2048]{0,1:T(8,128)(2,1)} %bitcast.47, bf16[384,2048]{1,0:T(8,128)(2,1)S(1)} %copy-done, bf16[384,256]{0,1:T(8,128)(2,1)S(1)} %copy.34), kind=kOutput, calls=%fused_computation.12 | convolution fusion | flops 403144704 | bytes 3014656 | tf_op jit(solution)/shard_map/dot_general | solution.py:28
  42.1 0.0 copy-done.1
  42.1 0.7 fusion.1
  42.8 0.3 copy.50
  43.1 0.2 broadcast_in_dim.7
  43.3 1.5 pad_maximum_fusion.1
  44.8 7.6 %all-to-all-start.1 = ((bf16[16,512,128]{2,1,0:T(8,128)(2,1)}), bf16[16,512,128]{2,1,0:T(8,128)(2,1)}, u32[]{:S(2)}, u32[]{:S(2)}) async-start(bf16[16,512,128]{2,1,0:T(8,128)(2,1)} %pad_maximum_fusion.1), calls=%async_computation.1 | async-start | bytes 4194304 | tf_op jit(solution)/shard_map/all_to_all | solution.py:15
  52.4 5.0 %collective-permute-start.1 = (bf16[384,256]{0,1:T(8,128)(2,1)S(1)}, bf16[384,256]{0,1:T(8,128)(2,1)S(1)}, u32[]{:S(2)}, u32[]{:S(2)}) collective-permute-start(bf16[384,256]{0,1:T(8,128)(2,1)S(1)} %fusion.3), channel_id=1, source_target_pairs={{0,1},{1,0},{2,3},{3,2},{4,5},{5,4},{6,7},{7,6},{8,9},{9,8},{10,11... | collective-permute-start | bytes 589832 | tf_op jit(solution)/shard_map/ppermute | solution.py:24
  57.4 20.2 %all-to-all-done.1 = bf16[16,512,128]{2,1,0:T(8,128)(2,1)} async-done(((bf16[16,512,128]{2,1,0:T(8,128)(2,1)}), bf16[16,512,128]{2,1,0:T(8,128)(2,1)}, u32[]{:S(2)}, u32[]{:S(2)}) %all-to-all-start.1) | async-done | bytes 2097184 | tf_op jit(solution)/shard_map/all_to_all | solution.py:15
  77.6 2.3 %slice.27 = bf16[16,256,128]{2,1,0:T(8,128)(2,1)} slice(bf16[16,512,128]{2,1,0:T(8,128)(2,1)} %all-to-all-done.1), slice={[0:16], [0:256], [0:128]} | slice | bytes 2097152 | tf_op jit(solution)/shard_map/slice | solution.py:39
  79.9 1.5 copy.39
  81.4 0.1 fusion.6
  81.5 0.4 fusion.7
  81.9 1.4 convert_reduce_fusion.1
  83.3 0.0 collective-permute-done.1
  83.3 0.4 convolution_add_fusion
  83.7 72.4 %all-reduce.2 = (bf16[384,1024]{1,0:T(8,128)(2,1)}, f32[128]{0:T(128)S(1)}) all-reduce(f32[384,1024]{1,0:T(8,128)S(1)} %convolution_add_fusion, f32[128]{0:T(128)S(1)} %multiply_reduce_fusion.1), channel_id=1, replica_groups=mesh['yh'=2,'yl'=2,'x'=4,'zh'=4,'zl'=4,'core'=2] {'zh','zl'}, use_global_device_ids=true, to_apply=%region_0.0 | all-reduce | flops 393344 | bytes 2360320 | tf_op jit(solution)/shard_map/psum | solution.py:66
  156.1 0.0 copy-start.2
  156.1 16.9 %collective-permute-start.2 = (bf16[384,1024]{1,0:T(8,128)(2,1)}, bf16[384,1024]{1,0:T(8,128)(2,1)S(1)}, u32[]{:S(2)}, u32[]{:S(2)}) collective-permute-start(bf16[384,1024]{1,0:T(8,128)(2,1)} %get-tuple-element.25), channel_id=1, source_target_pairs={{0,1},{1,0},{2,3},{3,2},{4,5},{5,4},{6,7},{7,6},{8,9},{9,8},{10,11... | collective-permute-start | bytes 2359304 | tf_op jit(solution)/shard_map/ppermute | solution.py:24
  173.0 1.4 convert_reduce_fusion
  174.4 0.0 copy-start.3
  174.4 0.1 multiply_reduce_fusion
  174.5 0.6 broadcast_in_dim.8
  175.2 4.2 %all-to-all-start.2 = ((f32[16,1,256]{2,1,0:T(1,128)}), f32[16,1,256]{2,1,0:T(1,128)S(1)}, u32[]{:S(2)}, u32[]{:S(2)}) async-start(f32[16,1,256]{2,1,0:T(1,128)} %broadcast_in_dim.8), calls=%async_computation.2 | async-start | bytes 32768 | tf_op jit(solution)/shard_map/all_to_all | solution.py:15
  179.3 2.2 %collective-permute-start.3 = (f32[128]{0:T(128)S(1)}, f32[128]{0:T(128)S(1)}, u32[]{:S(2)}, u32[]{:S(2)}) collective-permute-start(f32[128]{0:T(128)S(1)} %get-tuple-element.26), channel_id=1, source_target_pairs={{0,1},{1,0},{2,3},{3,2},{4,5},{5,4},{6,7},{7,6},{8,9},{9,8},{10,11... | collective-permute-start | bytes 1544 | tf_op jit(solution)/shard_map/ppermute | solution.py:24
  181.6 4.2 %all-to-all-done.2 = f32[16,1,256]{2,1,0:T(1,128)S(1)} async-done(((f32[16,1,256]{2,1,0:T(1,128)}), f32[16,1,256]{2,1,0:T(1,128)S(1)}, u32[]{:S(2)}, u32[]{:S(2)}) %all-to-all-start.2) | async-done | bytes 16416 | tf_op jit(solution)/shard_map/all_to_all | solution.py:15
  185.8 0.6 reduce_sum.49
  186.4 0.8 copy.42
  187.1 0.0 collective-permute-done.3
  187.1 0.5 add.11
  187.7 0.0 collective-permute-done.2
  187.7 0.0 copy-done.2
  187.7 0.1 broadcast_select_fusion.1
  187.8 1.2 pad_maximum_fusion.2
  189.0 0.0 copy-done.3
  (1 shorter events, 0.0 us)
Async XLA Ops:
  0.6 1.5 copy-start
  2.1 1.0 copy-start.4
  4.8 7.8 %copy-start.5 = (bf16[128,256]{1,0:T(8,128)(2,1)S(1)}, bf16[128,256]{1,0:T(8,128)(2,1)}, u32[]{:S(2)}) copy-start(bf16[128,256]{1,0:T(8,128)(2,1)} %param.8) | copy-start | bytes 196612
  4.8 32.5 %all-to-all-start = ((bf16[16,512,128]{2,1,0:T(8,128)(2,1)}), bf16[16,512,128]{2,1,0:T(8,128)(2,1)}, u32[]{:S(2)}, u32[]{:S(2)}) async-start(bf16[16,512,128]{2,1,0:T(8,128)(2,1)} %pad_maximum_fusion), calls=%async_computation | async-start | bytes 4194304 | tf_op jit(solution)/shard_map/all_to_all | solution.py:15
  12.6 23.5 %collective-permute-start = (bf16[256,128]{0,1:T(8,128)(2,1)S(1)}, bf16[256,128]{0,1:T(8,128)(2,1)S(1)}, u32[]{:S(2)}, u32[]{:S(2)}) collective-permute-start(bf16[256,128]{0,1:T(8,128)(2,1)S(1)} %bitcast.48), channel_id=1, source_target_pairs={{0,0},{1,256},{256,257},{257,1},{2,2},{3,258},{258,259},{259,3},{4... | collective-permute-start | bytes 196616 | tf_op jit(solution)/shard_map/ppermute | solution.py:56
  40.0 2.1 %copy-start.1 = (bf16[384,2048]{1,0:T(8,128)(2,1)S(1)}, bf16[384,2048]{1,0:T(8,128)(2,1)}, u32[]{:S(2)}) copy-start(bf16[384,2048]{1,0:T(8,128)(2,1)} %param.5) | copy-start | bytes 4718596
  44.8 32.8 %all-to-all-start.1 = ((bf16[16,512,128]{2,1,0:T(8,128)(2,1)}), bf16[16,512,128]{2,1,0:T(8,128)(2,1)}, u32[]{:S(2)}, u32[]{:S(2)}) async-start(bf16[16,512,128]{2,1,0:T(8,128)(2,1)} %pad_maximum_fusion.1), calls=%async_computation.1 | async-start | bytes 4194304 | tf_op jit(solution)/shard_map/all_to_all | solution.py:15
  52.4 31.0 %collective-permute-start.1 = (bf16[384,256]{0,1:T(8,128)(2,1)S(1)}, bf16[384,256]{0,1:T(8,128)(2,1)S(1)}, u32[]{:S(2)}, u32[]{:S(2)}) collective-permute-start(bf16[384,256]{0,1:T(8,128)(2,1)S(1)} %fusion.3), channel_id=1, source_target_pairs={{0,1},{1,0},{2,3},{3,2},{4,5},{5,4},{6,7},{7,6},{8,9},{9,8},{10,11... | collective-permute-start | bytes 589832 | tf_op jit(solution)/shard_map/ppermute | solution.py:24
  156.1 31.6 %copy-start.2 = (bf16[384,1024]{1,0:T(8,128)(2,1)S(1)}, bf16[384,1024]{1,0:T(8,128)(2,1)}, u32[]{:S(2)}) copy-start(bf16[384,1024]{1,0:T(8,128)(2,1)} %get-tuple-element.25) | copy-start | bytes 2359300
  156.1 31.5 %collective-permute-start.2 = (bf16[384,1024]{1,0:T(8,128)(2,1)}, bf16[384,1024]{1,0:T(8,128)(2,1)S(1)}, u32[]{:S(2)}, u32[]{:S(2)}) collective-permute-start(bf16[384,1024]{1,0:T(8,128)(2,1)} %get-tuple-element.25), channel_id=1, source_target_pairs={{0,1},{1,0},{2,3},{3,2},{4,5},{5,4},{6,7},{7,6},{8,9},{9,8},{10,11... | collective-permute-start | bytes 2359304 | tf_op jit(solution)/shard_map/ppermute | solution.py:24
  174.4 14.6 %copy-start.3 = (f32[256,128]{1,0:T(8,128)}, f32[256,128]{1,0:T(8,128)S(1)}, u32[]{:S(2)}) copy-start(f32[256,128]{1,0:T(8,128)S(1)} %convert_reduce_fusion) | copy-start | bytes 393220
  175.2 10.6 %all-to-all-start.2 = ((f32[16,1,256]{2,1,0:T(1,128)}), f32[16,1,256]{2,1,0:T(1,128)S(1)}, u32[]{:S(2)}, u32[]{:S(2)}) async-start(f32[16,1,256]{2,1,0:T(1,128)} %broadcast_in_dim.8), calls=%async_computation.2 | async-start | bytes 32768 | tf_op jit(solution)/shard_map/all_to_all | solution.py:15
  179.3 7.8 %collective-permute-start.3 = (f32[128]{0:T(128)S(1)}, f32[128]{0:T(128)S(1)}, u32[]{:S(2)}, u32[]{:S(2)}) collective-permute-start(f32[128]{0:T(128)S(1)} %get-tuple-element.26), channel_id=1, source_target_pairs={{0,1},{1,0},{2,3},{3,2},{4,5},{5,4},{6,7},{7,6},{8,9},{9,8},{10,11... | collective-permute-start | bytes 1544 | tf_op jit(solution)/shard_map/ppermute | solution.py:24

commit v8 on v3

--- a/solution.py
+++ b/solution.py
@@ -44,7 +44,7 @@
 
 
 def local(inputs, pre_act, cotangent, up_weight, down_weight):
-    tokens, width = inputs.shape
+    _, width = inputs.shape
     hidden = pre_act.shape[1]
     many = lax.axis_size(FS)
     core = lax.axis_index("core")
@@ -69,11 +69,9 @@
     down_grad, up_grad = grads[:hidden], grads[hidden:]
 
     half = sum_near(half, "zl")
-    pieces = exchange(half.reshape(4, tokens // 16, width // 2), "zh")
-    half = jnp.sum(pieces.astype(F32), axis=0).astype(BF)
-
     up_norms = from_everyone(jnp.sum(up_grad * up_grad, axis=0), TP)
-    half = lax.all_gather(half, "zh", axis=0, tiled=True)
+    groups = lax.all_gather(half, "zh", axis=0, tiled=False)
+    half = jnp.sum(groups.astype(F32), axis=0).astype(BF)
     down_norms = from_everyone(jnp.sum(down_grad * down_grad, axis=1), FS)
     half = lax.all_gather(half, "zl", axis=0, tiled=True)
     both = other_core(half)

time: 185 us -> 177 us (0.957)
  blocking collectives: 35.6 us -> 59.6 us
  starting transfers between devices: 82.4 us -> 64.2 us
  waiting for transfers between devices: 42.6 us -> 32 us
  matrix products: 4.98 us -> 2.83 us
    all_to_all x6 -> x5, starting transfers between devices: 47.4 us -> 32.3 us  [exchange(): return lax.all_to_all(array, axes, 0, 0, tiled=True)]
    all_gather x1, blocking collectives: 15.9 us -> 28.2 us  [local(): groups = lax.all_gather(half, 'zh', axis=0, tiled=False)]
    all_gather x1, blocking collectives: 19.7 us -> 31.4 us  [local(): half = lax.all_gather(half, 'zl', axis=0, tiled=True)]
    all_to_all x6 -> x5, waiting for transfers between devices: 29.6 us -> 18.9 us  [exchange(): return lax.all_to_all(array, axes, 0, 0, tiled=True)]
    ppermute x2, starting transfers between devices: 14 us -> 10.5 us  [other_core(): return lax.ppermute(array, 'core', [(0, 1), (1, 0)])]
    dot_general x5, matrix products: 4.98 us -> 2.83 us  [dot(): lax.dot_general(left, right, ((over[:1], over[1:]), ((), ())), preferred_...]
  transfers between devices with their start and end apart: 12 -> 11, of which waited for: 7 -> 6; matrix products, arithmetic and copies ran while one was open for 8% -> 8% of each run, Pallas kernels for 0% -> 0%
where the time goes in v8:
time: 177 us; the launch traced here: 176 us
  starting transfers between devices  64.2 us (36%)
  blocking collectives  59.6 us (34%)
  waiting for transfers between devices  32 us (18%)
  other arithmetic  10.4 us (6%)
  local copies, waits for them, and re-layouts  6.07 us (3%)
  matrix products  2.83 us (2%)
    all_to_all x5, starting transfers between devices, exchange(): return lax.all_to_all(array, axes, 0, 0, tiled=True)  32.3 us
    all_gather x1, blocking collectives, local(): half = lax.all_gather(half, 'zl', axis=0, tiled=True)  31.4 us
    all_gather x1, blocking collectives, local(): groups = lax.all_gather(half, 'zh', axis=0, tiled=False)  28.2 us
    all_to_all x5, waiting for transfers between devices, exchange(): return lax.all_to_all(array, axes, 0, 0, tiled=True)  18.9 us
    ppermute x3, starting transfers between devices, sum_near(): total += lax.ppermute(piece, axis, ring).astype(F32)  13.6 us
    ppermute x2, starting transfers between devices, other_core(): return lax.ppermute(array, 'core', [(0, 1), (1, 0)])  10.5 us
    ppermute x3, waiting for transfers between devices, sum_near(): total += lax.ppermute(piece, axis, ring).astype(F32)  8.42 us
    ppermute x1, starting transfers between devices, local(): lax.ppermute(up_weight, ('yh', 'core'), [(0, 0), (1, 2), (2, 3), (3, 1)])  7.79 us
  transfers between devices with their start and end apart: 11, of which 6 were waited for; matrix products, arithmetic and copies ran while one was open for 8% of the time, Pallas kernels for 0%

profile of v8, /device:TPU:1, one launch (start us, length us, event | category | flops | bytes accessed | tf_op | source)
XLA Modules:
  0.0 175.9 jit_solution(8466154171031114489)
XLA Ops:
  0.6 0.0 copy-start
  0.6 1.1 copy.18
  1.7 0.0 copy-start.5
  1.7 1.1 broadcast_in_dim.8
  2.8 7.6 %all-to-all-start = ((bf16[16,128,256]{2,1,0:T(8,128)(2,1)}), bf16[16,128,256]{2,1,0:T(8,128)(2,1)S(1)}, u32[]{:S(2)}, u32[]{:S(2)}) async-start(bf16[16,128,256]{2,1,0:T(8,128)(2,1)} %broadcast_in_dim.8), calls=%async_computation | async-start | bytes 2097152 | tf_op jit(solution)/shard_map/all_to_all | solution.py:15
  10.4 0.0 copy-done.5
  10.4 7.8 %collective-permute-start = (bf16[128,256]{1,0:T(8,128)(2,1)S(1)}, bf16[128,256]{1,0:T(8,128)(2,1)S(1)}, u32[]{:S(2)}, u32[]{:S(2)}) collective-permute-start(bf16[128,256]{1,0:T(8,128)(2,1)S(1)} %copy-done.5), channel_id=1, source_target_pairs={{0,0},{1,256},{256,257},{257,1},{2,2},{3,258},{258,259},{259,3},{4... | collective-permute-start | bytes 196616 | tf_op jit(solution)/shard_map/ppermute | solution.py:55
  18.2 0.0 copy-start.4
  18.2 4.6 %collective-permute-done = bf16[128,256]{1,0:T(8,128)(2,1)S(1)} collective-permute-done((bf16[128,256]{1,0:T(8,128)(2,1)S(1)}, bf16[128,256]{1,0:T(8,128)(2,1)S(1)}, u32[]{:S(2)}, u32[]{:S(2)}) %collective-permute-start) | collective-permute-done | bytes 65568 | tf_op jit(solution)/shard_map/ppermute | solution.py:55
  22.9 2.1 %all-to-all-done = bf16[16,128,256]{2,1,0:T(8,128)(2,1)S(1)} async-done(((bf16[16,128,256]{2,1,0:T(8,128)(2,1)}), bf16[16,128,256]{2,1,0:T(8,128)(2,1)S(1)}, u32[]{:S(2)}, u32[]{:S(2)}) %all-to-all-start) | async-done | bytes 1048608 | tf_op jit(solution)/shard_map/all_to_all | solution.py:15
  25.0 0.0 copy-start.2
  25.0 1.2 broadcast_in_dim.9
  26.2 0.1 copy-done.2
  26.3 4.7 %all-to-all-start.1 = ((bf16[16,128,256]{2,1,0:T(8,128)(2,1)}), bf16[16,128,256]{2,1,0:T(8,128)(2,1)S(1)}, u32[]{:S(2)}, u32[]{:S(2)}) async-start(bf16[16,128,256]{2,1,0:T(8,128)(2,1)} %broadcast_in_dim.9), calls=%async_computation.1 | async-start | bytes 2097152 | tf_op jit(solution)/shard_map/all_to_all | solution.py:15
  31.0 0.0 copy-done
  31.0 0.0 copy-done.4
  31.0 0.0 copy-start.3
  31.0 0.7 convolution_convert_fusion.1
  31.8 0.5 copy-done.3
  32.2 0.0 copy-start.1
  32.2 0.6 fusion
  32.8 5.2 %collective-permute-start.1 = (bf16[384,256]{1,0:T(8,128)(2,1)S(1)}, bf16[384,256]{1,0:T(8,128)(2,1)S(1)}, u32[]{:S(2)}, u32[]{:S(2)}) collective-permute-start(bf16[384,256]{1,0:T(8,128)(2,1)S(1)} %fusion), channel_id=1, source_target_pairs={{0,1},{1,0},{2,3},{3,2},{4,5},{5,4},{6,7},{7,6},{8,9},{9,8},{10,11... | collective-permute-start | bytes 589832 | tf_op jit(solution)/shard_map/ppermute | solution.py:24
  38.0 0.0 copy-done.1
  38.0 0.7 convolution_convert_fusion
  38.7 1.9 %bitcast_bitcast_fusion = bf16[16,512,128]{2,1,0:T(8,128)(2,1)} fusion(bf16[256,2048]{1,0:T(8,128)(2,1)S(1)} %convolution_convert_fusion, bf16[256,2048]{1,0:T(8,128)(2,1)S(1)} %convolution_convert_fusion.1), kind=kLoop, calls=%fused_computation.3 | loop fusion | flops 4194304 | bytes 4194304 | tf_op jit(solution)/shard_map/transpose | solution.py:66
  40.6 4.4 %all-to-all-done.1 = bf16[16,128,256]{2,1,0:T(8,128)(2,1)S(1)} async-done(((bf16[16,128,256]{2,1,0:T(8,128)(2,1)}), bf16[16,128,256]{2,1,0:T(8,128)(2,1)S(1)}, u32[]{:S(2)}, u32[]{:S(2)}) %all-to-all-start.1) | async-done | bytes 1048608 | tf_op jit(solution)/shard_map/all_to_all | solution.py:15
  45.0 4.4 %all-to-all-start.2 = ((bf16[16,512,128]{2,1,0:T(8,128)(2,1)}), bf16[16,512,128]{2,1,0:T(8,128)(2,1)}, u32[]{:S(2)}, u32[]{:S(2)}) async-start(bf16[16,512,128]{2,1,0:T(8,128)(2,1)} %bitcast_bitcast_fusion), calls=%async_computation.2 | async-start | bytes 4194304 | tf_op jit(solution)/shard_map/all_to_all | solution.py:15
  49.5 0.1 fusion.6
  49.6 0.0 collective-permute-done.1
  49.6 0.4 fusion.7
  50.0 0.4 add_convert_fusion
  50.4 0.1 dynamic-slice_bitcast_fusion.2
  50.5 6.1 %collective-permute-start.2 = (bf16[96,1024]{1,0:T(8,128)(2,1)S(1)}, bf16[96,1024]{1,0:T(8,128)(2,1)S(1)}, u32[]{:S(2)}, u32[]{:S(2)}) collective-permute-start(bf16[96,1024]{1,0:T(8,128)(2,1)S(1)} %get-tuple-element.31), channel_id=1, source_target_pairs={{0,2},{2,4},{4,6},{6,0},{1,3},{3,5},{5,7},{7,1},{8,10},{10,12},{12... | collective-permute-start | bytes 589832 | tf_op jit(solution)/shard_map/ppermute | solution.py:42
  56.6 4.9 %collective-permute-start.4 = (bf16[96,1024]{1,0:T(8,128)(2,1)S(1)}, bf16[96,1024]{1,0:T(8,128)(2,1)S(1)}, u32[]{:S(2)}, u32[]{:S(2)}) collective-permute-start(bf16[96,1024]{1,0:T(8,128)(2,1)S(1)} %get-tuple-element.32), channel_id=1, source_target_pairs={{0,4},{2,6},{4,0},{6,2},{1,5},{3,7},{5,1},{7,3},{8,12},{10,14},{12... | collective-permute-start | bytes 589832 | tf_op jit(solution)/shard_map/ppermute | solution.py:42
  61.5 2.6 %collective-permute-start.3 = (bf16[96,1024]{1,0:T(8,128)(2,1)S(1)}, bf16[96,1024]{1,0:T(8,128)(2,1)S(1)}, u32[]{:S(2)}, u32[]{:S(2)}) collective-permute-start(bf16[96,1024]{1,0:T(8,128)(2,1)S(1)} %get-tuple-element.33), channel_id=1, source_target_pairs={{0,6},{2,0},{4,2},{6,4},{1,7},{3,1},{5,3},{7,5},{8,14},{10,8},{12,... | collective-permute-start | bytes 589832 | tf_op jit(solution)/shard_map/ppermute | solution.py:42
  64.1 0.0 collective-permute-done.2
  64.1 8.4 %collective-permute-done.4 = bf16[96,1024]{1,0:T(8,128)(2,1)S(1)} collective-permute-done((bf16[96,1024]{1,0:T(8,128)(2,1)S(1)}, bf16[96,1024]{1,0:T(8,128)(2,1)S(1)}, u32[]{:S(2)}, u32[]{:S(2)}) %collective-permute-start.4) | collective-permute-done | bytes 196640 | tf_op jit(solution)/shard_map/ppermute | solution.py:42
  72.5 0.0 collective-permute-done.3
  72.5 0.1 fusion.3
  72.7 28.2 %all-gather = bf16[384,1024]{1,0:T(8,128)(2,1)S(1)} all-gather(bf16[96,1024]{1,0:T(8,128)(2,1)S(1)} %fusion.3), channel_id=2, replica_groups=mesh['yh'=2,'yl'=2,'x'=4,'zh'=4,'zl'=4,'core'=2] {'zh'}, dimensions={0}, use_global_device_ids=true | all-gather | bytes 983040 | tf_op jit(solution)/shard_map/all_gather | solution.py:73
  100.9 0.1 reduce_sum.57
  101.0 31.4 %all_gather.11 = bf16[384,1024]{1,0:T(8,128)(2,1)S(1)} all-gather(bf16[96,1024]{1,0:T(8,128)(2,1)S(1)} %reduce_sum.57), channel_id=1, replica_groups=mesh['yh'=2,'yl'=2,'x'=4,'zh'=4,'zl'=4,'core'=2] {'zl'}, dimensions={0}, use_global_device_ids=true | all-gather | bytes 983040 | tf_op jit(solution)/shard_map/all_gather | solution.py:76
  132.4 5.3 %collective-permute-start.5 = (bf16[384,1024]{1,0:T(8,128)(2,1)S(1)}, bf16[384,1024]{1,0:T(8,128)(2,1)}, u32[]{:S(2)}, u32[]{:S(2)}) collective-permute-start(bf16[384,1024]{1,0:T(8,128)(2,1)S(1)} %all_gather.11), channel_id=1, source_target_pairs={{0,1},{1,0},{2,3},{3,2},{4,5},{5,4},{6,7},{7,6},{8,9},{9,8},{10,11... | collective-permute-start | bytes 2359304 | tf_op jit(solution)/shard_map/ppermute | solution.py:24
  137.7 0.0 all-to-all-done.2
  137.7 1.9 %convert_reduce_fusion = f32[512,128]{1,0:T(8,128)S(1)} fusion(bf16[16,512,128]{2,1,0:T(8,128)(2,1)} %all-to-all-done.2), kind=kLoop, calls=%fused_computation | loop fusion | flops 2031616 | bytes 2359296 | tf_op jit(solution)/shard_map/reduce_sum | solution.py:68
  139.6 0.7 multiply_reduce_fusion
  140.3 0.6 broadcast_in_dim.11
  140.9 7.3 %all-to-all-start.4 = ((f32[16,1,256]{2,1,0:T(1,128)}), f32[16,1,256]{2,1,0:T(1,128)S(1)}, u32[]{:S(2)}, u32[]{:S(2)}) async-start(f32[16,1,256]{2,1,0:T(1,128)} %broadcast_in_dim.11), calls=%async_computation.4 | async-start | bytes 32768 | tf_op jit(solution)/shard_map/all_to_all | solution.py:15
  148.3 0.0 collective-permute-done.5
  148.3 2.1 %broadcast_select_fusion.1 = (bf16[384,1024]{1,0:T(8,128)(2,1)S(1)}, bf16[384,1024]{1,0:T(8,128)(2,1)}) fusion(bf16[384,1024]{1,0:T(8,128)(2,1)S(1)} %all_gather.11, bf16[384,1024]{1,0:T(8,128)(2,1)} %collective-permute-done.5, pred[]{:T(512)S(6)} %eq.4), kind=kLoop, calls=%fused_computation.10 | loop fusion | flops 786432 | bytes 3145729 | tf_op jit(solution)/shard_map/jit(_where)/select_n | solution.py:79
  150.4 4.3 %all-to-all-done.4 = f32[16,1,256]{2,1,0:T(1,128)S(1)} async-done(((f32[16,1,256]{2,1,0:T(1,128)}), f32[16,1,256]{2,1,0:T(1,128)S(1)}, u32[]{:S(2)}, u32[]{:S(2)}) %all-to-all-start.4) | async-done | bytes 16416 | tf_op jit(solution)/shard_map/all_to_all | solution.py:15
  154.7 0.6 broadcast_in_dim.10
  155.3 8.2 %all-to-all-start.3 = ((f32[32,1,128]{2,1,0:T(1,128)}), f32[32,1,128]{2,1,0:T(1,128)S(1)}, u32[]{:S(2)}, u32[]{:S(2)}) async-start(f32[32,1,128]{2,1,0:T(1,128)} %broadcast_in_dim.10), calls=%async_computation.3 | async-start | bytes 32768 | tf_op jit(solution)/shard_map/all_to_all | solution.py:15
  163.6 2.4 %pad_maximum_fusion = bf16[384,2048]{1,0:T(8,128)(2,1)} fusion(bf16[384,1024]{1,0:T(8,128)(2,1)} %get-tuple-element.28, bf16[384,1024]{1,0:T(8,128)(2,1)S(1)} %get-tuple-element.27), kind=kLoop, calls=%fused_computation.5 | loop fusion | flops 3145728 | bytes 3145728 | tf_op jit(solution)/shard_map/concatenate | solution.py:78
  166.0 0.8 copy.22
  166.8 0.6 reduce_sum.62
  167.4 8.1 %all-to-all-done.3 = f32[32,1,128]{2,1,0:T(1,128)S(1)} async-done(((f32[32,1,128]{2,1,0:T(1,128)}), f32[32,1,128]{2,1,0:T(1,128)S(1)}, u32[]{:S(2)}, u32[]{:S(2)}) %all-to-all-start.3) | async-done | bytes 16416 | tf_op jit(solution)/shard_map/all_to_all | solution.py:15
  175.4 0.5 reduce_sum.60
Async XLA Ops:
  0.6 30.4 %copy-start = (bf16[384,2048]{1,0:T(8,128)(2,1)S(1)}, bf16[384,2048]{1,0:T(8,128)(2,1)}, u32[]{:S(2)}) copy-start(bf16[384,2048]{1,0:T(8,128)(2,1)} %param.7) | copy-start | bytes 4718596
  1.7 8.7 %copy-start.5 = (bf16[128,256]{1,0:T(8,128)(2,1)S(1)}, bf16[128,256]{1,0:T(8,128)(2,1)}, u32[]{:S(2)}) copy-start(bf16[128,256]{1,0:T(8,128)(2,1)} %param.8) | copy-start | bytes 196612
  2.8 22.2 %all-to-all-start = ((bf16[16,128,256]{2,1,0:T(8,128)(2,1)}), bf16[16,128,256]{2,1,0:T(8,128)(2,1)S(1)}, u32[]{:S(2)}, u32[]{:S(2)}) async-start(bf16[16,128,256]{2,1,0:T(8,128)(2,1)} %broadcast_in_dim.8), calls=%async_computation | async-start | bytes 2097152 | tf_op jit(solution)/shard_map/all_to_all | solution.py:15
  10.4 12.5 %collective-permute-start = (bf16[128,256]{1,0:T(8,128)(2,1)S(1)}, bf16[128,256]{1,0:T(8,128)(2,1)S(1)}, u32[]{:S(2)}, u32[]{:S(2)}) collective-permute-start(bf16[128,256]{1,0:T(8,128)(2,1)S(1)} %copy-done.5), channel_id=1, source_target_pairs={{0,0},{1,256},{256,257},{257,1},{2,2},{3,258},{258,259},{259,3},{4... | collective-permute-start | bytes 196616 | tf_op jit(solution)/shard_map/ppermute | solution.py:55
  18.2 12.8 %copy-start.4 = (bf16[384,256]{1,0:T(8,128)(2,1)S(1)}, bf16[384,256]{1,0:T(8,128)(2,1)}, u32[]{:S(2)}) copy-start(bf16[384,256]{1,0:T(8,128)(2,1)} %param.6) | copy-start | bytes 589828
  25.0 1.3 copy-start.2
  26.3 18.8 %all-to-all-start.1 = ((bf16[16,128,256]{2,1,0:T(8,128)(2,1)}), bf16[16,128,256]{2,1,0:T(8,128)(2,1)S(1)}, u32[]{:S(2)}, u32[]{:S(2)}) async-start(bf16[16,128,256]{2,1,0:T(8,128)(2,1)} %broadcast_in_dim.9), calls=%async_computation.1 | async-start | bytes 2097152 | tf_op jit(solution)/shard_map/all_to_all | solution.py:15
  31.0 1.2 copy-start.3
  32.2 5.8 %copy-start.1 = (bf16[384,2048]{1,0:T(8,128)(2,1)S(1)}, bf16[384,2048]{1,0:T(8,128)(2,1)}, u32[]{:S(2)}) copy-start(bf16[384,2048]{1,0:T(8,128)(2,1)} %param.5) | copy-start | bytes 4718596
  32.8 16.8 %collective-permute-start.1 = (bf16[384,256]{1,0:T(8,128)(2,1)S(1)}, bf16[384,256]{1,0:T(8,128)(2,1)S(1)}, u32[]{:S(2)}, u32[]{:S(2)}) collective-permute-start(bf16[384,256]{1,0:T(8,128)(2,1)S(1)} %fusion), channel_id=1, source_target_pairs={{0,1},{1,0},{2,3},{3,2},{4,5},{5,4},{6,7},{7,6},{8,9},{9,8},{10,11... | collective-permute-start | bytes 589832 | tf_op jit(solution)/shard_map/ppermute | solution.py:24
  45.0 92.7 %all-to-all-start.2 = ((bf16[16,512,128]{2,1,0:T(8,128)(2,1)}), bf16[16,512,128]{2,1,0:T(8,128)(2,1)}, u32[]{:S(2)}, u32[]{:S(2)}) async-start(bf16[16,512,128]{2,1,0:T(8,128)(2,1)} %bitcast_bitcast_fusion), calls=%async_computation.2 | async-start | bytes 4194304 | tf_op jit(solution)/shard_map/all_to_all | solution.py:15
  50.5 13.6 %collective-permute-start.2 = (bf16[96,1024]{1,0:T(8,128)(2,1)S(1)}, bf16[96,1024]{1,0:T(8,128)(2,1)S(1)}, u32[]{:S(2)}, u32[]{:S(2)}) collective-permute-start(bf16[96,1024]{1,0:T(8,128)(2,1)S(1)} %get-tuple-element.31), channel_id=1, source_target_pairs={{0,2},{2,4},{4,6},{6,0},{1,3},{3,5},{5,7},{7,1},{8,10},{10,12},{12... | collective-permute-start | bytes 589832 | tf_op jit(solution)/shard_map/ppermute | solution.py:42
  56.6 16.0 %collective-permute-start.4 = (bf16[96,1024]{1,0:T(8,128)(2,1)S(1)}, bf16[96,1024]{1,0:T(8,128)(2,1)S(1)}, u32[]{:S(2)}, u32[]{:S(2)}) collective-permute-start(bf16[96,1024]{1,0:T(8,128)(2,1)S(1)} %get-tuple-element.32), channel_id=1, source_target_pairs={{0,4},{2,6},{4,0},{6,2},{1,5},{3,7},{5,1},{7,3},{8,12},{10,14},{12... | collective-permute-start | bytes 589832 | tf_op jit(solution)/shard_map/ppermute | solution.py:42
  61.5 11.1 %collective-permute-start.3 = (bf16[96,1024]{1,0:T(8,128)(2,1)S(1)}, bf16[96,1024]{1,0:T(8,128)(2,1)S(1)}, u32[]{:S(2)}, u32[]{:S(2)}) collective-permute-start(bf16[96,1024]{1,0:T(8,128)(2,1)S(1)} %get-tuple-element.33), channel_id=1, source_target_pairs={{0,6},{2,0},{4,2},{6,4},{1,7},{3,1},{5,3},{7,5},{8,14},{10,8},{12,... | collective-permute-start | bytes 589832 | tf_op jit(solution)/shard_map/ppermute | solution.py:42
  132.4 15.9 %collective-permute-start.5 = (bf16[384,1024]{1,0:T(8,128)(2,1)S(1)}, bf16[384,1024]{1,0:T(8,128)(2,1)}, u32[]{:S(2)}, u32[]{:S(2)}) collective-permute-start(bf16[384,1024]{1,0:T(8,128)(2,1)S(1)} %all_gather.11), channel_id=1, source_target_pairs={{0,1},{1,0},{2,3},{3,2},{4,5},{5,4},{6,7},{7,6},{8,9},{9,8},{10,11... | collective-permute-start | bytes 2359304 | tf_op jit(solution)/shard_map/ppermute | solution.py:24
  140.9 13.8 %all-to-all-start.4 = ((f32[16,1,256]{2,1,0:T(1,128)}), f32[16,1,256]{2,1,0:T(1,128)S(1)}, u32[]{:S(2)}, u32[]{:S(2)}) async-start(f32[16,1,256]{2,1,0:T(1,128)} %broadcast_in_dim.11), calls=%async_computation.4 | async-start | bytes 32768 | tf_op jit(solution)/shard_map/all_to_all | solution.py:15
  155.3 20.1 %all-to-all-start.3 = ((f32[32,1,128]{2,1,0:T(1,128)}), f32[32,1,128]{2,1,0:T(1,128)S(1)}, u32[]{:S(2)}, u32[]{:S(2)}) async-start(f32[32,1,128]{2,1,0:T(1,128)} %broadcast_in_dim.10), calls=%async_computation.3 | async-start | bytes 32768 | tf_op jit(solution)/shard_map/all_to_all | solution.py:15

commit v9 on v3

--- a/solution.py
+++ b/solution.py
@@ -8,6 +8,7 @@
 FS = ("yh", "yl", "x")
 TP = ("zh", "zl", "core")
 BF = jnp.bfloat16
+EXTRA = 8
 F32 = jnp.float32
 
 
@@ -43,10 +44,29 @@
     return total.astype(BF)
 
 
+def sum_at_owner(part):
+    rows, width = part.shape
+    many = lax.axis_size(FS)
+    blocks = jnp.moveaxis(part.reshape(rows, many, width // many), 1, 0)
+    return jnp.sum(exchange(blocks, FS).astype(F32), axis=0)
+
+
+def with_row(array, values):
+    high = lax.reduce_precision(values, 8, 7)
+    row = jnp.concatenate([high, values - high]).astype(BF)[None]
+    return jnp.concatenate(
+        [array, jnp.pad(row, ((0, EXTRA - 1), (0, array.shape[1] - row.shape[1])))], axis=0
+    )
+
+
+def without_row(array):
+    row = array[..., -EXTRA, :]
+    return array[..., :-EXTRA, :], row[..., :128] + row[..., 128:256]
+
+
 def local(inputs, pre_act, cotangent, up_weight, down_weight):
     tokens, width = inputs.shape
     hidden = pre_act.shape[1]
-    many = lax.axis_size(FS)
     core = lax.axis_index("core")
     active = jnp.maximum(pre_act.astype(F32), 0.0)
     squared = (active * active).astype(BF)
@@ -60,27 +80,25 @@
     theirs = other_core(pre_grad)
     half = (dot(pre_grad, up_rows[0], (1, 1)) + dot(theirs, up_rows[1], (1, 1))).astype(BF)
 
-    down_part = dot(squared, cotangent, (0, 0)).astype(BF)
-    up_part = dot(pre_grad, inputs, (0, 0)).astype(BF)
-    parts = jnp.concatenate([down_part, up_part], axis=0)
-    parts = jnp.moveaxis(parts.reshape(2 * hidden, many, width // many), 1, 0)
-    grads = exchange(parts, FS)
-    grads = jnp.sum(grads.astype(F32), axis=0)
-    down_grad, up_grad = grads[:hidden], grads[hidden:]
+    up_grad = sum_at_owner(dot(pre_grad, inputs, (0, 0)).astype(BF))
+    down_grad = sum_at_owner(dot(squared, cotangent, (0, 0)).astype(BF))
 
-    half = sum_near(half, "zl")
-    pieces = exchange(half.reshape(4, tokens // 16, width // 2), "zh")
-    half = jnp.sum(pieces.astype(F32), axis=0).astype(BF)
-
-    up_norms = from_everyone(jnp.sum(up_grad * up_grad, axis=0), TP)
-    half = lax.all_gather(half, "zh", axis=0, tiled=True)
+    quarter = sum_near(half, "zl")
+    quarter = with_row(quarter, jnp.sum(up_grad * up_grad, axis=0))
+    groups = lax.all_gather(quarter, "zh", axis=0, tiled=False)
+    quarter, squares = without_row(jnp.sum(groups.astype(F32), axis=0))
+    quarter = with_row(quarter.astype(BF), squares)
     down_norms = from_everyone(jnp.sum(down_grad * down_grad, axis=1), FS)
-    half = lax.all_gather(half, "zl", axis=0, tiled=True)
+    half = lax.all_gather(quarter, "zl", axis=0, tiled=False)
+    row = half[:, -EXTRA].astype(F32)
+    up_norms = jnp.sum(row[:, :128] + row[:, 128:256], axis=0)
+    half = half[:, :-EXTRA].reshape(tokens, width // 2)
     both = other_core(half)
+    up_norms += other_core(up_norms)
     input_grad = jnp.concatenate(
         [jnp.where(core == 0, half, both), jnp.where(core == 0, both, half)], axis=1
     )
-    up_norms, down_norms = jnp.sum(up_norms, axis=0), jnp.sum(down_norms, axis=0)
+    down_norms = jnp.sum(down_norms, axis=0)
     return input_grad, up_grad.T, down_grad, up_norms, down_norms
 
 

time: 185 us -> 171 us (0.924)
  blocking collectives: 35.6 us -> 60.5 us
  waiting for transfers between devices: 42.6 us -> 22.1 us
  starting transfers between devices: 82.4 us -> 64.9 us
  other arithmetic: 11.9 us -> 6.8 us
  local copies, waits for them, and re-layouts: 5.58 us -> 10.6 us
    all_gather x2, blocking collectives: 35.6 us -> 60.5 us  [the longest x1 30.4 us: local(): groups = lax.all_gather(quarter, 'zh', axis=0, tiled=False)]
    all_to_all x6 -> x5, waiting for transfers between devices: 29.6 us -> 11 us  [exchange(): return lax.all_to_all(array, axes, 0, 0, tiled=True)]
    all_to_all x6 -> x5, starting transfers between devices: 47.4 us -> 29.3 us  [exchange(): return lax.all_to_all(array, axes, 0, 0, tiled=True)]
    reshape x0 -> x2, local copies, waits for them, and re-layouts: none -> 2.48 us  [sum_at_owner(): blocks = jnp.moveaxis(part.reshape(rows, many, width // many), 1, 0)]
    unnamed x11 -> x18, local copies, waits for them, and re-layouts: 0.96 us -> 3.08 us
    ppermute x3, waiting for transfers between devices: 8.31 us -> 6.43 us  [sum_near(): total += lax.ppermute(piece, axis, ring).astype(F32)]
    transpose x1 -> x0, other arithmetic: 1.86 us -> none  [local(): parts = jnp.moveaxis(parts.reshape(2 * hidden, many, width // many), 1, 0)]
    ppermute x2 -> x3, starting transfers between devices: 14 us -> 13.9 us  [other_core(): return lax.ppermute(array, 'core', [(0, 1), (1, 0)])]
  transfers between devices with their start and end apart: 12 -> 12, of which waited for: 7 -> 5; matrix products, arithmetic and copies ran while one was open for 8% -> 8% of each run, Pallas kernels for 0% -> 0%
where the time goes in v9:
time: 171 us; the launch traced here: 170 us
  starting transfers between devices  64.9 us (38%)
  blocking collectives  60.5 us (35%)
  waiting for transfers between devices  22.1 us (13%)
  local copies, waits for them, and re-layouts  10.6 us (6%)
  other arithmetic  6.8 us (4%)
  matrix products  4.18 us (2%)
    all_gather x1, blocking collectives, local(): groups = lax.all_gather(quarter, 'zh', axis=0, tiled=False)  30.4 us
    all_gather x1, blocking collectives, local(): half = lax.all_gather(quarter, 'zl', axis=0, tiled=False)  30.1 us
    all_to_all x5, starting transfers between devices, exchange(): return lax.all_to_all(array, axes, 0, 0, tiled=True)  29.3 us
    ppermute x3, starting transfers between devices, other_core(): return lax.ppermute(array, 'core', [(0, 1), (1, 0)])  13.9 us
    ppermute x3, starting transfers between devices, sum_near(): total += lax.ppermute(piece, axis, ring).astype(F32)  13.7 us
    all_to_all x5, waiting for transfers between devices, exchange(): return lax.all_to_all(array, axes, 0, 0, tiled=True)  11 us
    ppermute x1, starting transfers between devices, local(): lax.ppermute(up_weight, ('yh', 'core'), [(0, 0), (1, 2), (2, 3), (3, 1)])  7.92 us
    ppermute x3, waiting for transfers between devices, sum_near(): total += lax.ppermute(piece, axis, ring).astype(F32)  6.43 us
  transfers between devices with their start and end apart: 12, of which 5 were waited for; matrix products, arithmetic and copies ran while one was open for 8% of the time, Pallas kernels for 0%

profile of v9, /device:TPU:1, one launch (start us, length us, event | category | flops | bytes accessed | tf_op | source)
XLA Modules:
  0.0 170.0 jit_solution(5098012545874044966)
XLA Ops:
  0.6 0.0 copy-start
  0.6 1.1 copy.21
  1.7 0.0 copy-start.7
  1.7 1.1 broadcast_in_dim.6
  2.8 7.6 %all-to-all-start = ((bf16[16,128,256]{2,1,0:T(8,128)(2,1)}), bf16[16,128,256]{2,1,0:T(8,128)(2,1)S(1)}, u32[]{:S(2)}, u32[]{:S(2)}) async-start(bf16[16,128,256]{2,1,0:T(8,128)(2,1)} %broadcast_in_dim.6), calls=%async_computation | async-start | bytes 2097152 | tf_op jit(solution)/shard_map/all_to_all | solution.py:16
  10.4 0.0 copy-done.7
  10.4 0.0 copy-start.5
  10.4 7.9 %collective-permute-start = (bf16[128,256]{1,0:T(8,128)(2,1)S(1)}, bf16[128,256]{1,0:T(8,128)(2,1)S(1)}, u32[]{:S(2)}, u32[]{:S(2)}) collective-permute-start(bf16[128,256]{1,0:T(8,128)(2,1)S(1)} %copy-done.7), channel_id=1, source_target_pairs={{0,0},{1,256},{256,257},{257,1},{2,2},{3,258},{258,259},{259,3},{4... | collective-permute-start | bytes 196616 | tf_op jit(solution)/shard_map/ppermute | solution.py:75
  18.3 4.6 %collective-permute-done = bf16[128,256]{1,0:T(8,128)(2,1)S(1)} collective-permute-done((bf16[128,256]{1,0:T(8,128)(2,1)S(1)}, bf16[128,256]{1,0:T(8,128)(2,1)S(1)}, u32[]{:S(2)}, u32[]{:S(2)}) %collective-permute-start) | collective-permute-done | bytes 65568 | tf_op jit(solution)/shard_map/ppermute | solution.py:75
  23.0 1.9 %all-to-all-done = bf16[16,128,256]{2,1,0:T(8,128)(2,1)S(1)} async-done(((bf16[16,128,256]{2,1,0:T(8,128)(2,1)}), bf16[16,128,256]{2,1,0:T(8,128)(2,1)S(1)}, u32[]{:S(2)}, u32[]{:S(2)}) %all-to-all-start) | async-done | bytes 1048608 | tf_op jit(solution)/shard_map/all_to_all | solution.py:16
  24.9 1.1 broadcast_in_dim.7
  26.1 0.2 copy-done.3
  26.2 4.7 %all-to-all-start.1 = ((bf16[16,128,256]{2,1,0:T(8,128)(2,1)}), bf16[16,128,256]{2,1,0:T(8,128)(2,1)S(1)}, u32[]{:S(2)}, u32[]{:S(2)}) async-start(bf16[16,128,256]{2,1,0:T(8,128)(2,1)} %broadcast_in_dim.7), calls=%async_computation.1 | async-start | bytes 2097152 | tf_op jit(solution)/shard_map/all_to_all | solution.py:16
  31.0 0.0 copy-done
  31.0 0.0 copy-done.5
  31.0 0.0 copy-start.1
  31.0 1.9 %fusion.2 = bf16[384,256]{1,0:T(8,128)(2,1)S(1)} fusion(bf16[384,2048]{1,0:T(8,128)(2,1)S(1)} %copy-done, bf16[2048,256]{1,0:T(8,128)(2,1)} %bitcast.62, bf16[384,256]{1,0:T(8,128)(2,1)S(1)} %copy-done.5), kind=kOutput, calls=%fused_computation.10 | convolution fusion | flops 403144704 | bytes 3014656 | tf_op jit(solution)/shard_map/dot_general | solution.py:29
  33.0 5.2 %collective-permute-start.1 = (bf16[384,256]{1,0:T(8,128)(2,1)S(1)}, bf16[384,256]{1,0:T(8,128)(2,1)S(1)}, u32[]{:S(2)}, u32[]{:S(2)}) collective-permute-start(bf16[384,256]{1,0:T(8,128)(2,1)S(1)} %fusion.2), channel_id=1, source_target_pairs={{0,1},{1,0},{2,3},{3,2},{4,5},{5,4},{6,7},{7,6},{8,9},{9,8},{10,11... | collective-permute-start | bytes 589832 | tf_op jit(solution)/shard_map/ppermute | solution.py:25
  38.1 0.0 copy-done.1
  38.2 0.7 fusion
  38.9 1.2 copy.36
  40.1 4.9 %all-to-all-done.1 = bf16[16,128,256]{2,1,0:T(8,128)(2,1)S(1)} async-done(((bf16[16,128,256]{2,1,0:T(8,128)(2,1)}), bf16[16,128,256]{2,1,0:T(8,128)(2,1)S(1)}, u32[]{:S(2)}, u32[]{:S(2)}) %all-to-all-start.1) | async-done | bytes 1048608 | tf_op jit(solution)/shard_map/all_to_all | solution.py:16
  45.0 4.3 %all-to-all-start.2 = ((bf16[16,256,128]{2,1,0:T(8,128)(2,1)}), bf16[16,256,128]{2,1,0:T(8,128)(2,1)}, u32[]{:S(2)}, u32[]{:S(2)}) async-start(bf16[16,256,128]{2,1,0:T(8,128)(2,1)} %bitcast.53), calls=%async_computation.2 | async-start | bytes 2097152 | tf_op jit(solution)/shard_map/all_to_all | solution.py:16
  49.4 0.1 fusion.24
  49.5 0.0 collective-permute-done.1
  49.5 0.4 fusion.25
  49.9 0.0 copy-start.6
  49.9 0.4 add_convert_fusion
  50.3 0.1 dynamic-slice_bitcast_fusion.2
  50.4 6.2 %collective-permute-start.2 = (bf16[96,1024]{1,0:T(8,128)(2,1)S(1)}, bf16[96,1024]{1,0:T(8,128)(2,1)S(1)}, u32[]{:S(2)}, u32[]{:S(2)}) collective-permute-start(bf16[96,1024]{1,0:T(8,128)(2,1)S(1)} %get-tuple-element.24), channel_id=1, source_target_pairs={{0,2},{2,4},{4,6},{6,0},{1,3},{3,5},{5,7},{7,1},{8,10},{10,12},{12... | collective-permute-start | bytes 589832 | tf_op jit(solution)/shard_map/ppermute | solution.py:43
  56.6 4.9 %collective-permute-start.4 = (bf16[96,1024]{1,0:T(8,128)(2,1)S(1)}, bf16[96,1024]{1,0:T(8,128)(2,1)S(1)}, u32[]{:S(2)}, u32[]{:S(2)}) collective-permute-start(bf16[96,1024]{1,0:T(8,128)(2,1)S(1)} %get-tuple-element.25), channel_id=1, source_target_pairs={{0,4},{2,6},{4,0},{6,2},{1,5},{3,7},{5,1},{7,3},{8,12},{10,14},{12... | collective-permute-start | bytes 589832 | tf_op jit(solution)/shard_map/ppermute | solution.py:43
  61.5 2.6 %collective-permute-start.3 = (bf16[96,1024]{1,0:T(8,128)(2,1)S(1)}, bf16[96,1024]{1,0:T(8,128)(2,1)}, u32[]{:S(2)}, u32[]{:S(2)}) collective-permute-start(bf16[96,1024]{1,0:T(8,128)(2,1)S(1)} %get-tuple-element.26), channel_id=1, source_target_pairs={{0,6},{2,0},{4,2},{6,4},{1,7},{3,1},{5,3},{7,5},{8,14},{10,8},{12,... | collective-permute-start | bytes 589832 | tf_op jit(solution)/shard_map/ppermute | solution.py:43
  64.1 0.0 copy-done.6
  64.1 0.7 fusion.1
  64.9 1.2 copy.35
  66.1 0.0 collective-permute-done.2
  66.1 6.4 %collective-permute-done.4 = bf16[96,1024]{1,0:T(8,128)(2,1)S(1)} collective-permute-done((bf16[96,1024]{1,0:T(8,128)(2,1)S(1)}, bf16[96,1024]{1,0:T(8,128)(2,1)S(1)}, u32[]{:S(2)}, u32[]{:S(2)}) %collective-permute-start.4) | collective-permute-done | bytes 196640 | tf_op jit(solution)/shard_map/ppermute | solution.py:43
  72.5 0.0 collective-permute-done.3
  72.5 1.0 fusion.5
  73.6 0.0 all-to-all-done.2
  73.6 6.5 %all-to-all-start.3 = ((bf16[16,256,128]{2,1,0:T(8,128)(2,1)}), bf16[16,256,128]{2,1,0:T(8,128)(2,1)S(1)}, u32[]{:S(2)}, u32[]{:S(2)}) async-start(bf16[16,256,128]{2,1,0:T(8,128)(2,1)} %bitcast.49), calls=%async_computation.3 | async-start | bytes 2097152 | tf_op jit(solution)/shard_map/all_to_all | solution.py:16
  80.1 1.4 convert_reduce_fusion.1
  81.6 0.6 copy-done.2
  82.1 30.4 %all-gather = bf16[416,1024]{1,0:T(8,128)(2,1)S(1)} all-gather(bf16[104,1024]{1,0:T(8,128)(2,1)S(1)} %pad_maximum_fusion.1), channel_id=2, replica_groups=mesh['yh'=2,'yl'=2,'x'=4,'zh'=4,'zl'=4,'core'=2] {'zh'}, dimensions={0}, use_global_device_ids=true | all-gather | bytes 1064960 | tf_op jit(solution)/shard_map/all_gather | solution.py:88
  112.5 0.1 convert_reduce_fusion.2
  112.8 30.1 %all-gather.1 = bf16[416,1024]{1,0:T(8,128)(2,1)S(1)} all-gather(bf16[104,1024]{1,0:T(8,128)(2,1)S(1)} %pad_maximum_fusion.2), channel_id=3, replica_groups=mesh['yh'=2,'yl'=2,'x'=4,'zh'=4,'zl'=4,'core'=2] {'zl'}, dimensions={0}, use_global_device_ids=true | all-gather | bytes 1064960 | tf_op jit(solution)/shard_map/all_gather | solution.py:92
  142.9 0.9 slice.49
  143.8 6.6 %collective-permute-start.5 = (bf16[384,1024]{1,0:T(8,128)(2,1)}, bf16[384,1024]{1,0:T(8,128)(2,1)}, u32[]{:S(2)}, u32[]{:S(2)}) collective-permute-start(bf16[384,1024]{1,0:T(8,128)(2,1)} %bitcast.14), channel_id=1, source_target_pairs={{0,1},{1,0},{2,3},{3,2},{4,5},{5,4},{6,7},{7,6},{8,9},{9,8},{10,11... | collective-permute-start | bytes 2359304 | tf_op jit(solution)/shard_map/ppermute | solution.py:25
  150.4 0.0 all-to-all-done.3
  150.4 0.1 convert_reduce_fusion
  150.5 0.0 copy-start.4
  150.5 0.6 copy-done.4
  151.2 0.1 multiply_reduce_fusion
  151.3 0.6 broadcast_in_dim.8
  151.9 6.2 %all-to-all-start.4 = ((f32[16,1,256]{2,1,0:T(1,128)}), f32[16,1,256]{2,1,0:T(1,128)S(1)}, u32[]{:S(2)}, u32[]{:S(2)}) async-start(f32[16,1,256]{2,1,0:T(1,128)} %broadcast_in_dim.8), calls=%async_computation.4 | async-start | bytes 32768 | tf_op jit(solution)/shard_map/all_to_all | solution.py:16
  158.1 2.2 %collective-permute-start.6 = (f32[128]{0:T(128)S(1)}, f32[128]{0:T(128)S(1)}, u32[]{:S(2)}, u32[]{:S(2)}) collective-permute-start(f32[128]{0:T(128)S(1)} %fusion.18), channel_id=1, source_target_pairs={{0,1},{1,0},{2,3},{3,2},{4,5},{5,4},{6,7},{7,6},{8,9},{9,8},{10,11... | collective-permute-start | bytes 1544 | tf_op jit(solution)/shard_map/ppermute | solution.py:25
  160.3 4.2 %all-to-all-done.4 = f32[16,1,256]{2,1,0:T(1,128)S(1)} async-done(((f32[16,1,256]{2,1,0:T(1,128)}), f32[16,1,256]{2,1,0:T(1,128)S(1)}, u32[]{:S(2)}, u32[]{:S(2)}) %all-to-all-start.4) | async-done | bytes 16416 | tf_op jit(solution)/shard_map/all_to_all | solution.py:16
  164.5 0.6 reduce_sum.69
  165.1 1.7 copy.26
  166.8 0.0 collective-permute-done.6
  166.8 0.5 add.62
  167.3 0.0 collective-permute-done.5
  167.3 1.5 broadcast_select_fusion.1
  168.8 1.2 pad_maximum_fusion
  (13 shorter events, 0.2 us)
Async XLA Ops:
  0.6 30.4 %copy-start = (bf16[384,2048]{1,0:T(8,128)(2,1)S(1)}, bf16[384,2048]{1,0:T(8,128)(2,1)}, u32[]{:S(2)}) copy-start(bf16[384,2048]{1,0:T(8,128)(2,1)} %param.7) | copy-start | bytes 4718596
  1.7 8.7 %copy-start.7 = (bf16[128,256]{1,0:T(8,128)(2,1)S(1)}, bf16[128,256]{1,0:T(8,128)(2,1)}, u32[]{:S(2)}) copy-start(bf16[128,256]{1,0:T(8,128)(2,1)} %param.8) | copy-start | bytes 196612
  2.8 22.1 %all-to-all-start = ((bf16[16,128,256]{2,1,0:T(8,128)(2,1)}), bf16[16,128,256]{2,1,0:T(8,128)(2,1)S(1)}, u32[]{:S(2)}, u32[]{:S(2)}) async-start(bf16[16,128,256]{2,1,0:T(8,128)(2,1)} %broadcast_in_dim.6), calls=%async_computation | async-start | bytes 2097152 | tf_op jit(solution)/shard_map/all_to_all | solution.py:16
  10.4 20.6 %copy-start.5 = (bf16[384,256]{1,0:T(8,128)(2,1)S(1)}, bf16[384,256]{1,0:T(8,128)(2,1)}, u32[]{:S(2)}) copy-start(bf16[384,256]{1,0:T(8,128)(2,1)} %param.6) | copy-start | bytes 589828
  10.4 12.6 %collective-permute-start = (bf16[128,256]{1,0:T(8,128)(2,1)S(1)}, bf16[128,256]{1,0:T(8,128)(2,1)S(1)}, u32[]{:S(2)}, u32[]{:S(2)}) collective-permute-start(bf16[128,256]{1,0:T(8,128)(2,1)S(1)} %copy-done.7), channel_id=1, source_target_pairs={{0,0},{1,256},{256,257},{257,1},{2,2},{3,258},{258,259},{259,3},{4... | collective-permute-start | bytes 196616 | tf_op jit(solution)/shard_map/ppermute | solution.py:75
  24.9 1.3 copy-start.3
  26.2 18.8 %all-to-all-start.1 = ((bf16[16,128,256]{2,1,0:T(8,128)(2,1)}), bf16[16,128,256]{2,1,0:T(8,128)(2,1)S(1)}, u32[]{:S(2)}, u32[]{:S(2)}) async-start(bf16[16,128,256]{2,1,0:T(8,128)(2,1)} %broadcast_in_dim.7), calls=%async_computation.1 | async-start | bytes 2097152 | tf_op jit(solution)/shard_map/all_to_all | solution.py:16
  31.0 7.1 %copy-start.1 = (bf16[384,2048]{1,0:T(8,128)(2,1)S(1)}, bf16[384,2048]{1,0:T(8,128)(2,1)}, u32[]{:S(2)}) copy-start(bf16[384,2048]{1,0:T(8,128)(2,1)} %param.5) | copy-start | bytes 4718596
  33.0 16.5 %collective-permute-start.1 = (bf16[384,256]{1,0:T(8,128)(2,1)S(1)}, bf16[384,256]{1,0:T(8,128)(2,1)S(1)}, u32[]{:S(2)}, u32[]{:S(2)}) collective-permute-start(bf16[384,256]{1,0:T(8,128)(2,1)S(1)} %fusion.2), channel_id=1, source_target_pairs={{0,1},{1,0},{2,3},{3,2},{4,5},{5,4},{6,7},{7,6},{8,9},{9,8},{10,11... | collective-permute-start | bytes 589832 | tf_op jit(solution)/shard_map/ppermute | solution.py:25
  45.0 28.5 %all-to-all-start.2 = ((bf16[16,256,128]{2,1,0:T(8,128)(2,1)}), bf16[16,256,128]{2,1,0:T(8,128)(2,1)}, u32[]{:S(2)}, u32[]{:S(2)}) async-start(bf16[16,256,128]{2,1,0:T(8,128)(2,1)} %bitcast.53), calls=%async_computation.2 | async-start | bytes 2097152 | tf_op jit(solution)/shard_map/all_to_all | solution.py:16
  49.9 14.2 %copy-start.6 = (bf16[384,256]{1,0:T(8,128)(2,1)S(1)}, bf16[384,256]{1,0:T(8,128)(2,1)}, u32[]{:S(2)}) copy-start(bf16[384,256]{1,0:T(8,128)(2,1)} %param.6) | copy-start | bytes 589828
  50.4 15.7 %collective-permute-start.2 = (bf16[96,1024]{1,0:T(8,128)(2,1)S(1)}, bf16[96,1024]{1,0:T(8,128)(2,1)S(1)}, u32[]{:S(2)}, u32[]{:S(2)}) collective-permute-start(bf16[96,1024]{1,0:T(8,128)(2,1)S(1)} %get-tuple-element.24), channel_id=1, source_target_pairs={{0,2},{2,4},{4,6},{6,0},{1,3},{3,5},{5,7},{7,1},{8,10},{10,12},{12... | collective-permute-start | bytes 589832 | tf_op jit(solution)/shard_map/ppermute | solution.py:43
  56.6 16.0 %collective-permute-start.4 = (bf16[96,1024]{1,0:T(8,128)(2,1)S(1)}, bf16[96,1024]{1,0:T(8,128)(2,1)S(1)}, u32[]{:S(2)}, u32[]{:S(2)}) collective-permute-start(bf16[96,1024]{1,0:T(8,128)(2,1)S(1)} %get-tuple-element.25), channel_id=1, source_target_pairs={{0,4},{2,6},{4,0},{6,2},{1,5},{3,7},{5,1},{7,3},{8,12},{10,14},{12... | collective-permute-start | bytes 589832 | tf_op jit(solution)/shard_map/ppermute | solution.py:43
  61.5 11.1 %collective-permute-start.3 = (bf16[96,1024]{1,0:T(8,128)(2,1)S(1)}, bf16[96,1024]{1,0:T(8,128)(2,1)}, u32[]{:S(2)}, u32[]{:S(2)}) collective-permute-start(bf16[96,1024]{1,0:T(8,128)(2,1)S(1)} %get-tuple-element.26), channel_id=1, source_target_pairs={{0,6},{2,0},{4,2},{6,4},{1,7},{3,1},{5,3},{7,5},{8,14},{10,8},{12,... | collective-permute-start | bytes 589832 | tf_op jit(solution)/shard_map/ppermute | solution.py:43
  73.6 76.8 %all-to-all-start.3 = ((bf16[16,256,128]{2,1,0:T(8,128)(2,1)}), bf16[16,256,128]{2,1,0:T(8,128)(2,1)S(1)}, u32[]{:S(2)}, u32[]{:S(2)}) async-start(bf16[16,256,128]{2,1,0:T(8,128)(2,1)} %bitcast.49), calls=%async_computation.3 | async-start | bytes 2097152 | tf_op jit(solution)/shard_map/all_to_all | solution.py:16
  81.5 0.6 copy-start.2
  143.8 23.5 %collective-permute-start.5 = (bf16[384,1024]{1,0:T(8,128)(2,1)}, bf16[384,1024]{1,0:T(8,128)(2,1)}, u32[]{:S(2)}, u32[]{:S(2)}) collective-permute-start(bf16[384,1024]{1,0:T(8,128)(2,1)} %bitcast.14), channel_id=1, source_target_pairs={{0,1},{1,0},{2,3},{3,2},{4,5},{5,4},{6,7},{7,6},{8,9},{9,8},{10,11... | collective-permute-start | bytes 2359304 | tf_op jit(solution)/shard_map/ppermute | solution.py:25
  150.5 0.7 copy-start.4
  151.9 12.6 %all-to-all-start.4 = ((f32[16,1,256]{2,1,0:T(1,128)}), f32[16,1,256]{2,1,0:T(1,128)S(1)}, u32[]{:S(2)}, u32[]{:S(2)}) async-start(f32[16,1,256]{2,1,0:T(1,128)} %broadcast_in_dim.8), calls=%async_computation.4 | async-start | bytes 32768 | tf_op jit(solution)/shard_map/all_to_all | solution.py:16
  158.1 8.6 %collective-permute-start.6 = (f32[128]{0:T(128)S(1)}, f32[128]{0:T(128)S(1)}, u32[]{:S(2)}, u32[]{:S(2)}) collective-permute-start(f32[128]{0:T(128)S(1)} %fusion.18), channel_id=1, source_target_pairs={{0,1},{1,0},{2,3},{3,2},{4,5},{5,4},{6,7},{7,6},{8,9},{9,8},{10,11... | collective-permute-start | bytes 1544 | tf_op jit(solution)/shard_map/ppermute | solution.py:25

commit v10 on v9

--- a/solution.py
+++ b/solution.py
@@ -36,18 +36,24 @@
     here = lax.axis_index(axis)
     pieces = half.reshape(count, half.shape[0] // count, half.shape[1])
     total = lax.dynamic_index_in_dim(pieces, here, 0, False).astype(F32)
+    others = []
     for step in (1, 3, 2):
         there = lax.rem(here + step, count)
         piece = lax.dynamic_index_in_dim(pieces, there, 0, False)
         ring = [(i, (i + step) % count) for i in range(count)]
-        total += lax.ppermute(piece, axis, ring).astype(F32)
+        others.append(lax.ppermute(piece, axis, ring))
+    for other in others:
+        total += other.astype(F32)
     return total.astype(BF)
 
 
-def sum_at_owner(part):
+def in_blocks(part):
     rows, width = part.shape
     many = lax.axis_size(FS)
-    blocks = jnp.moveaxis(part.reshape(rows, many, width // many), 1, 0)
+    return jnp.moveaxis(part.reshape(rows, many, width // many), 1, 0)
+
+
+def sum_at_owner(blocks):
     return jnp.sum(exchange(blocks, FS).astype(F32), axis=0)
 
 
@@ -80,8 +86,9 @@
     theirs = other_core(pre_grad)
     half = (dot(pre_grad, up_rows[0], (1, 1)) + dot(theirs, up_rows[1], (1, 1))).astype(BF)
 
-    up_grad = sum_at_owner(dot(pre_grad, inputs, (0, 0)).astype(BF))
-    down_grad = sum_at_owner(dot(squared, cotangent, (0, 0)).astype(BF))
+    up_grad = sum_at_owner(in_blocks(dot(pre_grad, inputs, (0, 0)).astype(BF)))
+    down_part = in_blocks(dot(squared, cotangent, (0, 0)).astype(BF))
+    down_grad = sum_at_owner(down_part)
 
     quarter = sum_near(half, "zl")
     quarter = with_row(quarter, jnp.sum(up_grad * up_grad, axis=0))

time: 171 us -> 171 us (level)
  no operation moved by 1% of the time
where the time goes in v10:
time: 171 us; the launch traced here: 170 us
  starting transfers between devices  64.9 us (38%)
  blocking collectives  60.5 us (35%)
  waiting for transfers between devices  22.1 us (13%)
  local copies, waits for them, and re-layouts  10.6 us (6%)
  other arithmetic  6.8 us (4%)
  matrix products  4.18 us (2%)
    all_gather x1, blocking collectives, local(): groups = lax.all_gather(quarter, 'zh', axis=0, tiled=False)  30.4 us
    all_gather x1, blocking collectives, local(): half = lax.all_gather(quarter, 'zl', axis=0, tiled=False)  30.1 us
    all_to_all x5, starting transfers between devices, exchange(): return lax.all_to_all(array, axes, 0, 0, tiled=True)  29.3 us
    ppermute x3, starting transfers between devices, other_core(): return lax.ppermute(array, 'core', [(0, 1), (1, 0)])  13.9 us
    ppermute x3, starting transfers between devices, sum_near(): others.append(lax.ppermute(piece, axis, ring))  13.7 us
    all_to_all x5, waiting for transfers between devices, exchange(): return lax.all_to_all(array, axes, 0, 0, tiled=True)  11 us
    ppermute x1, starting transfers between devices, local(): lax.ppermute(up_weight, ('yh', 'core'), [(0, 0), (1, 2), (2, 3), (3, 1)])  7.92 us
    ppermute x3, waiting for transfers between devices, sum_near(): others.append(lax.ppermute(piece, axis, ring))  6.43 us
  transfers between devices with their start and end apart: 12, of which 5 were waited for; matrix products, arithmetic and copies ran while one was open for 8% of the time, Pallas kernels for 0%

profile of v10, /device:TPU:1, one launch (start us, length us, event | category | flops | bytes accessed | tf_op | source)
XLA Modules:
  0.0 170.0 jit_solution(5098012545874044966)
XLA Ops:
  0.6 0.0 copy-start
  0.6 1.1 copy.21
  1.7 0.0 copy-start.7
  1.7 1.1 broadcast_in_dim.6
  2.8 7.6 %all-to-all-start = ((bf16[16,128,256]{2,1,0:T(8,128)(2,1)}), bf16[16,128,256]{2,1,0:T(8,128)(2,1)S(1)}, u32[]{:S(2)}, u32[]{:S(2)}) async-start(bf16[16,128,256]{2,1,0:T(8,128)(2,1)} %broadcast_in_dim.6), calls=%async_computation | async-start | bytes 2097152 | tf_op jit(solution)/shard_map/all_to_all | solution.py:16
  10.4 0.0 copy-done.7
  10.4 0.0 copy-start.5
  10.4 7.9 %collective-permute-start = (bf16[128,256]{1,0:T(8,128)(2,1)S(1)}, bf16[128,256]{1,0:T(8,128)(2,1)S(1)}, u32[]{:S(2)}, u32[]{:S(2)}) collective-permute-start(bf16[128,256]{1,0:T(8,128)(2,1)S(1)} %copy-done.7), channel_id=1, source_target_pairs={{0,0},{1,256},{256,257},{257,1},{2,2},{3,258},{258,259},{259,3},{4... | collective-permute-start | bytes 196616 | tf_op jit(solution)/shard_map/ppermute | solution.py:81
  18.3 4.6 %collective-permute-done = bf16[128,256]{1,0:T(8,128)(2,1)S(1)} collective-permute-done((bf16[128,256]{1,0:T(8,128)(2,1)S(1)}, bf16[128,256]{1,0:T(8,128)(2,1)S(1)}, u32[]{:S(2)}, u32[]{:S(2)}) %collective-permute-start) | collective-permute-done | bytes 65568 | tf_op jit(solution)/shard_map/ppermute | solution.py:81
  23.0 1.9 %all-to-all-done = bf16[16,128,256]{2,1,0:T(8,128)(2,1)S(1)} async-done(((bf16[16,128,256]{2,1,0:T(8,128)(2,1)}), bf16[16,128,256]{2,1,0:T(8,128)(2,1)S(1)}, u32[]{:S(2)}, u32[]{:S(2)}) %all-to-all-start) | async-done | bytes 1048608 | tf_op jit(solution)/shard_map/all_to_all | solution.py:16
  24.9 1.1 broadcast_in_dim.7
  26.1 0.2 copy-done.3
  26.2 4.7 %all-to-all-start.1 = ((bf16[16,128,256]{2,1,0:T(8,128)(2,1)}), bf16[16,128,256]{2,1,0:T(8,128)(2,1)S(1)}, u32[]{:S(2)}, u32[]{:S(2)}) async-start(bf16[16,128,256]{2,1,0:T(8,128)(2,1)} %broadcast_in_dim.7), calls=%async_computation.1 | async-start | bytes 2097152 | tf_op jit(solution)/shard_map/all_to_all | solution.py:16
  31.0 0.0 copy-done
  31.0 0.0 copy-done.5
  31.0 0.0 copy-start.1
  31.0 1.9 %fusion.2 = bf16[384,256]{1,0:T(8,128)(2,1)S(1)} fusion(bf16[384,2048]{1,0:T(8,128)(2,1)S(1)} %copy-done, bf16[2048,256]{1,0:T(8,128)(2,1)} %bitcast.62, bf16[384,256]{1,0:T(8,128)(2,1)S(1)} %copy-done.5), kind=kOutput, calls=%fused_computation.10 | convolution fusion | flops 403144704 | bytes 3014656 | tf_op jit(solution)/shard_map/dot_general | solution.py:29
  33.0 5.2 %collective-permute-start.1 = (bf16[384,256]{1,0:T(8,128)(2,1)S(1)}, bf16[384,256]{1,0:T(8,128)(2,1)S(1)}, u32[]{:S(2)}, u32[]{:S(2)}) collective-permute-start(bf16[384,256]{1,0:T(8,128)(2,1)S(1)} %fusion.2), channel_id=1, source_target_pairs={{0,1},{1,0},{2,3},{3,2},{4,5},{5,4},{6,7},{7,6},{8,9},{9,8},{10,11... | collective-permute-start | bytes 589832 | tf_op jit(solution)/shard_map/ppermute | solution.py:25
  38.1 0.0 copy-done.1
  38.2 0.7 fusion
  38.9 1.2 copy.36
  40.1 4.9 %all-to-all-done.1 = bf16[16,128,256]{2,1,0:T(8,128)(2,1)S(1)} async-done(((bf16[16,128,256]{2,1,0:T(8,128)(2,1)}), bf16[16,128,256]{2,1,0:T(8,128)(2,1)S(1)}, u32[]{:S(2)}, u32[]{:S(2)}) %all-to-all-start.1) | async-done | bytes 1048608 | tf_op jit(solution)/shard_map/all_to_all | solution.py:16
  45.0 4.3 %all-to-all-start.2 = ((bf16[16,256,128]{2,1,0:T(8,128)(2,1)}), bf16[16,256,128]{2,1,0:T(8,128)(2,1)}, u32[]{:S(2)}, u32[]{:S(2)}) async-start(bf16[16,256,128]{2,1,0:T(8,128)(2,1)} %bitcast.53), calls=%async_computation.2 | async-start | bytes 2097152 | tf_op jit(solution)/shard_map/all_to_all | solution.py:16
  49.4 0.1 fusion.24
  49.5 0.0 collective-permute-done.1
  49.5 0.4 fusion.25
  49.9 0.0 copy-start.6
  49.9 0.4 add_convert_fusion
  50.3 0.1 dynamic-slice_bitcast_fusion.2
  50.4 6.2 %collective-permute-start.2 = (bf16[96,1024]{1,0:T(8,128)(2,1)S(1)}, bf16[96,1024]{1,0:T(8,128)(2,1)S(1)}, u32[]{:S(2)}, u32[]{:S(2)}) collective-permute-start(bf16[96,1024]{1,0:T(8,128)(2,1)S(1)} %get-tuple-element.24), channel_id=1, source_target_pairs={{0,2},{2,4},{4,6},{6,0},{1,3},{3,5},{5,7},{7,1},{8,10},{10,12},{12... | collective-permute-start | bytes 589832 | tf_op jit(solution)/shard_map/ppermute | solution.py:44
  56.6 4.9 %collective-permute-start.4 = (bf16[96,1024]{1,0:T(8,128)(2,1)S(1)}, bf16[96,1024]{1,0:T(8,128)(2,1)S(1)}, u32[]{:S(2)}, u32[]{:S(2)}) collective-permute-start(bf16[96,1024]{1,0:T(8,128)(2,1)S(1)} %get-tuple-element.25), channel_id=1, source_target_pairs={{0,4},{2,6},{4,0},{6,2},{1,5},{3,7},{5,1},{7,3},{8,12},{10,14},{12... | collective-permute-start | bytes 589832 | tf_op jit(solution)/shard_map/ppermute | solution.py:44
  61.5 2.6 %collective-permute-start.3 = (bf16[96,1024]{1,0:T(8,128)(2,1)S(1)}, bf16[96,1024]{1,0:T(8,128)(2,1)}, u32[]{:S(2)}, u32[]{:S(2)}) collective-permute-start(bf16[96,1024]{1,0:T(8,128)(2,1)S(1)} %get-tuple-element.26), channel_id=1, source_target_pairs={{0,6},{2,0},{4,2},{6,4},{1,7},{3,1},{5,3},{7,5},{8,14},{10,8},{12,... | collective-permute-start | bytes 589832 | tf_op jit(solution)/shard_map/ppermute | solution.py:44
  64.1 0.0 copy-done.6
  64.1 0.7 fusion.1
  64.9 1.2 copy.35
  66.1 0.0 collective-permute-done.2
  66.1 6.4 %collective-permute-done.4 = bf16[96,1024]{1,0:T(8,128)(2,1)S(1)} collective-permute-done((bf16[96,1024]{1,0:T(8,128)(2,1)S(1)}, bf16[96,1024]{1,0:T(8,128)(2,1)S(1)}, u32[]{:S(2)}, u32[]{:S(2)}) %collective-permute-start.4) | collective-permute-done | bytes 196640 | tf_op jit(solution)/shard_map/ppermute | solution.py:44
  72.5 0.0 collective-permute-done.3
  72.5 1.0 fusion.5
  73.6 0.0 all-to-all-done.2
  73.6 6.5 %all-to-all-start.3 = ((bf16[16,256,128]{2,1,0:T(8,128)(2,1)}), bf16[16,256,128]{2,1,0:T(8,128)(2,1)S(1)}, u32[]{:S(2)}, u32[]{:S(2)}) async-start(bf16[16,256,128]{2,1,0:T(8,128)(2,1)} %bitcast.49), calls=%async_computation.3 | async-start | bytes 2097152 | tf_op jit(solution)/shard_map/all_to_all | solution.py:16
  80.1 1.4 convert_reduce_fusion.1
  81.6 0.6 copy-done.2
  82.1 30.4 %all-gather = bf16[416,1024]{1,0:T(8,128)(2,1)S(1)} all-gather(bf16[104,1024]{1,0:T(8,128)(2,1)S(1)} %pad_maximum_fusion.1), channel_id=2, replica_groups=mesh['yh'=2,'yl'=2,'x'=4,'zh'=4,'zl'=4,'core'=2] {'zh'}, dimensions={0}, use_global_device_ids=true | all-gather | bytes 1064960 | tf_op jit(solution)/shard_map/all_gather | solution.py:95
  112.5 0.1 convert_reduce_fusion.2
  112.8 30.1 %all-gather.1 = bf16[416,1024]{1,0:T(8,128)(2,1)S(1)} all-gather(bf16[104,1024]{1,0:T(8,128)(2,1)S(1)} %pad_maximum_fusion.2), channel_id=3, replica_groups=mesh['yh'=2,'yl'=2,'x'=4,'zh'=4,'zl'=4,'core'=2] {'zl'}, dimensions={0}, use_global_device_ids=true | all-gather | bytes 1064960 | tf_op jit(solution)/shard_map/all_gather | solution.py:99
  142.9 0.9 slice.49
  143.8 6.6 %collective-permute-start.5 = (bf16[384,1024]{1,0:T(8,128)(2,1)}, bf16[384,1024]{1,0:T(8,128)(2,1)}, u32[]{:S(2)}, u32[]{:S(2)}) collective-permute-start(bf16[384,1024]{1,0:T(8,128)(2,1)} %bitcast.14), channel_id=1, source_target_pairs={{0,1},{1,0},{2,3},{3,2},{4,5},{5,4},{6,7},{7,6},{8,9},{9,8},{10,11... | collective-permute-start | bytes 2359304 | tf_op jit(solution)/shard_map/ppermute | solution.py:25
  150.4 0.0 all-to-all-done.3
  150.4 0.1 convert_reduce_fusion
  150.5 0.0 copy-start.4
  150.5 0.6 copy-done.4
  151.2 0.1 multiply_reduce_fusion
  151.3 0.6 broadcast_in_dim.8
  151.9 6.2 %all-to-all-start.4 = ((f32[16,1,256]{2,1,0:T(1,128)}), f32[16,1,256]{2,1,0:T(1,128)S(1)}, u32[]{:S(2)}, u32[]{:S(2)}) async-start(f32[16,1,256]{2,1,0:T(1,128)} %broadcast_in_dim.8), calls=%async_computation.4 | async-start | bytes 32768 | tf_op jit(solution)/shard_map/all_to_all | solution.py:16
  158.1 2.2 %collective-permute-start.6 = (f32[128]{0:T(128)S(1)}, f32[128]{0:T(128)S(1)}, u32[]{:S(2)}, u32[]{:S(2)}) collective-permute-start(f32[128]{0:T(128)S(1)} %fusion.18), channel_id=1, source_target_pairs={{0,1},{1,0},{2,3},{3,2},{4,5},{5,4},{6,7},{7,6},{8,9},{9,8},{10,11... | collective-permute-start | bytes 1544 | tf_op jit(solution)/shard_map/ppermute | solution.py:25
  160.3 4.2 %all-to-all-done.4 = f32[16,1,256]{2,1,0:T(1,128)S(1)} async-done(((f32[16,1,256]{2,1,0:T(1,128)}), f32[16,1,256]{2,1,0:T(1,128)S(1)}, u32[]{:S(2)}, u32[]{:S(2)}) %all-to-all-start.4) | async-done | bytes 16416 | tf_op jit(solution)/shard_map/all_to_all | solution.py:16
  164.5 0.6 reduce_sum.69
  165.1 1.7 copy.26
  166.8 0.0 collective-permute-done.6
  166.8 0.5 add.62
  167.3 0.0 collective-permute-done.5
  167.3 1.5 broadcast_select_fusion.1
  168.8 1.2 pad_maximum_fusion
  (13 shorter events, 0.2 us)
Async XLA Ops:
  0.6 30.4 %copy-start = (bf16[384,2048]{1,0:T(8,128)(2,1)S(1)}, bf16[384,2048]{1,0:T(8,128)(2,1)}, u32[]{:S(2)}) copy-start(bf16[384,2048]{1,0:T(8,128)(2,1)} %param.7) | copy-start | bytes 4718596
  1.7 8.7 %copy-start.7 = (bf16[128,256]{1,0:T(8,128)(2,1)S(1)}, bf16[128,256]{1,0:T(8,128)(2,1)}, u32[]{:S(2)}) copy-start(bf16[128,256]{1,0:T(8,128)(2,1)} %param.8) | copy-start | bytes 196612
  2.8 22.1 %all-to-all-start = ((bf16[16,128,256]{2,1,0:T(8,128)(2,1)}), bf16[16,128,256]{2,1,0:T(8,128)(2,1)S(1)}, u32[]{:S(2)}, u32[]{:S(2)}) async-start(bf16[16,128,256]{2,1,0:T(8,128)(2,1)} %broadcast_in_dim.6), calls=%async_computation | async-start | bytes 2097152 | tf_op jit(solution)/shard_map/all_to_all | solution.py:16
  10.4 20.6 %copy-start.5 = (bf16[384,256]{1,0:T(8,128)(2,1)S(1)}, bf16[384,256]{1,0:T(8,128)(2,1)}, u32[]{:S(2)}) copy-start(bf16[384,256]{1,0:T(8,128)(2,1)} %param.6) | copy-start | bytes 589828
  10.4 12.6 %collective-permute-start = (bf16[128,256]{1,0:T(8,128)(2,1)S(1)}, bf16[128,256]{1,0:T(8,128)(2,1)S(1)}, u32[]{:S(2)}, u32[]{:S(2)}) collective-permute-start(bf16[128,256]{1,0:T(8,128)(2,1)S(1)} %copy-done.7), channel_id=1, source_target_pairs={{0,0},{1,256},{256,257},{257,1},{2,2},{3,258},{258,259},{259,3},{4... | collective-permute-start | bytes 196616 | tf_op jit(solution)/shard_map/ppermute | solution.py:81
  24.9 1.3 copy-start.3
  26.2 18.8 %all-to-all-start.1 = ((bf16[16,128,256]{2,1,0:T(8,128)(2,1)}), bf16[16,128,256]{2,1,0:T(8,128)(2,1)S(1)}, u32[]{:S(2)}, u32[]{:S(2)}) async-start(bf16[16,128,256]{2,1,0:T(8,128)(2,1)} %broadcast_in_dim.7), calls=%async_computation.1 | async-start | bytes 2097152 | tf_op jit(solution)/shard_map/all_to_all | solution.py:16
  31.0 7.1 %copy-start.1 = (bf16[384,2048]{1,0:T(8,128)(2,1)S(1)}, bf16[384,2048]{1,0:T(8,128)(2,1)}, u32[]{:S(2)}) copy-start(bf16[384,2048]{1,0:T(8,128)(2,1)} %param.5) | copy-start | bytes 4718596
  33.0 16.5 %collective-permute-start.1 = (bf16[384,256]{1,0:T(8,128)(2,1)S(1)}, bf16[384,256]{1,0:T(8,128)(2,1)S(1)}, u32[]{:S(2)}, u32[]{:S(2)}) collective-permute-start(bf16[384,256]{1,0:T(8,128)(2,1)S(1)} %fusion.2), channel_id=1, source_target_pairs={{0,1},{1,0},{2,3},{3,2},{4,5},{5,4},{6,7},{7,6},{8,9},{9,8},{10,11... | collective-permute-start | bytes 589832 | tf_op jit(solution)/shard_map/ppermute | solution.py:25
  45.0 28.5 %all-to-all-start.2 = ((bf16[16,256,128]{2,1,0:T(8,128)(2,1)}), bf16[16,256,128]{2,1,0:T(8,128)(2,1)}, u32[]{:S(2)}, u32[]{:S(2)}) async-start(bf16[16,256,128]{2,1,0:T(8,128)(2,1)} %bitcast.53), calls=%async_computation.2 | async-start | bytes 2097152 | tf_op jit(solution)/shard_map/all_to_all | solution.py:16
  49.9 14.2 %copy-start.6 = (bf16[384,256]{1,0:T(8,128)(2,1)S(1)}, bf16[384,256]{1,0:T(8,128)(2,1)}, u32[]{:S(2)}) copy-start(bf16[384,256]{1,0:T(8,128)(2,1)} %param.6) | copy-start | bytes 589828
  50.4 15.7 %collective-permute-start.2 = (bf16[96,1024]{1,0:T(8,128)(2,1)S(1)}, bf16[96,1024]{1,0:T(8,128)(2,1)S(1)}, u32[]{:S(2)}, u32[]{:S(2)}) collective-permute-start(bf16[96,1024]{1,0:T(8,128)(2,1)S(1)} %get-tuple-element.24), channel_id=1, source_target_pairs={{0,2},{2,4},{4,6},{6,0},{1,3},{3,5},{5,7},{7,1},{8,10},{10,12},{12... | collective-permute-start | bytes 589832 | tf_op jit(solution)/shard_map/ppermute | solution.py:44
  56.6 16.0 %collective-permute-start.4 = (bf16[96,1024]{1,0:T(8,128)(2,1)S(1)}, bf16[96,1024]{1,0:T(8,128)(2,1)S(1)}, u32[]{:S(2)}, u32[]{:S(2)}) collective-permute-start(bf16[96,1024]{1,0:T(8,128)(2,1)S(1)} %get-tuple-element.25), channel_id=1, source_target_pairs={{0,4},{2,6},{4,0},{6,2},{1,5},{3,7},{5,1},{7,3},{8,12},{10,14},{12... | collective-permute-start | bytes 589832 | tf_op jit(solution)/shard_map/ppermute | solution.py:44
  61.5 11.1 %collective-permute-start.3 = (bf16[96,1024]{1,0:T(8,128)(2,1)S(1)}, bf16[96,1024]{1,0:T(8,128)(2,1)}, u32[]{:S(2)}, u32[]{:S(2)}) collective-permute-start(bf16[96,1024]{1,0:T(8,128)(2,1)S(1)} %get-tuple-element.26), channel_id=1, source_target_pairs={{0,6},{2,0},{4,2},{6,4},{1,7},{3,1},{5,3},{7,5},{8,14},{10,8},{12,... | collective-permute-start | bytes 589832 | tf_op jit(solution)/shard_map/ppermute | solution.py:44
  73.6 76.8 %all-to-all-start.3 = ((bf16[16,256,128]{2,1,0:T(8,128)(2,1)}), bf16[16,256,128]{2,1,0:T(8,128)(2,1)S(1)}, u32[]{:S(2)}, u32[]{:S(2)}) async-start(bf16[16,256,128]{2,1,0:T(8,128)(2,1)} %bitcast.49), calls=%async_computation.3 | async-start | bytes 2097152 | tf_op jit(solution)/shard_map/all_to_all | solution.py:16
  81.5 0.6 copy-start.2
  143.8 23.5 %collective-permute-start.5 = (bf16[384,1024]{1,0:T(8,128)(2,1)}, bf16[384,1024]{1,0:T(8,128)(2,1)}, u32[]{:S(2)}, u32[]{:S(2)}) collective-permute-start(bf16[384,1024]{1,0:T(8,128)(2,1)} %bitcast.14), channel_id=1, source_target_pairs={{0,1},{1,0},{2,3},{3,2},{4,5},{5,4},{6,7},{7,6},{8,9},{9,8},{10,11... | collective-permute-start | bytes 2359304 | tf_op jit(solution)/shard_map/ppermute | solution.py:25
  150.5 0.7 copy-start.4
  151.9 12.6 %all-to-all-start.4 = ((f32[16,1,256]{2,1,0:T(1,128)}), f32[16,1,256]{2,1,0:T(1,128)S(1)}, u32[]{:S(2)}, u32[]{:S(2)}) async-start(f32[16,1,256]{2,1,0:T(1,128)} %broadcast_in_dim.8), calls=%async_computation.4 | async-start | bytes 32768 | tf_op jit(solution)/shard_map/all_to_all | solution.py:16
  158.1 8.6 %collective-permute-start.6 = (f32[128]{0:T(128)S(1)}, f32[128]{0:T(128)S(1)}, u32[]{:S(2)}, u32[]{:S(2)}) collective-permute-start(f32[128]{0:T(128)S(1)} %fusion.18), channel_id=1, source_target_pairs={{0,1},{1,0},{2,3},{3,2},{4,5},{5,4},{6,7},{7,6},{8,9},{9,8},{10,11... | collective-permute-start | bytes 1544 | tf_op jit(solution)/shard_map/ppermute | solution.py:25

commit v11 on v10

--- a/solution.py
+++ b/solution.py
@@ -57,21 +57,26 @@
     return jnp.sum(exchange(blocks, FS).astype(F32), axis=0)
 
 
-def with_row(array, values):
-    high = lax.reduce_precision(values, 8, 7)
-    row = jnp.concatenate([high, values - high]).astype(BF)[None]
-    return jnp.concatenate(
-        [array, jnp.pad(row, ((0, EXTRA - 1), (0, array.shape[1] - row.shape[1])))], axis=0
-    )
+def tile_rows(array):
+    rows, columns = array.shape
+    tiles = array.reshape(rows // 8, 8, columns // 128, 128)
+    return jnp.swapaxes(tiles, 1, 2).reshape(-1, 128)
 
 
-def without_row(array):
-    row = array[..., -EXTRA, :]
-    return array[..., :-EXTRA, :], row[..., :128] + row[..., 128:256]
+def from_tile_rows(tiles, columns):
+    count = tiles.shape[0]
+    tiles = tiles.reshape(count, -1, columns // 128, 8, 128)
+    return jnp.swapaxes(tiles, 2, 3).reshape(-1, columns)
+
+
+def with_row(tiles, values):
+    high = lax.reduce_precision(values, 8, 7)
+    rows = jnp.stack([high, values - high]).astype(BF)
+    return jnp.concatenate([tiles, jnp.pad(rows, ((0, EXTRA - 2), (0, 0)))], axis=0)
 
 
 def local(inputs, pre_act, cotangent, up_weight, down_weight):
-    tokens, width = inputs.shape
+    _, width = inputs.shape
     hidden = pre_act.shape[1]
     core = lax.axis_index("core")
     active = jnp.maximum(pre_act.astype(F32), 0.0)
@@ -90,16 +95,17 @@
     down_part = in_blocks(dot(squared, cotangent, (0, 0)).astype(BF))
     down_grad = sum_at_owner(down_part)
 
-    quarter = sum_near(half, "zl")
+    quarter = tile_rows(sum_near(half, "zl"))
     quarter = with_row(quarter, jnp.sum(up_grad * up_grad, axis=0))
     groups = lax.all_gather(quarter, "zh", axis=0, tiled=False)
-    quarter, squares = without_row(jnp.sum(groups.astype(F32), axis=0))
-    quarter = with_row(quarter.astype(BF), squares)
+    quarter = jnp.sum(groups.astype(F32), axis=0)
+    squares = quarter[-EXTRA] + quarter[1 - EXTRA]
+    quarter = with_row(quarter[:-EXTRA].astype(BF), squares)
     down_norms = from_everyone(jnp.sum(down_grad * down_grad, axis=1), FS)
     half = lax.all_gather(quarter, "zl", axis=0, tiled=False)
-    row = half[:, -EXTRA].astype(F32)
-    up_norms = jnp.sum(row[:, :128] + row[:, 128:256], axis=0)
-    half = half[:, :-EXTRA].reshape(tokens, width // 2)
+    rows = half[:, -EXTRA : 2 - EXTRA].astype(F32)
+    up_norms = jnp.sum(rows, axis=(0, 1))
+    half = from_tile_rows(half[:, :-EXTRA], width // 2)
     both = other_core(half)
     up_norms += other_core(up_norms)
     input_grad = jnp.concatenate(

time: 171 us -> 166 us (0.971)
  blocking collectives: 60.5 us -> 57.3 us
    all_gather x1, blocking collectives: 30.1 us -> 28.2 us  [local(): half = lax.all_gather(quarter, 'zl', axis=0, tiled=False)]
  transfers between devices with their start and end apart: 12 -> 12, of which waited for: 5 -> 5; matrix products, arithmetic and copies ran while one was open for 8% -> 7% of each run, Pallas kernels for 0% -> 0%
where the time goes in v11:
time: 166 us; the launch traced here: 165 us
  starting transfers between devices  65.8 us (40%)
  blocking collectives  57.3 us (35%)
  waiting for transfers between devices  22.1 us (13%)
  local copies, waits for them, and re-layouts  9.08 us (5%)
  other arithmetic  5.85 us (4%)
  matrix products  4.18 us (3%)
    all_to_all x5, starting transfers between devices, exchange(): return lax.all_to_all(array, axes, 0, 0, tiled=True)  30.7 us
    all_gather x1, blocking collectives, local(): groups = lax.all_gather(quarter, 'zh', axis=0, tiled=False)  29.1 us
    all_gather x1, blocking collectives, local(): half = lax.all_gather(quarter, 'zl', axis=0, tiled=False)  28.2 us
    ppermute x3, starting transfers between devices, sum_near(): others.append(lax.ppermute(piece, axis, ring))  13.7 us
    ppermute x3, starting transfers between devices, other_core(): return lax.ppermute(array, 'core', [(0, 1), (1, 0)])  13.5 us
    all_to_all x5, waiting for transfers between devices, exchange(): return lax.all_to_all(array, axes, 0, 0, tiled=True)  11.1 us
    ppermute x1, starting transfers between devices, local(): lax.ppermute(up_weight, ('yh', 'core'), [(0, 0), (1, 2), (2, 3), (3, 1)])  7.92 us
    ppermute x3, waiting for transfers between devices, sum_near(): others.append(lax.ppermute(piece, axis, ring))  6.43 us
  transfers between devices with their start and end apart: 12, of which 5 were waited for; matrix products, arithmetic and copies ran while one was open for 7% of the time, Pallas kernels for 0%

profile of v11, /device:TPU:1, one launch (start us, length us, event | category | flops | bytes accessed | tf_op | source)
XLA Modules:
  0.0 165.3 jit_solution(13959066629125496293)
XLA Ops:
  0.6 0.0 copy-start
  0.6 1.1 copy.21
  1.7 0.0 copy-start.6
  1.7 1.1 broadcast_in_dim.6
  2.8 7.6 %all-to-all-start = ((bf16[16,128,256]{2,1,0:T(8,128)(2,1)}), bf16[16,128,256]{2,1,0:T(8,128)(2,1)S(1)}, u32[]{:S(2)}, u32[]{:S(2)}) async-start(bf16[16,128,256]{2,1,0:T(8,128)(2,1)} %broadcast_in_dim.6), calls=%async_computation | async-start | bytes 2097152 | tf_op jit(solution)/shard_map/all_to_all | solution.py:16
  10.4 0.0 copy-done.6
  10.4 0.0 copy-start.4
  10.4 7.9 %collective-permute-start = (bf16[128,256]{1,0:T(8,128)(2,1)S(1)}, bf16[128,256]{1,0:T(8,128)(2,1)S(1)}, u32[]{:S(2)}, u32[]{:S(2)}) collective-permute-start(bf16[128,256]{1,0:T(8,128)(2,1)S(1)} %copy-done.6), channel_id=1, source_target_pairs={{0,0},{1,256},{256,257},{257,1},{2,2},{3,258},{258,259},{259,3},{4... | collective-permute-start | bytes 196616 | tf_op jit(solution)/shard_map/ppermute | solution.py:86
  18.3 4.6 %collective-permute-done = bf16[128,256]{1,0:T(8,128)(2,1)S(1)} collective-permute-done((bf16[128,256]{1,0:T(8,128)(2,1)S(1)}, bf16[128,256]{1,0:T(8,128)(2,1)S(1)}, u32[]{:S(2)}, u32[]{:S(2)}) %collective-permute-start) | collective-permute-done | bytes 65568 | tf_op jit(solution)/shard_map/ppermute | solution.py:86
  23.0 1.9 %all-to-all-done = bf16[16,128,256]{2,1,0:T(8,128)(2,1)S(1)} async-done(((bf16[16,128,256]{2,1,0:T(8,128)(2,1)}), bf16[16,128,256]{2,1,0:T(8,128)(2,1)S(1)}, u32[]{:S(2)}, u32[]{:S(2)}) %all-to-all-start) | async-done | bytes 1048608 | tf_op jit(solution)/shard_map/all_to_all | solution.py:16
  24.9 0.0 copy-start.2
  24.9 1.2 broadcast_in_dim.7
  26.1 0.2 copy-done.2
  26.2 4.7 %all-to-all-start.1 = ((bf16[16,128,256]{2,1,0:T(8,128)(2,1)}), bf16[16,128,256]{2,1,0:T(8,128)(2,1)S(1)}, u32[]{:S(2)}, u32[]{:S(2)}) async-start(bf16[16,128,256]{2,1,0:T(8,128)(2,1)} %broadcast_in_dim.7), calls=%async_computation.1 | async-start | bytes 2097152 | tf_op jit(solution)/shard_map/all_to_all | solution.py:16
  31.0 0.0 copy-done
  31.0 0.0 copy-done.4
  31.0 0.0 copy-start.1
  31.0 1.9 %fusion.2 = bf16[384,256]{1,0:T(8,128)(2,1)S(1)} fusion(bf16[384,2048]{1,0:T(8,128)(2,1)S(1)} %copy-done, bf16[2048,256]{1,0:T(8,128)(2,1)} %bitcast.65, bf16[384,256]{1,0:T(8,128)(2,1)S(1)} %copy-done.4), kind=kOutput, calls=%fused_computation.10 | convolution fusion | flops 403144704 | bytes 3014656 | tf_op jit(solution)/shard_map/dot_general | solution.py:29
  33.0 5.2 %collective-permute-start.1 = (bf16[384,256]{1,0:T(8,128)(2,1)S(1)}, bf16[384,256]{1,0:T(8,128)(2,1)S(1)}, u32[]{:S(2)}, u32[]{:S(2)}) collective-permute-start(bf16[384,256]{1,0:T(8,128)(2,1)S(1)} %fusion.2), channel_id=1, source_target_pairs={{0,1},{1,0},{2,3},{3,2},{4,5},{5,4},{6,7},{7,6},{8,9},{9,8},{10,11... | collective-permute-start | bytes 589832 | tf_op jit(solution)/shard_map/ppermute | solution.py:25
  38.1 0.0 copy-done.1
  38.2 0.7 fusion
  38.9 1.2 copy.34
  40.1 4.9 %all-to-all-done.1 = bf16[16,128,256]{2,1,0:T(8,128)(2,1)S(1)} async-done(((bf16[16,128,256]{2,1,0:T(8,128)(2,1)}), bf16[16,128,256]{2,1,0:T(8,128)(2,1)S(1)}, u32[]{:S(2)}, u32[]{:S(2)}) %all-to-all-start.1) | async-done | bytes 1048608 | tf_op jit(solution)/shard_map/all_to_all | solution.py:16
  45.0 4.3 %all-to-all-start.2 = ((bf16[16,256,128]{2,1,0:T(8,128)(2,1)}), bf16[16,256,128]{2,1,0:T(8,128)(2,1)}, u32[]{:S(2)}, u32[]{:S(2)}) async-start(bf16[16,256,128]{2,1,0:T(8,128)(2,1)} %bitcast.56), calls=%async_computation.2 | async-start | bytes 2097152 | tf_op jit(solution)/shard_map/all_to_all | solution.py:16
  49.4 0.1 fusion.16
  49.5 0.0 collective-permute-done.1
  49.5 0.4 fusion.17
  49.9 0.0 copy-start.5
  49.9 0.4 add_convert_fusion
  50.3 0.1 dynamic-slice_bitcast_fusion.2
  50.4 6.2 %collective-permute-start.2 = (bf16[96,1024]{1,0:T(8,128)(2,1)S(1)}, bf16[96,1024]{1,0:T(8,128)(2,1)S(1)}, u32[]{:S(2)}, u32[]{:S(2)}) collective-permute-start(bf16[96,1024]{1,0:T(8,128)(2,1)S(1)} %get-tuple-element.24), channel_id=1, source_target_pairs={{0,2},{2,4},{4,6},{6,0},{1,3},{3,5},{5,7},{7,1},{8,10},{10,12},{12... | collective-permute-start | bytes 589832 | tf_op jit(solution)/shard_map/ppermute | solution.py:44
  56.6 4.9 %collective-permute-start.4 = (bf16[96,1024]{1,0:T(8,128)(2,1)S(1)}, bf16[96,1024]{1,0:T(8,128)(2,1)S(1)}, u32[]{:S(2)}, u32[]{:S(2)}) collective-permute-start(bf16[96,1024]{1,0:T(8,128)(2,1)S(1)} %get-tuple-element.25), channel_id=1, source_target_pairs={{0,4},{2,6},{4,0},{6,2},{1,5},{3,7},{5,1},{7,3},{8,12},{10,14},{12... | collective-permute-start | bytes 589832 | tf_op jit(solution)/shard_map/ppermute | solution.py:44
  61.5 2.6 %collective-permute-start.3 = (bf16[96,1024]{1,0:T(8,128)(2,1)S(1)}, bf16[96,1024]{1,0:T(8,128)(2,1)S(1)}, u32[]{:S(2)}, u32[]{:S(2)}) collective-permute-start(bf16[96,1024]{1,0:T(8,128)(2,1)S(1)} %get-tuple-element.26), channel_id=1, source_target_pairs={{0,6},{2,0},{4,2},{6,4},{1,7},{3,1},{5,3},{7,5},{8,14},{10,8},{12,... | collective-permute-start | bytes 589832 | tf_op jit(solution)/shard_map/ppermute | solution.py:44
  64.1 0.0 copy-done.5
  64.1 0.7 fusion.1
  64.9 1.2 copy.33
  66.1 0.0 collective-permute-done.2
  66.1 6.4 %collective-permute-done.4 = bf16[96,1024]{1,0:T(8,128)(2,1)S(1)} collective-permute-done((bf16[96,1024]{1,0:T(8,128)(2,1)S(1)}, bf16[96,1024]{1,0:T(8,128)(2,1)S(1)}, u32[]{:S(2)}, u32[]{:S(2)}) %collective-permute-start.4) | collective-permute-done | bytes 196640 | tf_op jit(solution)/shard_map/ppermute | solution.py:44
  72.5 0.0 collective-permute-done.3
  72.5 0.1 fusion.5
  72.7 0.0 all-to-all-done.2
  72.7 6.5 %all-to-all-start.3 = ((bf16[16,256,128]{2,1,0:T(8,128)(2,1)}), bf16[16,256,128]{2,1,0:T(8,128)(2,1)S(1)}, u32[]{:S(2)}, u32[]{:S(2)}) async-start(bf16[16,256,128]{2,1,0:T(8,128)(2,1)} %bitcast.53), calls=%async_computation.3 | async-start | bytes 2097152 | tf_op jit(solution)/shard_map/all_to_all | solution.py:16
  79.2 1.4 convert_reduce_fusion.1
  80.7 29.1 %all-gather = bf16[3104,128]{1,0:T(8,128)(2,1)S(1)} all-gather(bf16[776,128]{1,0:T(8,128)(2,1)S(1)} %pad_maximum_fusion.1), channel_id=2, replica_groups=mesh['yh'=2,'yl'=2,'x'=4,'zh'=4,'zl'=4,'core'=2] {'zh'}, dimensions={0}, use_global_device_ids=true | all-gather | bytes 993280 | tf_op jit(solution)/shard_map/all_gather | solution.py:100
  109.8 0.1 convert_reduce_fusion.2
  110.0 28.2 %all-gather.1 = bf16[3104,128]{1,0:T(8,128)(2,1)S(1)} all-gather(bf16[776,128]{1,0:T(8,128)(2,1)S(1)} %pad_maximum_fusion.2), channel_id=3, replica_groups=mesh['yh'=2,'yl'=2,'x'=4,'zh'=4,'zl'=4,'core'=2] {'zl'}, dimensions={0}, use_global_device_ids=true | all-gather | bytes 993280 | tf_op jit(solution)/shard_map/all_gather | solution.py:105
  138.1 0.9 slice.36
  139.1 6.1 %collective-permute-start.5 = (bf16[384,1024]{1,0:T(8,128)(2,1)}, bf16[384,1024]{1,0:T(8,128)(2,1)}, u32[]{:S(2)}, u32[]{:S(2)}) collective-permute-start(bf16[384,1024]{1,0:T(8,128)(2,1)} %bitcast.18), channel_id=1, source_target_pairs={{0,1},{1,0},{2,3},{3,2},{4,5},{5,4},{6,7},{7,6},{8,9},{9,8},{10,11... | collective-permute-start | bytes 2359304 | tf_op jit(solution)/shard_map/ppermute | solution.py:25
  145.2 0.0 all-to-all-done.3
  145.2 0.1 convert_reduce_fusion
  145.4 0.0 copy-start.3
  145.4 0.6 copy-done.3
  146.0 0.1 multiply_reduce_fusion
  146.1 0.6 broadcast_in_dim.8
  146.7 7.5 %all-to-all-start.4 = ((f32[16,1,256]{2,1,0:T(1,128)}), f32[16,1,256]{2,1,0:T(1,128)S(1)}, u32[]{:S(2)}, u32[]{:S(2)}) async-start(f32[16,1,256]{2,1,0:T(1,128)} %broadcast_in_dim.8), calls=%async_computation.4 | async-start | bytes 32768 | tf_op jit(solution)/shard_map/all_to_all | solution.py:16
  154.3 2.2 %collective-permute-start.6 = (f32[128]{0:T(128)S(1)}, f32[128]{0:T(128)S(1)}, u32[]{:S(2)}, u32[]{:S(2)}) collective-permute-start(f32[128]{0:T(128)S(1)} %convert_reduce_fusion.3), channel_id=1, source_target_pairs={{0,1},{1,0},{2,3},{3,2},{4,5},{5,4},{6,7},{7,6},{8,9},{9,8},{10,11... | collective-permute-start | bytes 1544 | tf_op jit(solution)/shard_map/ppermute | solution.py:25
  156.5 4.2 %all-to-all-done.4 = f32[16,1,256]{2,1,0:T(1,128)S(1)} async-done(((f32[16,1,256]{2,1,0:T(1,128)}), f32[16,1,256]{2,1,0:T(1,128)S(1)}, u32[]{:S(2)}, u32[]{:S(2)}) %all-to-all-start.4) | async-done | bytes 16416 | tf_op jit(solution)/shard_map/all_to_all | solution.py:16
  160.7 0.6 reduce_sum.72
  161.3 0.8 copy.26
  162.1 0.0 collective-permute-done.6
  162.1 0.5 add.58
  162.6 0.0 collective-permute-done.5
  162.6 1.5 broadcast_select_fusion.1
  164.1 1.2 pad_maximum_fusion
  (9 shorter events, 0.2 us)
Async XLA Ops:
  0.6 30.4 %copy-start = (bf16[384,2048]{1,0:T(8,128)(2,1)S(1)}, bf16[384,2048]{1,0:T(8,128)(2,1)}, u32[]{:S(2)}) copy-start(bf16[384,2048]{1,0:T(8,128)(2,1)} %param.7) | copy-start | bytes 4718596
  1.7 8.7 %copy-start.6 = (bf16[128,256]{1,0:T(8,128)(2,1)S(1)}, bf16[128,256]{1,0:T(8,128)(2,1)}, u32[]{:S(2)}) copy-start(bf16[128,256]{1,0:T(8,128)(2,1)} %param.8) | copy-start | bytes 196612
  2.8 22.1 %all-to-all-start = ((bf16[16,128,256]{2,1,0:T(8,128)(2,1)}), bf16[16,128,256]{2,1,0:T(8,128)(2,1)S(1)}, u32[]{:S(2)}, u32[]{:S(2)}) async-start(bf16[16,128,256]{2,1,0:T(8,128)(2,1)} %broadcast_in_dim.6), calls=%async_computation | async-start | bytes 2097152 | tf_op jit(solution)/shard_map/all_to_all | solution.py:16
  10.4 20.6 %copy-start.4 = (bf16[384,256]{1,0:T(8,128)(2,1)S(1)}, bf16[384,256]{1,0:T(8,128)(2,1)}, u32[]{:S(2)}) copy-start(bf16[384,256]{1,0:T(8,128)(2,1)} %param.6) | copy-start | bytes 589828
  10.4 12.6 %collective-permute-start = (bf16[128,256]{1,0:T(8,128)(2,1)S(1)}, bf16[128,256]{1,0:T(8,128)(2,1)S(1)}, u32[]{:S(2)}, u32[]{:S(2)}) collective-permute-start(bf16[128,256]{1,0:T(8,128)(2,1)S(1)} %copy-done.6), channel_id=1, source_target_pairs={{0,0},{1,256},{256,257},{257,1},{2,2},{3,258},{258,259},{259,3},{4... | collective-permute-start | bytes 196616 | tf_op jit(solution)/shard_map/ppermute | solution.py:86
  24.9 1.3 copy-start.2
  26.2 18.8 %all-to-all-start.1 = ((bf16[16,128,256]{2,1,0:T(8,128)(2,1)}), bf16[16,128,256]{2,1,0:T(8,128)(2,1)S(1)}, u32[]{:S(2)}, u32[]{:S(2)}) async-start(bf16[16,128,256]{2,1,0:T(8,128)(2,1)} %broadcast_in_dim.7), calls=%async_computation.1 | async-start | bytes 2097152 | tf_op jit(solution)/shard_map/all_to_all | solution.py:16
  31.0 7.1 %copy-start.1 = (bf16[384,2048]{1,0:T(8,128)(2,1)S(1)}, bf16[384,2048]{1,0:T(8,128)(2,1)}, u32[]{:S(2)}) copy-start(bf16[384,2048]{1,0:T(8,128)(2,1)} %param.5) | copy-start | bytes 4718596
  33.0 16.5 %collective-permute-start.1 = (bf16[384,256]{1,0:T(8,128)(2,1)S(1)}, bf16[384,256]{1,0:T(8,128)(2,1)S(1)}, u32[]{:S(2)}, u32[]{:S(2)}) collective-permute-start(bf16[384,256]{1,0:T(8,128)(2,1)S(1)} %fusion.2), channel_id=1, source_target_pairs={{0,1},{1,0},{2,3},{3,2},{4,5},{5,4},{6,7},{7,6},{8,9},{9,8},{10,11... | collective-permute-start | bytes 589832 | tf_op jit(solution)/shard_map/ppermute | solution.py:25
  45.0 27.6 %all-to-all-start.2 = ((bf16[16,256,128]{2,1,0:T(8,128)(2,1)}), bf16[16,256,128]{2,1,0:T(8,128)(2,1)}, u32[]{:S(2)}, u32[]{:S(2)}) async-start(bf16[16,256,128]{2,1,0:T(8,128)(2,1)} %bitcast.56), calls=%async_computation.2 | async-start | bytes 2097152 | tf_op jit(solution)/shard_map/all_to_all | solution.py:16
  49.9 14.2 %copy-start.5 = (bf16[384,256]{1,0:T(8,128)(2,1)S(1)}, bf16[384,256]{1,0:T(8,128)(2,1)}, u32[]{:S(2)}) copy-start(bf16[384,256]{1,0:T(8,128)(2,1)} %param.6) | copy-start | bytes 589828
  50.4 15.7 %collective-permute-start.2 = (bf16[96,1024]{1,0:T(8,128)(2,1)S(1)}, bf16[96,1024]{1,0:T(8,128)(2,1)S(1)}, u32[]{:S(2)}, u32[]{:S(2)}) collective-permute-start(bf16[96,1024]{1,0:T(8,128)(2,1)S(1)} %get-tuple-element.24), channel_id=1, source_target_pairs={{0,2},{2,4},{4,6},{6,0},{1,3},{3,5},{5,7},{7,1},{8,10},{10,12},{12... | collective-permute-start | bytes 589832 | tf_op jit(solution)/shard_map/ppermute | solution.py:44
  56.6 16.0 %collective-permute-start.4 = (bf16[96,1024]{1,0:T(8,128)(2,1)S(1)}, bf16[96,1024]{1,0:T(8,128)(2,1)S(1)}, u32[]{:S(2)}, u32[]{:S(2)}) collective-permute-start(bf16[96,1024]{1,0:T(8,128)(2,1)S(1)} %get-tuple-element.25), channel_id=1, source_target_pairs={{0,4},{2,6},{4,0},{6,2},{1,5},{3,7},{5,1},{7,3},{8,12},{10,14},{12... | collective-permute-start | bytes 589832 | tf_op jit(solution)/shard_map/ppermute | solution.py:44
  61.5 11.1 %collective-permute-start.3 = (bf16[96,1024]{1,0:T(8,128)(2,1)S(1)}, bf16[96,1024]{1,0:T(8,128)(2,1)S(1)}, u32[]{:S(2)}, u32[]{:S(2)}) collective-permute-start(bf16[96,1024]{1,0:T(8,128)(2,1)S(1)} %get-tuple-element.26), channel_id=1, source_target_pairs={{0,6},{2,0},{4,2},{6,4},{1,7},{3,1},{5,3},{7,5},{8,14},{10,8},{12,... | collective-permute-start | bytes 589832 | tf_op jit(solution)/shard_map/ppermute | solution.py:44
  72.7 72.5 %all-to-all-start.3 = ((bf16[16,256,128]{2,1,0:T(8,128)(2,1)}), bf16[16,256,128]{2,1,0:T(8,128)(2,1)S(1)}, u32[]{:S(2)}, u32[]{:S(2)}) async-start(bf16[16,256,128]{2,1,0:T(8,128)(2,1)} %bitcast.53), calls=%async_computation.3 | async-start | bytes 2097152 | tf_op jit(solution)/shard_map/all_to_all | solution.py:16
  139.1 23.5 %collective-permute-start.5 = (bf16[384,1024]{1,0:T(8,128)(2,1)}, bf16[384,1024]{1,0:T(8,128)(2,1)}, u32[]{:S(2)}, u32[]{:S(2)}) collective-permute-start(bf16[384,1024]{1,0:T(8,128)(2,1)} %bitcast.18), channel_id=1, source_target_pairs={{0,1},{1,0},{2,3},{3,2},{4,5},{5,4},{6,7},{7,6},{8,9},{9,8},{10,11... | collective-permute-start | bytes 2359304 | tf_op jit(solution)/shard_map/ppermute | solution.py:25
  145.4 0.7 copy-start.3
  146.7 14.0 %all-to-all-start.4 = ((f32[16,1,256]{2,1,0:T(1,128)}), f32[16,1,256]{2,1,0:T(1,128)S(1)}, u32[]{:S(2)}, u32[]{:S(2)}) async-start(f32[16,1,256]{2,1,0:T(1,128)} %broadcast_in_dim.8), calls=%async_computation.4 | async-start | bytes 32768 | tf_op jit(solution)/shard_map/all_to_all | solution.py:16
  154.3 7.8 %collective-permute-start.6 = (f32[128]{0:T(128)S(1)}, f32[128]{0:T(128)S(1)}, u32[]{:S(2)}, u32[]{:S(2)}) collective-permute-start(f32[128]{0:T(128)S(1)} %convert_reduce_fusion.3), channel_id=1, source_target_pairs={{0,1},{1,0},{2,3},{3,2},{4,5},{5,4},{6,7},{7,6},{8,9},{9,8},{10,11... | collective-permute-start | bytes 1544 | tf_op jit(solution)/shard_map/ppermute | solution.py:25

commit v12 on v11

--- a/solution.py
+++ b/solution.py
@@ -37,7 +37,7 @@
     pieces = half.reshape(count, half.shape[0] // count, half.shape[1])
     total = lax.dynamic_index_in_dim(pieces, here, 0, False).astype(F32)
     others = []
-    for step in (1, 3, 2):
+    for step in (2, 1, 3):
         there = lax.rem(here + step, count)
         piece = lax.dynamic_index_in_dim(pieces, there, 0, False)
         ring = [(i, (i + step) % count) for i in range(count)]
@@ -102,15 +102,15 @@
     squares = quarter[-EXTRA] + quarter[1 - EXTRA]
     quarter = with_row(quarter[:-EXTRA].astype(BF), squares)
     down_norms = from_everyone(jnp.sum(down_grad * down_grad, axis=1), FS)
-    half = lax.all_gather(quarter, "zl", axis=0, tiled=False)
-    rows = half[:, -EXTRA : 2 - EXTRA].astype(F32)
-    up_norms = jnp.sum(rows, axis=(0, 1))
-    half = from_tile_rows(half[:, :-EXTRA], width // 2)
+    half = lax.all_gather(quarter, "zl", axis=0, tiled=True)
     both = other_core(half)
-    up_norms += other_core(up_norms)
-    input_grad = jnp.concatenate(
-        [jnp.where(core == 0, half, both), jnp.where(core == 0, both, half)], axis=1
-    )
+    half, both = (each.reshape(4, -1, 128) for each in (half, both))
+    rows = [each[:, -EXTRA : 2 - EXTRA].astype(F32) for each in (half, both)]
+    up_norms = jnp.sum(rows[0] + rows[1], axis=(0, 1))
+    half, both = (each[:, :-EXTRA] for each in (half, both))
+    first = from_tile_rows(jnp.where(core == 0, half, both), width // 2)
+    second = from_tile_rows(jnp.where(core == 0, both, half), width // 2)
+    input_grad = jnp.concatenate([first, second], axis=1)
     down_norms = jnp.sum(down_norms, axis=0)
     return input_grad, up_grad.T, down_grad, up_norms, down_norms
 

time: 166 us -> 166 us (level)
  waiting for transfers between devices: 22.1 us -> 23.8 us
    all_gather x1, blocking collectives: 28.2 us -> 16.6 us  [local(): half = lax.all_gather(quarter, 'zl', axis=0, tiled=True)]
    all_gather x1, blocking collectives: 29.1 us -> 39.2 us  [local(): groups = lax.all_gather(quarter, 'zh', axis=0, tiled=False)]
    all_to_all x5, waiting for transfers between devices: 11.1 us -> 13.3 us  [exchange(): return lax.all_to_all(array, axes, 0, 0, tiled=True)]
    ppermute x3 -> x2, starting transfers between devices: 13.5 us -> 13.4 us  [other_core(): return lax.ppermute(array, 'core', [(0, 1), (1, 0)])]
  transfers between devices with their start and end apart: 12 -> 11, of which waited for: 5 -> 6; matrix products, arithmetic and copies ran while one was open for 7% -> 7% of each run, Pallas kernels for 0% -> 0%
where the time goes in v12:
time: 166 us; the launch traced here: 165 us
  starting transfers between devices  65.7 us (40%)
  blocking collectives  55.8 us (34%)
  waiting for transfers between devices  23.8 us (14%)
  local copies, waits for them, and re-layouts  8.15 us (5%)
  other arithmetic  6.3 us (4%)
  matrix products  4.18 us (3%)
    all_gather x1, blocking collectives, local(): groups = lax.all_gather(quarter, 'zh', axis=0, tiled=False)  39.2 us
    all_to_all x5, starting transfers between devices, exchange(): return lax.all_to_all(array, axes, 0, 0, tiled=True)  31.4 us
    all_gather x1, blocking collectives, local(): half = lax.all_gather(quarter, 'zl', axis=0, tiled=True)  16.6 us
    ppermute x2, starting transfers between devices, other_core(): return lax.ppermute(array, 'core', [(0, 1), (1, 0)])  13.4 us
    all_to_all x5, waiting for transfers between devices, exchange(): return lax.all_to_all(array, axes, 0, 0, tiled=True)  13.3 us
    ppermute x3, starting transfers between devices, sum_near(): others.append(lax.ppermute(piece, axis, ring))  13 us
    ppermute x1, starting transfers between devices, local(): lax.ppermute(up_weight, ('yh', 'core'), [(0, 0), (1, 2), (2, 3), (3, 1)])  7.92 us
    ppermute x3, waiting for transfers between devices, sum_near(): others.append(lax.ppermute(piece, axis, ring))  5.81 us
  transfers between devices with their start and end apart: 11, of which 6 were waited for; matrix products, arithmetic and copies ran while one was open for 7% of the time, Pallas kernels for 0%

profile of v12, /device:TPU:1, one launch (start us, length us, event | category | flops | bytes accessed | tf_op | source)
XLA Modules:
  0.0 164.8 jit_solution(16883364341522284598)
XLA Ops:
  0.6 0.0 copy-start
  0.6 1.1 copy.21
  1.7 0.0 copy-start.6
  1.7 1.1 broadcast_in_dim.6
  2.8 7.6 %all-to-all-start = ((bf16[16,128,256]{2,1,0:T(8,128)(2,1)}), bf16[16,128,256]{2,1,0:T(8,128)(2,1)S(1)}, u32[]{:S(2)}, u32[]{:S(2)}) async-start(bf16[16,128,256]{2,1,0:T(8,128)(2,1)} %broadcast_in_dim.6), calls=%async_computation | async-start | bytes 2097152 | tf_op jit(solution)/shard_map/all_to_all | solution.py:16
  10.4 0.0 copy-done.6
  10.4 0.0 copy-start.4
  10.4 7.9 %collective-permute-start = (bf16[128,256]{1,0:T(8,128)(2,1)S(1)}, bf16[128,256]{1,0:T(8,128)(2,1)S(1)}, u32[]{:S(2)}, u32[]{:S(2)}) collective-permute-start(bf16[128,256]{1,0:T(8,128)(2,1)S(1)} %copy-done.6), channel_id=1, source_target_pairs={{0,0},{1,256},{256,257},{257,1},{2,2},{3,258},{258,259},{259,3},{4... | collective-permute-start | bytes 196616 | tf_op jit(solution)/shard_map/ppermute | solution.py:86
  18.3 4.6 %collective-permute-done = bf16[128,256]{1,0:T(8,128)(2,1)S(1)} collective-permute-done((bf16[128,256]{1,0:T(8,128)(2,1)S(1)}, bf16[128,256]{1,0:T(8,128)(2,1)S(1)}, u32[]{:S(2)}, u32[]{:S(2)}) %collective-permute-start) | collective-permute-done | bytes 65568 | tf_op jit(solution)/shard_map/ppermute | solution.py:86
  23.0 1.9 %all-to-all-done = bf16[16,128,256]{2,1,0:T(8,128)(2,1)S(1)} async-done(((bf16[16,128,256]{2,1,0:T(8,128)(2,1)}), bf16[16,128,256]{2,1,0:T(8,128)(2,1)S(1)}, u32[]{:S(2)}, u32[]{:S(2)}) %all-to-all-start) | async-done | bytes 1048608 | tf_op jit(solution)/shard_map/all_to_all | solution.py:16
  24.9 0.0 copy-start.2
  24.9 1.2 broadcast_in_dim.7
  26.1 0.2 copy-done.2
  26.2 4.7 %all-to-all-start.1 = ((bf16[16,128,256]{2,1,0:T(8,128)(2,1)}), bf16[16,128,256]{2,1,0:T(8,128)(2,1)S(1)}, u32[]{:S(2)}, u32[]{:S(2)}) async-start(bf16[16,128,256]{2,1,0:T(8,128)(2,1)} %broadcast_in_dim.7), calls=%async_computation.1 | async-start | bytes 2097152 | tf_op jit(solution)/shard_map/all_to_all | solution.py:16
  31.0 0.0 copy-done
  31.0 0.0 copy-done.4
  31.0 0.0 copy-start.1
  31.0 1.9 %fusion.2 = bf16[384,256]{1,0:T(8,128)(2,1)S(1)} fusion(bf16[384,2048]{1,0:T(8,128)(2,1)S(1)} %copy-done, bf16[2048,256]{1,0:T(8,128)(2,1)} %bitcast.73, bf16[384,256]{1,0:T(8,128)(2,1)S(1)} %copy-done.4), kind=kOutput, calls=%fused_computation.10 | convolution fusion | flops 403144704 | bytes 3014656 | tf_op jit(solution)/shard_map/dot_general | solution.py:29
  33.0 5.2 %collective-permute-start.1 = (bf16[384,256]{1,0:T(8,128)(2,1)S(1)}, bf16[384,256]{1,0:T(8,128)(2,1)S(1)}, u32[]{:S(2)}, u32[]{:S(2)}) collective-permute-start(bf16[384,256]{1,0:T(8,128)(2,1)S(1)} %fusion.2), channel_id=1, source_target_pairs={{0,1},{1,0},{2,3},{3,2},{4,5},{5,4},{6,7},{7,6},{8,9},{9,8},{10,11... | collective-permute-start | bytes 589832 | tf_op jit(solution)/shard_map/ppermute | solution.py:25
  38.1 0.0 copy-done.1
  38.2 0.7 fusion
  38.9 1.2 copy.34
  40.1 4.9 %all-to-all-done.1 = bf16[16,128,256]{2,1,0:T(8,128)(2,1)S(1)} async-done(((bf16[16,128,256]{2,1,0:T(8,128)(2,1)}), bf16[16,128,256]{2,1,0:T(8,128)(2,1)S(1)}, u32[]{:S(2)}, u32[]{:S(2)}) %all-to-all-start.1) | async-done | bytes 1048608 | tf_op jit(solution)/shard_map/all_to_all | solution.py:16
  45.0 4.3 %all-to-all-start.2 = ((bf16[16,256,128]{2,1,0:T(8,128)(2,1)}), bf16[16,256,128]{2,1,0:T(8,128)(2,1)}, u32[]{:S(2)}, u32[]{:S(2)}) async-start(bf16[16,256,128]{2,1,0:T(8,128)(2,1)} %bitcast.62), calls=%async_computation.2 | async-start | bytes 2097152 | tf_op jit(solution)/shard_map/all_to_all | solution.py:16
  49.4 0.1 fusion.16
  49.5 0.0 collective-permute-done.1
  49.5 0.4 fusion.17
  49.9 0.0 copy-start.5
  49.9 0.4 add_convert_fusion
  50.3 0.1 dynamic-slice_bitcast_fusion.2
  50.4 7.5 %collective-permute-start.2 = (bf16[96,1024]{1,0:T(8,128)(2,1)S(1)}, bf16[96,1024]{1,0:T(8,128)(2,1)S(1)}, u32[]{:S(2)}, u32[]{:S(2)}) collective-permute-start(bf16[96,1024]{1,0:T(8,128)(2,1)S(1)} %get-tuple-element.24), channel_id=1, source_target_pairs={{0,4},{2,6},{4,0},{6,2},{1,5},{3,7},{5,1},{7,3},{8,12},{10,14},{12... | collective-permute-start | bytes 589832 | tf_op jit(solution)/shard_map/ppermute | solution.py:44
  57.9 3.3 %collective-permute-start.4 = (bf16[96,1024]{1,0:T(8,128)(2,1)S(1)}, bf16[96,1024]{1,0:T(8,128)(2,1)S(1)}, u32[]{:S(2)}, u32[]{:S(2)}) collective-permute-start(bf16[96,1024]{1,0:T(8,128)(2,1)S(1)} %get-tuple-element.25), channel_id=1, source_target_pairs={{0,6},{2,0},{4,2},{6,4},{1,7},{3,1},{5,3},{7,5},{8,14},{10,8},{12,... | collective-permute-start | bytes 589832 | tf_op jit(solution)/shard_map/ppermute | solution.py:44
  61.2 2.2 %collective-permute-start.3 = (bf16[96,1024]{1,0:T(8,128)(2,1)S(1)}, bf16[96,1024]{1,0:T(8,128)(2,1)S(1)}, u32[]{:S(2)}, u32[]{:S(2)}) collective-permute-start(bf16[96,1024]{1,0:T(8,128)(2,1)S(1)} %get-tuple-element.26), channel_id=1, source_target_pairs={{0,2},{2,4},{4,6},{6,0},{1,3},{3,5},{5,7},{7,1},{8,10},{10,12},{12... | collective-permute-start | bytes 589832 | tf_op jit(solution)/shard_map/ppermute | solution.py:44
  63.4 0.0 copy-done.5
  63.4 0.7 fusion.1
  64.2 1.2 copy.33
  65.4 0.0 collective-permute-done.2
  65.4 1.9 %collective-permute-done.4 = bf16[96,1024]{1,0:T(8,128)(2,1)S(1)} collective-permute-done((bf16[96,1024]{1,0:T(8,128)(2,1)S(1)}, bf16[96,1024]{1,0:T(8,128)(2,1)S(1)}, u32[]{:S(2)}, u32[]{:S(2)}) %collective-permute-start.4) | collective-permute-done | bytes 196640 | tf_op jit(solution)/shard_map/ppermute | solution.py:44
  67.3 4.0 %collective-permute-done.3 = bf16[96,1024]{1,0:T(8,128)(2,1)S(1)} collective-permute-done((bf16[96,1024]{1,0:T(8,128)(2,1)S(1)}, bf16[96,1024]{1,0:T(8,128)(2,1)S(1)}, u32[]{:S(2)}, u32[]{:S(2)}) %collective-permute-start.3) | collective-permute-done | bytes 196640 | tf_op jit(solution)/shard_map/ppermute | solution.py:44
  71.2 0.1 fusion.5
  71.3 0.0 all-to-all-done.2
  71.3 6.3 %all-to-all-start.3 = ((bf16[16,256,128]{2,1,0:T(8,128)(2,1)}), bf16[16,256,128]{2,1,0:T(8,128)(2,1)S(1)}, u32[]{:S(2)}, u32[]{:S(2)}) async-start(bf16[16,256,128]{2,1,0:T(8,128)(2,1)} %bitcast.59), calls=%async_computation.3 | async-start | bytes 2097152 | tf_op jit(solution)/shard_map/all_to_all | solution.py:16
  77.7 1.4 convert_reduce_fusion.1
  79.1 39.2 %all-gather = bf16[3104,128]{1,0:T(8,128)(2,1)S(1)} all-gather(bf16[776,128]{1,0:T(8,128)(2,1)S(1)} %pad_maximum_fusion.1), channel_id=2, replica_groups=mesh['yh'=2,'yl'=2,'x'=4,'zh'=4,'zl'=4,'core'=2] {'zh'}, dimensions={0}, use_global_device_ids=true | all-gather | bytes 993280 | tf_op jit(solution)/shard_map/all_gather | solution.py:100
  118.3 0.1 convert_reduce_fusion.2
  118.5 16.6 %all_gather.11 = bf16[3104,128]{1,0:T(8,128)(2,1)S(1)} all-gather(bf16[776,128]{1,0:T(8,128)(2,1)S(1)} %pad_maximum_fusion.2), channel_id=1, replica_groups=mesh['yh'=2,'yl'=2,'x'=4,'zh'=4,'zl'=4,'core'=2] {'zl'}, dimensions={0}, use_global_device_ids=true | all-gather | bytes 993280 | tf_op jit(solution)/shard_map/all_gather | solution.py:105
  135.1 8.2 %collective-permute-start.5 = (bf16[3104,128]{1,0:T(8,128)(2,1)S(1)}, bf16[3104,128]{1,0:T(8,128)(2,1)}, u32[]{:S(2)}, u32[]{:S(2)}) collective-permute-start(bf16[3104,128]{1,0:T(8,128)(2,1)S(1)} %all_gather.11), channel_id=1, source_target_pairs={{0,1},{1,0},{2,3},{3,2},{4,5},{5,4},{6,7},{7,6},{8,9},{9,8},{10,11... | collective-permute-start | bytes 2383880 | tf_op jit(solution)/shard_map/ppermute | solution.py:25
  143.3 0.0 all-to-all-done.3
  143.3 0.1 convert_reduce_fusion
  143.5 0.0 copy-start.3
  143.5 0.6 copy-done.3
  144.1 0.1 multiply_reduce_fusion
  144.2 0.6 broadcast_in_dim.8
  144.9 8.5 %all-to-all-start.4 = ((f32[16,1,256]{2,1,0:T(1,128)}), f32[16,1,256]{2,1,0:T(1,128)S(1)}, u32[]{:S(2)}, u32[]{:S(2)}) async-start(f32[16,1,256]{2,1,0:T(1,128)} %broadcast_in_dim.8), calls=%async_computation.4 | async-start | bytes 32768 | tf_op jit(solution)/shard_map/all_to_all | solution.py:16
  153.3 6.4 %all-to-all-done.4 = f32[16,1,256]{2,1,0:T(1,128)S(1)} async-done(((f32[16,1,256]{2,1,0:T(1,128)}), f32[16,1,256]{2,1,0:T(1,128)S(1)}, u32[]{:S(2)}, u32[]{:S(2)}) %all-to-all-start.4) | async-done | bytes 16416 | tf_op jit(solution)/shard_map/all_to_all | solution.py:16
  159.8 0.6 reduce_sum.72
  160.4 0.8 copy.26
  161.1 0.0 collective-permute-done.5
  161.1 1.2 add_reduce_fusion
  162.3 1.2 broadcast_select_fusion.1
  163.6 1.2 pad_maximum_fusion
  (8 shorter events, 0.1 us)
Async XLA Ops:
  0.6 30.4 %copy-start = (bf16[384,2048]{1,0:T(8,128)(2,1)S(1)}, bf16[384,2048]{1,0:T(8,128)(2,1)}, u32[]{:S(2)}) copy-start(bf16[384,2048]{1,0:T(8,128)(2,1)} %param.7) | copy-start | bytes 4718596
  1.7 8.7 %copy-start.6 = (bf16[128,256]{1,0:T(8,128)(2,1)S(1)}, bf16[128,256]{1,0:T(8,128)(2,1)}, u32[]{:S(2)}) copy-start(bf16[128,256]{1,0:T(8,128)(2,1)} %param.8) | copy-start | bytes 196612
  2.8 22.1 %all-to-all-start = ((bf16[16,128,256]{2,1,0:T(8,128)(2,1)}), bf16[16,128,256]{2,1,0:T(8,128)(2,1)S(1)}, u32[]{:S(2)}, u32[]{:S(2)}) async-start(bf16[16,128,256]{2,1,0:T(8,128)(2,1)} %broadcast_in_dim.6), calls=%async_computation | async-start | bytes 2097152 | tf_op jit(solution)/shard_map/all_to_all | solution.py:16
  10.4 20.6 %copy-start.4 = (bf16[384,256]{1,0:T(8,128)(2,1)S(1)}, bf16[384,256]{1,0:T(8,128)(2,1)}, u32[]{:S(2)}) copy-start(bf16[384,256]{1,0:T(8,128)(2,1)} %param.6) | copy-start | bytes 589828
  10.4 12.6 %collective-permute-start = (bf16[128,256]{1,0:T(8,128)(2,1)S(1)}, bf16[128,256]{1,0:T(8,128)(2,1)S(1)}, u32[]{:S(2)}, u32[]{:S(2)}) collective-permute-start(bf16[128,256]{1,0:T(8,128)(2,1)S(1)} %copy-done.6), channel_id=1, source_target_pairs={{0,0},{1,256},{256,257},{257,1},{2,2},{3,258},{258,259},{259,3},{4... | collective-permute-start | bytes 196616 | tf_op jit(solution)/shard_map/ppermute | solution.py:86
  24.9 1.3 copy-start.2
  26.2 18.8 %all-to-all-start.1 = ((bf16[16,128,256]{2,1,0:T(8,128)(2,1)}), bf16[16,128,256]{2,1,0:T(8,128)(2,1)S(1)}, u32[]{:S(2)}, u32[]{:S(2)}) async-start(bf16[16,128,256]{2,1,0:T(8,128)(2,1)} %broadcast_in_dim.7), calls=%async_computation.1 | async-start | bytes 2097152 | tf_op jit(solution)/shard_map/all_to_all | solution.py:16
  31.0 7.1 %copy-start.1 = (bf16[384,2048]{1,0:T(8,128)(2,1)S(1)}, bf16[384,2048]{1,0:T(8,128)(2,1)}, u32[]{:S(2)}) copy-start(bf16[384,2048]{1,0:T(8,128)(2,1)} %param.5) | copy-start | bytes 4718596
  33.0 16.5 %collective-permute-start.1 = (bf16[384,256]{1,0:T(8,128)(2,1)S(1)}, bf16[384,256]{1,0:T(8,128)(2,1)S(1)}, u32[]{:S(2)}, u32[]{:S(2)}) collective-permute-start(bf16[384,256]{1,0:T(8,128)(2,1)S(1)} %fusion.2), channel_id=1, source_target_pairs={{0,1},{1,0},{2,3},{3,2},{4,5},{5,4},{6,7},{7,6},{8,9},{9,8},{10,11... | collective-permute-start | bytes 589832 | tf_op jit(solution)/shard_map/ppermute | solution.py:25
  45.0 26.3 %all-to-all-start.2 = ((bf16[16,256,128]{2,1,0:T(8,128)(2,1)}), bf16[16,256,128]{2,1,0:T(8,128)(2,1)}, u32[]{:S(2)}, u32[]{:S(2)}) async-start(bf16[16,256,128]{2,1,0:T(8,128)(2,1)} %bitcast.62), calls=%async_computation.2 | async-start | bytes 2097152 | tf_op jit(solution)/shard_map/all_to_all | solution.py:16
  49.9 13.5 %copy-start.5 = (bf16[384,256]{1,0:T(8,128)(2,1)S(1)}, bf16[384,256]{1,0:T(8,128)(2,1)}, u32[]{:S(2)}) copy-start(bf16[384,256]{1,0:T(8,128)(2,1)} %param.6) | copy-start | bytes 589828
  50.4 15.0 %collective-permute-start.2 = (bf16[96,1024]{1,0:T(8,128)(2,1)S(1)}, bf16[96,1024]{1,0:T(8,128)(2,1)S(1)}, u32[]{:S(2)}, u32[]{:S(2)}) collective-permute-start(bf16[96,1024]{1,0:T(8,128)(2,1)S(1)} %get-tuple-element.24), channel_id=1, source_target_pairs={{0,4},{2,6},{4,0},{6,2},{1,5},{3,7},{5,1},{7,3},{8,12},{10,14},{12... | collective-permute-start | bytes 589832 | tf_op jit(solution)/shard_map/ppermute | solution.py:44
  57.9 9.3 %collective-permute-start.4 = (bf16[96,1024]{1,0:T(8,128)(2,1)S(1)}, bf16[96,1024]{1,0:T(8,128)(2,1)S(1)}, u32[]{:S(2)}, u32[]{:S(2)}) collective-permute-start(bf16[96,1024]{1,0:T(8,128)(2,1)S(1)} %get-tuple-element.25), channel_id=1, source_target_pairs={{0,6},{2,0},{4,2},{6,4},{1,7},{3,1},{5,3},{7,5},{8,14},{10,8},{12,... | collective-permute-start | bytes 589832 | tf_op jit(solution)/shard_map/ppermute | solution.py:44
  61.2 10.0 %collective-permute-start.3 = (bf16[96,1024]{1,0:T(8,128)(2,1)S(1)}, bf16[96,1024]{1,0:T(8,128)(2,1)S(1)}, u32[]{:S(2)}, u32[]{:S(2)}) collective-permute-start(bf16[96,1024]{1,0:T(8,128)(2,1)S(1)} %get-tuple-element.26), channel_id=1, source_target_pairs={{0,2},{2,4},{4,6},{6,0},{1,3},{3,5},{5,7},{7,1},{8,10},{10,12},{12... | collective-permute-start | bytes 589832 | tf_op jit(solution)/shard_map/ppermute | solution.py:44
  71.3 72.0 %all-to-all-start.3 = ((bf16[16,256,128]{2,1,0:T(8,128)(2,1)}), bf16[16,256,128]{2,1,0:T(8,128)(2,1)S(1)}, u32[]{:S(2)}, u32[]{:S(2)}) async-start(bf16[16,256,128]{2,1,0:T(8,128)(2,1)} %bitcast.59), calls=%async_computation.3 | async-start | bytes 2097152 | tf_op jit(solution)/shard_map/all_to_all | solution.py:16
  135.1 26.0 %collective-permute-start.5 = (bf16[3104,128]{1,0:T(8,128)(2,1)S(1)}, bf16[3104,128]{1,0:T(8,128)(2,1)}, u32[]{:S(2)}, u32[]{:S(2)}) collective-permute-start(bf16[3104,128]{1,0:T(8,128)(2,1)S(1)} %all_gather.11), channel_id=1, source_target_pairs={{0,1},{1,0},{2,3},{3,2},{4,5},{5,4},{6,7},{7,6},{8,9},{9,8},{10,11... | collective-permute-start | bytes 2383880 | tf_op jit(solution)/shard_map/ppermute | solution.py:25
  143.5 0.7 copy-start.3
  144.9 14.9 %all-to-all-start.4 = ((f32[16,1,256]{2,1,0:T(1,128)}), f32[16,1,256]{2,1,0:T(1,128)S(1)}, u32[]{:S(2)}, u32[]{:S(2)}) async-start(f32[16,1,256]{2,1,0:T(1,128)} %broadcast_in_dim.8), calls=%async_computation.4 | async-start | bytes 32768 | tf_op jit(solution)/shard_map/all_to_all | solution.py:16

commit v13 on v12

--- a/solution.py
+++ b/solution.py
@@ -37,10 +37,10 @@
     pieces = half.reshape(count, half.shape[0] // count, half.shape[1])
     total = lax.dynamic_index_in_dim(pieces, here, 0, False).astype(F32)
     others = []
-    for step in (2, 1, 3):
-        there = lax.rem(here + step, count)
+    for step in (2, 3, 1):
+        there = lax.bitwise_xor(here, step)
         piece = lax.dynamic_index_in_dim(pieces, there, 0, False)
-        ring = [(i, (i + step) % count) for i in range(count)]
+        ring = [(i, i ^ step) for i in range(count)]
         others.append(lax.ppermute(piece, axis, ring))
     for other in others:
         total += other.astype(F32)

time: 166 us -> 168 us (1.012)
  local copies, waits for them, and re-layouts: 8.15 us -> 11 us
  starting transfers between devices: 65.7 us -> 63.3 us
    all_gather x1, blocking collectives: 16.6 us -> 26.3 us  [local(): half = lax.all_gather(quarter, 'zl', axis=0, tiled=True)]
    all_gather x1, blocking collectives: 39.2 us -> 30.8 us  [local(): groups = lax.all_gather(quarter, 'zh', axis=0, tiled=False)]
    ppermute x2, starting transfers between devices: 13.4 us -> 11.1 us  [other_core(): return lax.ppermute(array, 'core', [(0, 1), (1, 0)])]
    convert_element_type x1, other arithmetic: 0.13 us -> 1.9 us  [sum_near(): return total.astype(BF)]
  transfers between devices with their start and end apart: 11 -> 11, of which waited for: 6 -> 7; matrix products, arithmetic and copies ran while one was open for 7% -> 9% of each run, Pallas kernels for 0% -> 0%
where the time goes in v13:
time: 168 us; the launch traced here: 167 us
  starting transfers between devices  63.3 us (38%)
  blocking collectives  57.1 us (34%)
  waiting for transfers between devices  24.2 us (14%)
  local copies, waits for them, and re-layouts  11 us (7%)
  other arithmetic  6.25 us (4%)
  matrix products  4.18 us (2%)
    all_to_all x5, starting transfers between devices, exchange(): return lax.all_to_all(array, axes, 0, 0, tiled=True)  30.8 us
    all_gather x1, blocking collectives, local(): groups = lax.all_gather(quarter, 'zh', axis=0, tiled=False)  30.8 us
    all_gather x1, blocking collectives, local(): half = lax.all_gather(quarter, 'zl', axis=0, tiled=True)  26.3 us
    ppermute x3, starting transfers between devices, sum_near(): others.append(lax.ppermute(piece, axis, ring))  13.4 us
    all_to_all x5, waiting for transfers between devices, exchange(): return lax.all_to_all(array, axes, 0, 0, tiled=True)  13.3 us
    ppermute x2, starting transfers between devices, other_core(): return lax.ppermute(array, 'core', [(0, 1), (1, 0)])  11.1 us
    ppermute x1, starting transfers between devices, local(): lax.ppermute(up_weight, ('yh', 'core'), [(0, 0), (1, 2), (2, 3), (3, 1)])  7.92 us
    ppermute x3, waiting for transfers between devices, sum_near(): others.append(lax.ppermute(piece, axis, ring))  6.26 us
  transfers between devices with their start and end apart: 11, of which 7 were waited for; matrix products, arithmetic and copies ran while one was open for 9% of the time, Pallas kernels for 0%

profile of v13, /device:TPU:1, one launch (start us, length us, event | category | flops | bytes accessed | tf_op | source)
XLA Modules:
  0.0 166.9 jit_solution(5180819409684601438)
XLA Ops:
  0.6 0.0 copy-start
  0.6 1.1 copy.21
  1.7 0.0 copy-start.10
  1.7 1.1 broadcast_in_dim.6
  2.8 7.6 %all-to-all-start = ((bf16[16,128,256]{2,1,0:T(8,128)(2,1)}), bf16[16,128,256]{2,1,0:T(8,128)(2,1)S(1)}, u32[]{:S(2)}, u32[]{:S(2)}) async-start(bf16[16,128,256]{2,1,0:T(8,128)(2,1)} %broadcast_in_dim.6), calls=%async_computation | async-start | bytes 2097152 | tf_op jit(solution)/shard_map/all_to_all | solution.py:16
  10.4 0.0 copy-done.10
  10.4 0.0 copy-start.8
  10.4 7.9 %collective-permute-start = (bf16[128,256]{1,0:T(8,128)(2,1)S(1)}, bf16[128,256]{1,0:T(8,128)(2,1)S(1)}, u32[]{:S(2)}, u32[]{:S(2)}) collective-permute-start(bf16[128,256]{1,0:T(8,128)(2,1)S(1)} %copy-done.10), channel_id=1, source_target_pairs={{0,0},{1,256},{256,257},{257,1},{2,2},{3,258},{258,259},{259,3},{4... | collective-permute-start | bytes 196616 | tf_op jit(solution)/shard_map/ppermute | solution.py:86
  18.3 4.6 %collective-permute-done = bf16[128,256]{1,0:T(8,128)(2,1)S(1)} collective-permute-done((bf16[128,256]{1,0:T(8,128)(2,1)S(1)}, bf16[128,256]{1,0:T(8,128)(2,1)S(1)}, u32[]{:S(2)}, u32[]{:S(2)}) %collective-permute-start) | collective-permute-done | bytes 65568 | tf_op jit(solution)/shard_map/ppermute | solution.py:86
  23.0 1.9 %all-to-all-done = bf16[16,128,256]{2,1,0:T(8,128)(2,1)S(1)} async-done(((bf16[16,128,256]{2,1,0:T(8,128)(2,1)}), bf16[16,128,256]{2,1,0:T(8,128)(2,1)S(1)}, u32[]{:S(2)}, u32[]{:S(2)}) %all-to-all-start) | async-done | bytes 1048608 | tf_op jit(solution)/shard_map/all_to_all | solution.py:16
  24.9 1.1 broadcast_in_dim.7
  26.1 0.2 copy-done.3
  26.2 4.7 %all-to-all-start.1 = ((bf16[16,128,256]{2,1,0:T(8,128)(2,1)}), bf16[16,128,256]{2,1,0:T(8,128)(2,1)S(1)}, u32[]{:S(2)}, u32[]{:S(2)}) async-start(bf16[16,128,256]{2,1,0:T(8,128)(2,1)} %broadcast_in_dim.7), calls=%async_computation.1 | async-start | bytes 2097152 | tf_op jit(solution)/shard_map/all_to_all | solution.py:16
  31.0 0.0 copy-done
  31.0 0.0 copy-done.8
  31.0 0.0 copy-start.2
  31.0 1.9 %fusion.2 = bf16[384,256]{1,0:T(8,128)(2,1)S(1)} fusion(bf16[384,2048]{1,0:T(8,128)(2,1)S(1)} %copy-done, bf16[2048,256]{1,0:T(8,128)(2,1)} %bitcast.74, bf16[384,256]{1,0:T(8,128)(2,1)S(1)} %copy-done.8), kind=kOutput, calls=%fused_computation.10 | convolution fusion | flops 403144704 | bytes 3014656 | tf_op jit(solution)/shard_map/dot_general | solution.py:29
  33.0 0.0 copy-start.5
  33.0 5.2 %collective-permute-start.1 = (bf16[384,256]{1,0:T(8,128)(2,1)S(1)}, bf16[384,256]{1,0:T(8,128)(2,1)S(1)}, u32[]{:S(2)}, u32[]{:S(2)}) collective-permute-start(bf16[384,256]{1,0:T(8,128)(2,1)S(1)} %fusion.2), channel_id=1, source_target_pairs={{0,1},{1,0},{2,3},{3,2},{4,5},{5,4},{6,7},{7,6},{8,9},{9,8},{10,11... | collective-permute-start | bytes 589832 | tf_op jit(solution)/shard_map/ppermute | solution.py:25
  38.2 0.0 copy-done.2
  38.2 0.7 fusion
  38.9 1.2 copy.34
  40.1 0.0 copy-done.5
  40.1 4.9 %all-to-all-done.1 = bf16[16,128,256]{2,1,0:T(8,128)(2,1)S(1)} async-done(((bf16[16,128,256]{2,1,0:T(8,128)(2,1)}), bf16[16,128,256]{2,1,0:T(8,128)(2,1)S(1)}, u32[]{:S(2)}, u32[]{:S(2)}) %all-to-all-start.1) | async-done | bytes 1048608 | tf_op jit(solution)/shard_map/all_to_all | solution.py:16
  45.1 1.0 copy-done.1
  46.0 3.8 %all-to-all-start.2 = ((bf16[16,256,128]{2,1,0:T(8,128)(2,1)}), bf16[16,256,128]{2,1,0:T(8,128)(2,1)S(1)}, u32[]{:S(2)}, u32[]{:S(2)}) async-start(bf16[16,256,128]{2,1,0:T(8,128)(2,1)} %bitcast.62), calls=%async_computation.2 | async-start | bytes 2097152 | tf_op jit(solution)/shard_map/all_to_all | solution.py:16
  49.9 1.3 fusion.16
  51.1 0.0 copy-start.6
  51.1 0.0 collective-permute-done.1
  51.2 0.4 fusion.17
  51.6 0.5 copy-done.6
  52.1 0.4 add_convert_fusion
  52.5 0.8 dynamic-slice_bitcast_fusion.2
  53.3 8.0 %collective-permute-start.2 = (bf16[96,1024]{1,0:T(8,128)(2,1)}, bf16[96,1024]{1,0:T(8,128)(2,1)}, u32[]{:S(2)}, u32[]{:S(2)}) collective-permute-start(bf16[96,1024]{1,0:T(8,128)(2,1)} %get-tuple-element.24), channel_id=1, source_target_pairs={{0,4},{2,6},{4,0},{6,2},{1,5},{3,7},{5,1},{7,3},{8,12},{10,14},{12... | collective-permute-start | bytes 589832 | tf_op jit(solution)/shard_map/ppermute | solution.py:44
  61.3 3.5 %collective-permute-start.4 = (bf16[96,1024]{1,0:T(8,128)(2,1)}, bf16[96,1024]{1,0:T(8,128)(2,1)}, u32[]{:S(2)}, u32[]{:S(2)}) collective-permute-start(bf16[96,1024]{1,0:T(8,128)(2,1)} %get-tuple-element.25), channel_id=1, source_target_pairs={{0,2},{2,0},{4,6},{6,4},{1,3},{3,1},{5,7},{7,5},{8,10},{10,8},{12,... | collective-permute-start | bytes 589832 | tf_op jit(solution)/shard_map/ppermute | solution.py:44
  64.8 1.9 %collective-permute-start.3 = (bf16[96,1024]{1,0:T(8,128)(2,1)}, bf16[96,1024]{1,0:T(8,128)(2,1)}, u32[]{:S(2)}, u32[]{:S(2)}) collective-permute-start(bf16[96,1024]{1,0:T(8,128)(2,1)} %get-tuple-element.26), channel_id=1, source_target_pairs={{0,6},{2,4},{4,2},{6,0},{1,7},{3,5},{5,3},{7,1},{8,14},{10,12},{12... | collective-permute-start | bytes 589832 | tf_op jit(solution)/shard_map/ppermute | solution.py:44
  66.8 0.7 fusion.1
  67.5 1.2 copy.33
  68.8 0.3 collective-permute-done.2
  69.0 2.6 %collective-permute-done.4 = bf16[96,1024]{1,0:T(8,128)(2,1)} collective-permute-done((bf16[96,1024]{1,0:T(8,128)(2,1)}, bf16[96,1024]{1,0:T(8,128)(2,1)}, u32[]{:S(2)}, u32[]{:S(2)}) %collective-permute-start.4) | collective-permute-done | bytes 196640 | tf_op jit(solution)/shard_map/ppermute | solution.py:44
  71.6 3.4 %collective-permute-done.3 = bf16[96,1024]{1,0:T(8,128)(2,1)} collective-permute-done((bf16[96,1024]{1,0:T(8,128)(2,1)}, bf16[96,1024]{1,0:T(8,128)(2,1)}, u32[]{:S(2)}, u32[]{:S(2)}) %collective-permute-start.3) | collective-permute-done | bytes 196640 | tf_op jit(solution)/shard_map/ppermute | solution.py:44
  75.0 1.9 %fusion.5 = bf16[96,1024]{1,0:T(8,128)(2,1)} fusion(bf16[96,1024]{1,0:T(8,128)(2,1)} %collective-permute-done.4, bf16[96,1024]{1,0:T(8,128)(2,1)} %collective-permute-done.3, bf16[96,1024]{1,0:T(8,128)(2,1)} %collective-permute-done.2, bf16[4,96,1024]{2,1,0:T(8,128)(2,1)S(1)} %bitcast.68, s32[]{:T(128)S(6)} %select_n.26), kind=kLoop, calls=%fused_computation.19 | loop fusion | flops 786432 | bytes 983044 | tf_op jit(solution)/shard_map/convert_element_type | solution.py:47
  76.9 0.0 all-to-all-done.2
  76.9 6.7 %all-to-all-start.3 = ((bf16[16,256,128]{2,1,0:T(8,128)(2,1)}), bf16[16,256,128]{2,1,0:T(8,128)(2,1)}, u32[]{:S(2)}, u32[]{:S(2)}) async-start(bf16[16,256,128]{2,1,0:T(8,128)(2,1)} %bitcast.63), calls=%async_computation.3 | async-start | bytes 2097152 | tf_op jit(solution)/shard_map/all_to_all | solution.py:16
  83.6 0.1 convert_reduce_fusion.1
  83.8 0.0 copy-done.4
  83.8 30.8 %all-gather = bf16[3104,128]{1,0:T(8,128)(2,1)S(1)} all-gather(bf16[776,128]{1,0:T(8,128)(2,1)S(1)} %pad_maximum_fusion.1), channel_id=2, replica_groups=mesh['yh'=2,'yl'=2,'x'=4,'zh'=4,'zl'=4,'core'=2] {'zh'}, dimensions={0}, use_global_device_ids=true | all-gather | bytes 993280 | tf_op jit(solution)/shard_map/all_gather | solution.py:100
  114.6 0.1 convert_reduce_fusion.2
  114.8 26.3 %all_gather.11 = bf16[3104,128]{1,0:T(8,128)(2,1)S(1)} all-gather(bf16[776,128]{1,0:T(8,128)(2,1)S(1)} %pad_maximum_fusion.2), channel_id=1, replica_groups=mesh['yh'=2,'yl'=2,'x'=4,'zh'=4,'zl'=4,'core'=2] {'zl'}, dimensions={0}, use_global_device_ids=true | all-gather | bytes 993280 | tf_op jit(solution)/shard_map/all_gather | solution.py:105
  141.1 6.0 %collective-permute-start.5 = (bf16[3104,128]{1,0:T(8,128)(2,1)S(1)}, bf16[3104,128]{1,0:T(8,128)(2,1)S(1)}, u32[]{:S(2)}, u32[]{:S(2)}) collective-permute-start(bf16[3104,128]{1,0:T(8,128)(2,1)S(1)} %all_gather.11), channel_id=1, source_target_pairs={{0,1},{1,0},{2,3},{3,2},{4,5},{5,4},{6,7},{7,6},{8,9},{9,8},{10,11... | collective-permute-start | bytes 2383880 | tf_op jit(solution)/shard_map/ppermute | solution.py:25
  147.1 0.0 all-to-all-done.3
  147.1 1.4 convert_reduce_fusion
  148.5 0.0 copy-start.7
  148.5 0.1 multiply_reduce_fusion
  148.6 0.6 broadcast_in_dim.8
  149.2 8.0 %all-to-all-start.4 = ((f32[16,1,256]{2,1,0:T(1,128)}), f32[16,1,256]{2,1,0:T(1,128)S(1)}, u32[]{:S(2)}, u32[]{:S(2)}) async-start(f32[16,1,256]{2,1,0:T(1,128)} %broadcast_in_dim.8), calls=%async_computation.4 | async-start | bytes 32768 | tf_op jit(solution)/shard_map/all_to_all | solution.py:16
  157.2 6.4 %all-to-all-done.4 = f32[16,1,256]{2,1,0:T(1,128)S(1)} async-done(((f32[16,1,256]{2,1,0:T(1,128)}), f32[16,1,256]{2,1,0:T(1,128)S(1)}, u32[]{:S(2)}, u32[]{:S(2)}) %all-to-all-start.4) | async-done | bytes 16416 | tf_op jit(solution)/shard_map/all_to_all | solution.py:16
  163.7 0.6 reduce_sum.72
  164.3 0.8 copy.26
  165.0 0.0 collective-permute-done.5
  165.0 0.5 add_reduce_fusion
  165.5 0.1 broadcast_select_fusion.1
  165.7 0.0 copy-done.7
  165.7 1.2 pad_maximum_fusion
  (13 shorter events, 0.2 us)
Async XLA Ops:
  0.6 30.4 %copy-start = (bf16[384,2048]{1,0:T(8,128)(2,1)S(1)}, bf16[384,2048]{1,0:T(8,128)(2,1)}, u32[]{:S(2)}) copy-start(bf16[384,2048]{1,0:T(8,128)(2,1)} %param.7) | copy-start | bytes 4718596
  1.7 8.7 %copy-start.10 = (bf16[128,256]{1,0:T(8,128)(2,1)S(1)}, bf16[128,256]{1,0:T(8,128)(2,1)}, u32[]{:S(2)}) copy-start(bf16[128,256]{1,0:T(8,128)(2,1)} %param.8) | copy-start | bytes 196612
  2.8 22.1 %all-to-all-start = ((bf16[16,128,256]{2,1,0:T(8,128)(2,1)}), bf16[16,128,256]{2,1,0:T(8,128)(2,1)S(1)}, u32[]{:S(2)}, u32[]{:S(2)}) async-start(bf16[16,128,256]{2,1,0:T(8,128)(2,1)} %broadcast_in_dim.6), calls=%async_computation | async-start | bytes 2097152 | tf_op jit(solution)/shard_map/all_to_all | solution.py:16
  10.4 20.6 %copy-start.8 = (bf16[384,256]{1,0:T(8,128)(2,1)S(1)}, bf16[384,256]{1,0:T(8,128)(2,1)}, u32[]{:S(2)}) copy-start(bf16[384,256]{1,0:T(8,128)(2,1)} %param.6) | copy-start | bytes 589828
  10.4 12.6 %collective-permute-start = (bf16[128,256]{1,0:T(8,128)(2,1)S(1)}, bf16[128,256]{1,0:T(8,128)(2,1)S(1)}, u32[]{:S(2)}, u32[]{:S(2)}) collective-permute-start(bf16[128,256]{1,0:T(8,128)(2,1)S(1)} %copy-done.10), channel_id=1, source_target_pairs={{0,0},{1,256},{256,257},{257,1},{2,2},{3,258},{258,259},{259,3},{4... | collective-permute-start | bytes 196616 | tf_op jit(solution)/shard_map/ppermute | solution.py:86
  24.9 1.3 copy-start.3
  26.2 18.8 %all-to-all-start.1 = ((bf16[16,128,256]{2,1,0:T(8,128)(2,1)}), bf16[16,128,256]{2,1,0:T(8,128)(2,1)S(1)}, u32[]{:S(2)}, u32[]{:S(2)}) async-start(bf16[16,128,256]{2,1,0:T(8,128)(2,1)} %broadcast_in_dim.7), calls=%async_computation.1 | async-start | bytes 2097152 | tf_op jit(solution)/shard_map/all_to_all | solution.py:16
  31.0 7.1 %copy-start.2 = (bf16[384,2048]{1,0:T(8,128)(2,1)S(1)}, bf16[384,2048]{1,0:T(8,128)(2,1)}, u32[]{:S(2)}) copy-start(bf16[384,2048]{1,0:T(8,128)(2,1)} %param.5) | copy-start | bytes 4718596
  33.0 7.2 %copy-start.5 = (bf16[384,256]{1,0:T(8,128)(2,1)}, bf16[384,256]{1,0:T(8,128)(2,1)S(1)}, u32[]{:S(2)}) copy-start(bf16[384,256]{1,0:T(8,128)(2,1)S(1)} %fusion.2) | copy-start | bytes 589828
  33.0 18.2 %collective-permute-start.1 = (bf16[384,256]{1,0:T(8,128)(2,1)S(1)}, bf16[384,256]{1,0:T(8,128)(2,1)S(1)}, u32[]{:S(2)}, u32[]{:S(2)}) collective-permute-start(bf16[384,256]{1,0:T(8,128)(2,1)S(1)} %fusion.2), channel_id=1, source_target_pairs={{0,1},{1,0},{2,3},{3,2},{4,5},{5,4},{6,7},{7,6},{8,9},{9,8},{10,11... | collective-permute-start | bytes 589832 | tf_op jit(solution)/shard_map/ppermute | solution.py:25
  45.0 1.0 copy-start.1
  46.0 30.9 %all-to-all-start.2 = ((bf16[16,256,128]{2,1,0:T(8,128)(2,1)}), bf16[16,256,128]{2,1,0:T(8,128)(2,1)S(1)}, u32[]{:S(2)}, u32[]{:S(2)}) async-start(bf16[16,256,128]{2,1,0:T(8,128)(2,1)} %bitcast.62), calls=%async_computation.2 | async-start | bytes 2097152 | tf_op jit(solution)/shard_map/all_to_all | solution.py:16
  51.1 0.9 copy-start.6
  52.1 14.7 %copy-start.9 = (bf16[384,256]{1,0:T(8,128)(2,1)S(1)}, bf16[384,256]{1,0:T(8,128)(2,1)}, u32[]{:S(2)}) copy-start(bf16[384,256]{1,0:T(8,128)(2,1)} %param.6) | copy-start | bytes 589828
  53.3 15.7 %collective-permute-start.2 = (bf16[96,1024]{1,0:T(8,128)(2,1)}, bf16[96,1024]{1,0:T(8,128)(2,1)}, u32[]{:S(2)}, u32[]{:S(2)}) collective-permute-start(bf16[96,1024]{1,0:T(8,128)(2,1)} %get-tuple-element.24), channel_id=1, source_target_pairs={{0,4},{2,6},{4,0},{6,2},{1,5},{3,7},{5,1},{7,3},{8,12},{10,14},{12... | collective-permute-start | bytes 589832 | tf_op jit(solution)/shard_map/ppermute | solution.py:44
  61.3 10.3 %collective-permute-start.4 = (bf16[96,1024]{1,0:T(8,128)(2,1)}, bf16[96,1024]{1,0:T(8,128)(2,1)}, u32[]{:S(2)}, u32[]{:S(2)}) collective-permute-start(bf16[96,1024]{1,0:T(8,128)(2,1)} %get-tuple-element.25), channel_id=1, source_target_pairs={{0,2},{2,0},{4,6},{6,4},{1,3},{3,1},{5,7},{7,5},{8,10},{10,8},{12,... | collective-permute-start | bytes 589832 | tf_op jit(solution)/shard_map/ppermute | solution.py:44
  64.8 10.2 %collective-permute-start.3 = (bf16[96,1024]{1,0:T(8,128)(2,1)}, bf16[96,1024]{1,0:T(8,128)(2,1)}, u32[]{:S(2)}, u32[]{:S(2)}) collective-permute-start(bf16[96,1024]{1,0:T(8,128)(2,1)} %get-tuple-element.26), channel_id=1, source_target_pairs={{0,6},{2,4},{4,2},{6,0},{1,7},{3,5},{5,3},{7,1},{8,14},{10,12},{12... | collective-permute-start | bytes 589832 | tf_op jit(solution)/shard_map/ppermute | solution.py:44
  76.9 6.9 %copy-start.4 = (bf16[96,1024]{1,0:T(8,128)(2,1)S(1)}, bf16[96,1024]{1,0:T(8,128)(2,1)}, u32[]{:S(2)}) copy-start(bf16[96,1024]{1,0:T(8,128)(2,1)} %fusion.5) | copy-start | bytes 589828
  76.9 70.2 %all-to-all-start.3 = ((bf16[16,256,128]{2,1,0:T(8,128)(2,1)}), bf16[16,256,128]{2,1,0:T(8,128)(2,1)}, u32[]{:S(2)}, u32[]{:S(2)}) async-start(bf16[16,256,128]{2,1,0:T(8,128)(2,1)} %bitcast.63), calls=%async_computation.3 | async-start | bytes 2097152 | tf_op jit(solution)/shard_map/all_to_all | solution.py:16
  141.1 23.9 %collective-permute-start.5 = (bf16[3104,128]{1,0:T(8,128)(2,1)S(1)}, bf16[3104,128]{1,0:T(8,128)(2,1)S(1)}, u32[]{:S(2)}, u32[]{:S(2)}) collective-permute-start(bf16[3104,128]{1,0:T(8,128)(2,1)S(1)} %all_gather.11), channel_id=1, source_target_pairs={{0,1},{1,0},{2,3},{3,2},{4,5},{5,4},{6,7},{7,6},{8,9},{9,8},{10,11... | collective-permute-start | bytes 2383880 | tf_op jit(solution)/shard_map/ppermute | solution.py:25
  148.5 17.2 %copy-start.7 = (f32[256,128]{1,0:T(8,128)}, f32[256,128]{1,0:T(8,128)S(1)}, u32[]{:S(2)}) copy-start(f32[256,128]{1,0:T(8,128)S(1)} %convert_reduce_fusion) | copy-start | bytes 393220
  149.2 14.4 %all-to-all-start.4 = ((f32[16,1,256]{2,1,0:T(1,128)}), f32[16,1,256]{2,1,0:T(1,128)S(1)}, u32[]{:S(2)}, u32[]{:S(2)}) async-start(f32[16,1,256]{2,1,0:T(1,128)} %broadcast_in_dim.8), calls=%async_computation.4 | async-start | bytes 32768 | tf_op jit(solution)/shard_map/all_to_all | solution.py:16
